TPU v7x, 512 devices: a whole 4x4x16 slice. The times are simulated.
512 devices in a mesh: rep: 2 (over z_hi), fs: 32 (over z_lo, y), tp: 8 (over x, core).
Axes of the slice: x: 4, y: 4, z: 16 (z_hi: 2, z_lo: 8; z = z_hi * 8 + z_lo), core: 2. Of those that a mesh axis runs over, the one named last changes fastest.
Arguments:
- inputs: bfloat16 [8192, 2048], P(('rep', 'fs'), 'tp'), may hold values from -6 to 6
- cotangent: bfloat16 [8192, 2048], P(('rep', 'fs'), 'tp'), may hold values from -8 to 8
- gate_weight: bfloat16 [2048, 2816], P('fs', 'tp'), may hold values from -0.125 to 0.125
- up_weight: bfloat16 [2048, 2816], P('fs', 'tp'), may hold values from -0.125 to 0.125
- down_weight: bfloat16 [2816, 2048], P('tp', 'fs'), may hold values from -0.109375 to 0.109375
Outputs:
- grad_inputs: bfloat16 [8192, 2048], P(('rep', 'fs'), 'tp')
- grad_gate_weight: float32 [2048, 2816], P('fs', 'tp')
- grad_up_weight: float32 [2048, 2816], P('fs', 'tp')
- grad_down_weight: float32 [2816, 2048], P('tp', 'fs')
All inputs are finite; a program needn't handle non-finite values.
Results may differ from a plain program's by a relative error of at most 0.014.
Values may be sent and summed in bfloat16 or wider, within the bound.
No kernel may reach another device: no remote copies, remote signals or barrier semaphores. Data moves between devices by JAX's collectives and lax.ppermute only.
A program may use at most 64 MiB of HBM per device.

v0:
```python
import jax
import jax.numpy as jnp
from jax import lax
from jax.experimental import pallas as pl
from jax.experimental.pallas import tpu as pltpu
from jax.sharding import Mesh, PartitionSpec as P


BF = jnp.bfloat16
F32 = jnp.float32
NR, NY, NX, NC = 4, 4, 4, 2
PLANE = ("y", "x", "c")
QUADS = ("zh", "zq")
VM = pl.BlockSpec(memory_space=pltpu.VMEM)
NN = ((1,), (0,))
NT = ((1,), (1,))


def swapped(value, axis):
    return lax.ppermute(value, axis, [(0, 1), (1, 0)])


def moved(value, k, x_core):
    pairs = []
    for y in range(NY):
        for x in range(NX):
            for c in range(NC):
                ty, tx = (y, (x + k) % NX) if c == x_core else ((y + k) % NY, x)
                pairs.append(((y * NX + x) * NC + c, (ty * NX + tx) * NC + c))
    return lax.ppermute(value, PLANE, pairs)


def line_gather(value, x_core):
    return jnp.stack([value] + [moved(value, -k, x_core) for k in (1, 2, 3)])


def line_sum(value, x_core):
    total = value[0].astype(F32)
    for k in (1, 2, 3):
        total = total + moved(value[k], k, x_core).astype(F32)
    return total.astype(BF)


def dot(a, b, dims):
    return lax.dot_general(a, b, (dims, ((), ())), preferred_element_type=F32)


def sides(a, b):
    return jnp.concatenate([a, b], axis=1)


def call(body, args, shapes, scratch=(), mib=8):
    single = not isinstance(shapes, (list, tuple))
    return pl.pallas_call(
        body,
        in_specs=[VM] * len(args),
        out_specs=VM if single else [VM] * len(shapes),
        out_shape=shapes,
        scratch_shapes=scratch,
        compiler_params=pltpu.CompilerParams(vmem_limit_bytes=mib * 2**20),
    )(*args)


def pack_body(wg, wu, wd, out):
    hid = wd.shape[1] // NY
    tg = wg[...].astype(F32).T
    tu = wu[...].astype(F32).T
    td = wd[...].astype(F32).T
    parts = []
    for y in range(NY):
        s = slice(y * hid, (y + 1) * hid)
        parts.append(jnp.concatenate([tg[s], tu[s], td[s]], axis=0))
    out[0] = sides(parts[0], parts[2]).astype(BF)
    out[1] = sides(parts[1], parts[3]).astype(BF)


def spread_body(own, far, out):
    half = own.shape[2] // 2
    for i in range(2):
        o, f = own[i].astype(F32), far[i].astype(F32)
        low = sides(o[:, :half], f[:, :half]).astype(BF)
        high = sides(o[:, half:], f[:, half:]).astype(BF)
        for r in range(NR):
            out[r * NY + i] = low
            out[r * NY + i + 2] = high


def layer_body(mine, other, chunks, keep, send, pieces, wt):
    core = lax.axis_index("c")
    zq = lax.axis_index("zq")
    x_here = lax.axis_index("x")
    hid = chunks.shape[1] // 3
    half = chunks.shape[2] // 2

    def x_of(side, r):
        return (2 * (zq if side == 0 else 1 - zq) + r // NC + NX - x_here) % NX

    for r in range(NR):
        for side in range(2):
            cut = slice(side * half, (side + 1) * half)
            wt[2 * r + side] = jnp.concatenate(
                [chunks[r * NY + y][:, cut] for y in range(NY)], axis=1
            )

    def run(inputs, cotan, me):
        def tokens(part):
            return part.reshape(NY * part.shape[1], part.shape[2])

        def in_block(side, r):
            return tokens(inputs[:, x_of(side, r), r % NC])

        def co_block(side, r):
            return tokens(cotan[x_of(side, r), :, 1 - r % NC])

        pre = None
        hid_grad = None
        for r in range(NR):
            for side in range(2):
                p = dot(wt[2 * r + side, : 2 * hid, :], in_block(side, r), NT)
                q = dot(wt[2 * r + side, 2 * hid :, :], co_block(side, r), NT)
                pre = p if pre is None else pre + p
                hid_grad = q if hid_grad is None else hid_grad + q
        gate = pre[:hid]
        up = pre[hid:]
        sig = jax.nn.sigmoid(gate)
        act = gate * sig
        hidden = (act * up).astype(BF)
        g_gate = hid_grad * up * sig * (1.0 + gate * (1.0 - sig))
        g_up = hid_grad * act
        g_both = jnp.concatenate([g_gate, g_up], axis=0)
        g_turned = g_both.T.astype(BF)
        g_both = g_both.astype(BF)
        for r in range(NR):
            made = []
            for side in range(2):
                pw = dot(g_both, in_block(side, r), NN)
                pd = dot(hidden, co_block(side, r), NN)
                made.append(jnp.concatenate([pw, pd], axis=0))
                gi = dot(g_turned, wt[2 * r + side, : 2 * hid, :], NN).astype(BF)
                rows = gi.shape[0] // NY
                x = x_of(side, r)
                ref = keep if r % NC == me else send
                x_first = (r % NC) == 0
                for y in range(NY):
                    piece = gi[y * rows : (y + 1) * rows]
                    if x_first:
                        ref[x, y] = piece
                    else:
                        ref[y, x] = piece
            for y in range(NY):
                s = slice(y * half, (y + 1) * half)
                pieces[r * NY + y] = sides(made[0][:, s], made[1][:, s]).astype(BF)

    @pl.when(core == 0)
    def _():
        run(mine, other, 0)

    @pl.when(core == 1)
    def _():
        run(other, mine, 1)


def quad_body(pieces, out):
    zq = lax.axis_index("zq")
    half = pieces.shape[2] // 2

    def total(y):
        s = pieces[y].astype(F32)
        for r in range(1, NR):
            s = s + pieces[r * NY + y].astype(F32)
        return s

    for i in range(2):
        low, high = total(i), total(i + 2)
        own = sides(low[:, :half], high[:, :half]).astype(BF)
        far = sides(low[:, half:], high[:, half:]).astype(BF)
        for h in range(2):
            out[2 * h + zq, i] = own
            out[2 * h + 1 - zq, i] = far


def last_body(parts, gg, gu, gd):
    hid = parts.shape[2] // 3
    half = parts.shape[3] // 2
    s = []
    for i in range(2):
        v = parts[0, i].astype(F32)
        for q in range(1, 4):
            v = v + parts[q, i].astype(F32)
        s.append(v)
    by_y = [s[0][:, :half], s[1][:, :half], s[0][:, half:], s[1][:, half:]]
    gg[...] = jnp.concatenate([b[:hid] for b in by_y], axis=0).T
    gu[...] = jnp.concatenate([b[hid : 2 * hid] for b in by_y], axis=0).T
    gd[...] = jnp.concatenate([b[2 * hid :] for b in by_y], axis=0).T


def per_device(inputs, cotangent, gate_weight, up_weight, down_weight):
    S = jax.ShapeDtypeStruct
    rows_d, ff = gate_weight.shape
    hid = ff // NY
    rows, cols = inputs.shape

    first = lax.axis_index("c") == 0
    kept = jnp.where(first, inputs, cotangent)
    given = jnp.where(first, cotangent, inputs)
    got = swapped(given, "c")
    block = jnp.stack([kept, got])

    packed = call(pack_body, (gate_weight, up_weight, down_weight.T), S((2, 3 * hid, 2 * rows_d), BF))
    far = swapped(packed, "zq")
    chunks = call(spread_body, (packed, far), S((NR * NY, 3 * hid, 2 * rows_d), BF))
    chunks = lax.all_to_all(chunks, ("zr", "y"), 0, 0, tiled=True)

    line = line_gather(block, 0)
    mine = line_gather(line, 1)
    other = swapped(mine, "c")

    tiles = S((4, 4, rows, cols), BF)
    keep, send, pieces = call(
        layer_body,
        (mine, other, chunks),
        [tiles, tiles, S(chunks.shape, BF)],
        [pltpu.VMEM((2 * NR, 3 * hid, NY * rows_d), BF)],
        28,
    )

    pieces = lax.all_to_all(pieces, ("zr", "y"), 0, 0, tiled=True)
    quads = call(quad_body, (pieces,), S((4, 2, 3 * hid, 2 * rows_d), BF))
    quads = lax.all_to_all(quads, QUADS, 0, 0, tiled=True)
    g_gate, g_up, g_down = call(
        last_body,
        (quads,),
        [S((rows_d, ff), F32), S((rows_d, ff), F32), S((rows_d, ff), F32)],
    )

    theirs = swapped(send, "c")
    chip = (keep.astype(F32) + theirs.astype(F32)).astype(BF)
    part = line_sum(chip, 0)
    done = line_sum(part, 1)
    return (done, g_gate, g_up, g_down.T)


def solution(mesh):
    fine = Mesh(mesh.devices.reshape(2, 2, NR, NY, NX, NC), ("zh", "zq", "zr", "y", "x", "c"))
    tok, fs, tp = ("zh", "zq", "zr", "y"), ("zq", "zr", "y"), ("x", "c")

    return jax.shard_map(
        per_device,
        mesh=fine,
        in_specs=(P(tok, tp), P(tok, tp), P(fs, tp), P(fs, tp), P(tp, fs)),
        out_specs=(P(tok, tp), P(fs, tp), P(fs, tp), P(tp, fs)),
        check_vma=False,
    )
```

profile of v0, /device:TPU:32, one launch (start us, length us, event | category | flops | bytes accessed | tf_op | source)
XLA Modules:
  0.0 167.3 jit_solution(678534822655488845)
XLA Ops:
  3.3 9.1 %collective-permute-start.8 = (bf16[2,264,128]{2,1,0:T(8,128)(2,1)S(1)}, bf16[2,264,128]{2,1,0:T(8,128)(2,1)S(1)}, u32[]{:S(2)}, u32[]{:S(2)}) collective-permute-start(bf16[2,264,128]{2,1,0:T(8,128)(2,1)S(1)} %shard_map.84.own), channel_id=1, source_target_pairs={{0,128},{128,0},{1,129},{129,1},{2,130},{130,2},{3,131},{131,3},{4... | collective-permute-start | bytes 405512 | tf_op jit(solution)/shard_map/ppermute | solution.py:20
  12.4 9.5 %collective-permute-done.8.far = bf16[2,264,128]{2,1,0:T(8,128)(2,1)S(1)} collective-permute-done((bf16[2,264,128]{2,1,0:T(8,128)(2,1)S(1)}, bf16[2,264,128]{2,1,0:T(8,128)(2,1)S(1)}, u32[]{:S(2)}, u32[]{:S(2)}) %collective-permute-start.8) | collective-permute-done | bytes 135200 | tf_op jit(solution)/shard_map/ppermute | solution.py:20
  23.0 9.3 %all-to-all-start = ((bf16[16,264,128]{2,1,0:T(8,128)(2,1)}), bf16[16,264,128]{2,1,0:T(8,128)(2,1)S(1)}, u32[]{:S(2)}, u32[]{:S(2)}) async-start(bf16[16,264,128]{2,1,0:T(8,128)(2,1)} %shard_map.85), calls=%async_computation | async-start | bytes 2162688 | tf_op jit(solution)/shard_map/all_to_all | solution.py:212
  35.5 4.9 %collective-permute-start.2 = (bf16[2,128,256]{2,1,0:T(8,128)(2,1)S(1)}, bf16[2,128,256]{2,1,0:T(8,128)(2,1)S(1)}, u32[]{:S(2)}, u32[]{:S(2)}) collective-permute-start(bf16[2,128,256]{2,1,0:T(8,128)(2,1)S(1)} %get-tuple-element.25), channel_id=1, source_target_pairs={{0,4},{1,17},{2,6},{3,19},{4,0},{5,21},{6,2},{7,23},{8,12},{9,25},... | collective-permute-start | bytes 393224 | tf_op jit(solution)/shard_map/ppermute | solution.py:30
  40.5 3.0 %collective-permute-start.1 = (bf16[2,128,256]{2,1,0:T(8,128)(2,1)S(1)}, bf16[2,128,256]{2,1,0:T(8,128)(2,1)S(1)}, u32[]{:S(2)}, u32[]{:S(2)}) collective-permute-start(bf16[2,128,256]{2,1,0:T(8,128)(2,1)S(1)} %get-tuple-element.25), channel_id=1, source_target_pairs={{0,6},{1,25},{2,0},{3,27},{4,2},{5,29},{6,4},{7,31},{8,14},{9,1},{... | collective-permute-start | bytes 393224 | tf_op jit(solution)/shard_map/ppermute | solution.py:30
  43.5 2.8 %collective-permute-start.3 = (bf16[2,128,256]{2,1,0:T(8,128)(2,1)S(1)}, bf16[2,128,256]{2,1,0:T(8,128)(2,1)S(1)}, u32[]{:S(2)}, u32[]{:S(2)}) collective-permute-start(bf16[2,128,256]{2,1,0:T(8,128)(2,1)S(1)} %get-tuple-element.25), channel_id=1, source_target_pairs={{0,2},{1,9},{2,4},{3,11},{4,6},{5,13},{6,0},{7,15},{8,10},{9,17},{... | collective-permute-start | bytes 393224 | tf_op jit(solution)/shard_map/ppermute | solution.py:30
  47.3 4.3 %collective-permute-done.3 = bf16[2,128,256]{2,1,0:T(8,128)(2,1)S(1)} collective-permute-done((bf16[2,128,256]{2,1,0:T(8,128)(2,1)S(1)}, bf16[2,128,256]{2,1,0:T(8,128)(2,1)S(1)}, u32[]{:S(2)}, u32[]{:S(2)}) %collective-permute-start.3) | collective-permute-done | bytes 131104 | tf_op jit(solution)/shard_map/ppermute | solution.py:30
  51.7 4.9 %collective-permute-start.5 = (bf16[4,2,128,256]{3,2,1,0:T(8,128)(2,1)S(1)}, bf16[4,2,128,256]{3,2,1,0:T(8,128)(2,1)S(1)}, u32[]{:S(2)}, u32[]{:S(2)}) collective-permute-start(bf16[4,2,128,256]{3,2,1,0:T(8,128)(2,1)S(1)} %get-tuple-element.20), channel_id=1, source_target_pairs={{0,16},{1,5},{2,18},{3,7},{4,20},{5,1},{6,22},{7,3},{8,24},{9,13},... | collective-permute-start | bytes 1572872 | tf_op jit(solution)/shard_map/ppermute | solution.py:30
  56.6 3.1 %collective-permute-start.4 = (bf16[4,2,128,256]{3,2,1,0:T(8,128)(2,1)S(1)}, bf16[4,2,128,256]{3,2,1,0:T(8,128)(2,1)S(1)}, u32[]{:S(2)}, u32[]{:S(2)}) collective-permute-start(bf16[4,2,128,256]{3,2,1,0:T(8,128)(2,1)S(1)} %get-tuple-element.20), channel_id=1, source_target_pairs={{0,24},{1,7},{2,26},{3,1},{4,28},{5,3},{6,30},{7,5},{8,0},{9,15},{... | collective-permute-start | bytes 1572872 | tf_op jit(solution)/shard_map/ppermute | solution.py:30
  59.7 2.8 %collective-permute-start.6 = (bf16[4,2,128,256]{3,2,1,0:T(8,128)(2,1)S(1)}, bf16[4,2,128,256]{3,2,1,0:T(8,128)(2,1)S(1)}, u32[]{:S(2)}, u32[]{:S(2)}) collective-permute-start(bf16[4,2,128,256]{3,2,1,0:T(8,128)(2,1)S(1)} %get-tuple-element.20), channel_id=1, source_target_pairs={{0,8},{1,3},{2,10},{3,5},{4,12},{5,7},{6,14},{7,1},{8,16},{9,11},{... | collective-permute-start | bytes 1572872 | tf_op jit(solution)/shard_map/ppermute | solution.py:30
  62.4 2.7 %collective-permute-done.5 = bf16[4,2,128,256]{3,2,1,0:T(8,128)(2,1)S(1)} collective-permute-done((bf16[4,2,128,256]{3,2,1,0:T(8,128)(2,1)S(1)}, bf16[4,2,128,256]{3,2,1,0:T(8,128)(2,1)S(1)}, u32[]{:S(2)}, u32[]{:S(2)}) %collective-permute-start.5) | collective-permute-done | bytes 524320 | tf_op jit(solution)/shard_map/ppermute | solution.py:30
  65.1 4.8 %collective-permute-done.4 = bf16[4,2,128,256]{3,2,1,0:T(8,128)(2,1)S(1)} collective-permute-done((bf16[4,2,128,256]{3,2,1,0:T(8,128)(2,1)S(1)}, bf16[4,2,128,256]{3,2,1,0:T(8,128)(2,1)S(1)}, u32[]{:S(2)}, u32[]{:S(2)}) %collective-permute-start.4) | collective-permute-done | bytes 524320 | tf_op jit(solution)/shard_map/ppermute | solution.py:30
  74.2 4.1 %collective-permute-done.7.other = bf16[4,4,2,128,256]{4,3,2,1,0:T(8,128)(2,1)S(1)} collective-permute-done((bf16[4,4,2,128,256]{4,3,2,1,0:T(8,128)(2,1)S(1)}, bf16[4,4,2,128,256]{4,3,2,1,0:T(8,128)(2,1)S(1)}, u32[]{:S(2)}, u32[]{:S(2)}) %collective-permute-start.7) | collective-permute-done | bytes 2097184 | tf_op jit(solution)/shard_map/ppermute | solution.py:20
  81.2 3.2 %shard_map.86 = (bf16[4,4,128,256]{3,2,1,0:T(8,128)(2,1)S(1)}, bf16[4,4,128,256]{3,2,1,0:T(8,128)(2,1)S(1)}, bf16[16,264,128]{2,1,0:T(8,128)(2,1)S(1)}) custom-call(bf16[4,4,2,128,256]{4,3,2,1,0:T(8,128)(2,1)S(1)} %pad_maximum_fusion.mine, bf16[4,4,2,128,256]{4,3,2,1,0:T(8,128)(2,1)S(1)} %copy-done.1, bf16[16,264,128]{2,1,0:T(8,128)(2,1)S(1)} %all-to-all-done.chunks), custom_call_target="tpu_custom_call" | custom-call | tf_op jit(solution)/shard_map/pallas_call | solution.py:54
  87.4 5.6 %all-to-all-start.1 = ((bf16[16,264,128]{2,1,0:T(8,128)(2,1)}), bf16[16,264,128]{2,1,0:T(8,128)(2,1)S(1)}, u32[]{:S(2)}, u32[]{:S(2)}) async-start(bf16[16,264,128]{2,1,0:T(8,128)(2,1)} %copy-done.2), calls=%async_computation.1 | async-start | bytes 2162688 | tf_op jit(solution)/shard_map/all_to_all | solution.py:227
  94.9 24.8 %all-to-all-done.1.pieces = bf16[16,264,128]{2,1,0:T(8,128)(2,1)S(1)} async-done(((bf16[16,264,128]{2,1,0:T(8,128)(2,1)}), bf16[16,264,128]{2,1,0:T(8,128)(2,1)S(1)}, u32[]{:S(2)}, u32[]{:S(2)}) %all-to-all-start.1) | async-done | bytes 1081376 | tf_op jit(solution)/shard_map/all_to_all | solution.py:227
  120.7 11.6 %all-to-all-start.2 = ((bf16[4,2,264,128]{3,2,1,0:T(8,128)(2,1)}), bf16[4,2,264,128]{3,2,1,0:T(8,128)(2,1)S(1)}, u32[]{:S(2)}, u32[]{:S(2)}) async-start(bf16[4,2,264,128]{3,2,1,0:T(8,128)(2,1)} %shard_map.87), calls=%async_computation.2 | async-start | bytes 1081344 | tf_op jit(solution)/shard_map/all_to_all | solution.py:229
  135.8 5.1 %collective-permute-start.12 = (bf16[4,128,256]{2,1,0:T(8,128)(2,1)S(1)}, bf16[4,128,256]{2,1,0:T(8,128)(2,1)S(1)}, u32[]{:S(2)}, u32[]{:S(2)}) collective-permute-start(bf16[4,128,256]{2,1,0:T(8,128)(2,1)S(1)} %get-tuple-element.17), channel_id=1, source_target_pairs={{0,6},{1,25},{2,0},{3,27},{4,2},{5,29},{6,4},{7,31},{8,14},{9,1},{... | collective-permute-start | bytes 786440 | tf_op jit(solution)/shard_map/ppermute | solution.py:30
  143.4 4.3 %collective-permute-done.12 = bf16[4,128,256]{2,1,0:T(8,128)(2,1)S(1)} collective-permute-done((bf16[4,128,256]{2,1,0:T(8,128)(2,1)S(1)}, bf16[4,128,256]{2,1,0:T(8,128)(2,1)S(1)}, u32[]{:S(2)}, u32[]{:S(2)}) %collective-permute-start.12) | collective-permute-done | bytes 262176 | tf_op jit(solution)/shard_map/ppermute | solution.py:30
  147.7 3.1 %collective-permute-done.11 = bf16[4,128,256]{2,1,0:T(8,128)(2,1)S(1)} collective-permute-done((bf16[4,128,256]{2,1,0:T(8,128)(2,1)S(1)}, bf16[4,128,256]{2,1,0:T(8,128)(2,1)S(1)}, u32[]{:S(2)}, u32[]{:S(2)}) %collective-permute-start.11) | collective-permute-done | bytes 262176 | tf_op jit(solution)/shard_map/ppermute | solution.py:30
  150.9 2.2 %collective-permute-start.13 = (bf16[128,256]{1,0:T(8,128)(2,1)S(1)}, bf16[128,256]{1,0:T(8,128)(2,1)S(1)}, u32[]{:S(2)}, u32[]{:S(2)}) collective-permute-start(bf16[128,256]{1,0:T(8,128)(2,1)S(1)} %get-tuple-element.21), channel_id=1, source_target_pairs={{0,8},{1,3},{2,10},{3,5},{4,12},{5,7},{6,14},{7,1},{8,16},{9,11},{... | collective-permute-start | bytes 196616 | tf_op jit(solution)/shard_map/ppermute | solution.py:30
  153.1 4.9 %collective-permute-start.15 = (bf16[128,256]{1,0:T(8,128)(2,1)S(1)}, bf16[128,256]{1,0:T(8,128)(2,1)S(1)}, u32[]{:S(2)}, u32[]{:S(2)}) collective-permute-start(bf16[128,256]{1,0:T(8,128)(2,1)S(1)} %get-tuple-element.22), channel_id=1, source_target_pairs={{0,24},{1,7},{2,26},{3,1},{4,28},{5,3},{6,30},{7,5},{8,0},{9,15},{... | collective-permute-start | bytes 196616 | tf_op jit(solution)/shard_map/ppermute | solution.py:30
  158.0 2.9 %collective-permute-start.14 = (bf16[128,256]{1,0:T(8,128)(2,1)S(1)}, bf16[128,256]{1,0:T(8,128)(2,1)S(1)}, u32[]{:S(2)}, u32[]{:S(2)}) collective-permute-start(bf16[128,256]{1,0:T(8,128)(2,1)S(1)} %get-tuple-element.23), channel_id=1, source_target_pairs={{0,16},{1,5},{2,18},{3,7},{4,20},{5,1},{6,22},{7,3},{8,24},{9,13},... | collective-permute-start | bytes 196616 | tf_op jit(solution)/shard_map/ppermute | solution.py:30
  160.9 4.8 %collective-permute-done.14 = bf16[128,256]{1,0:T(8,128)(2,1)S(1)} collective-permute-done((bf16[128,256]{1,0:T(8,128)(2,1)S(1)}, bf16[128,256]{1,0:T(8,128)(2,1)S(1)}, u32[]{:S(2)}, u32[]{:S(2)}) %collective-permute-start.14) | collective-permute-done | bytes 65568 | tf_op jit(solution)/shard_map/ppermute | solution.py:30
  (52 shorter events, 28.8 us)
Async XLA Ops:
  3.0 29.3 %copy-start.10 = (bf16[128,256]{1,0:T(8,128)(2,1)S(1)}, bf16[128,256]{1,0:T(8,128)(2,1)}, u32[]{:S(2)}) copy-start(bf16[128,256]{1,0:T(8,128)(2,1)} %param.5) | copy-start | bytes 196612
  3.0 29.3 %copy-start.11 = (bf16[128,256]{1,0:T(8,128)(2,1)S(1)}, bf16[128,256]{1,0:T(8,128)(2,1)}, u32[]{:S(2)}) copy-start(bf16[128,256]{1,0:T(8,128)(2,1)} %param.6) | copy-start | bytes 196612
  3.3 18.6 %collective-permute-start.8 = (bf16[2,264,128]{2,1,0:T(8,128)(2,1)S(1)}, bf16[2,264,128]{2,1,0:T(8,128)(2,1)S(1)}, u32[]{:S(2)}, u32[]{:S(2)}) collective-permute-start(bf16[2,264,128]{2,1,0:T(8,128)(2,1)S(1)} %shard_map.84.own), channel_id=1, source_target_pairs={{0,128},{128,0},{1,129},{129,1},{2,130},{130,2},{3,131},{131,3},{4... | collective-permute-start | bytes 405512 | tf_op jit(solution)/shard_map/ppermute | solution.py:20
  23.0 56.6 %all-to-all-start = ((bf16[16,264,128]{2,1,0:T(8,128)(2,1)}), bf16[16,264,128]{2,1,0:T(8,128)(2,1)S(1)}, u32[]{:S(2)}, u32[]{:S(2)}) async-start(bf16[16,264,128]{2,1,0:T(8,128)(2,1)} %shard_map.85), calls=%async_computation | async-start | bytes 2162688 | tf_op jit(solution)/shard_map/all_to_all | solution.py:212
  32.4 3.1 %collective-permute-start = (bf16[128,256]{1,0:T(8,128)(2,1)S(1)}, bf16[128,256]{1,0:T(8,128)(2,1)S(1)}, u32[]{:S(2)}, u32[]{:S(2)}) collective-permute-start(bf16[128,256]{1,0:T(8,128)(2,1)S(1)} %get-tuple-element.27), channel_id=1, source_target_pairs={{0,1},{1,0},{2,3},{3,2},{4,5},{5,4},{6,7},{7,6},{8,9},{9,8},{10,11... | collective-permute-start | bytes 196616 | tf_op jit(solution)/shard_map/ppermute | solution.py:20
  35.5 10.8 %collective-permute-start.2 = (bf16[2,128,256]{2,1,0:T(8,128)(2,1)S(1)}, bf16[2,128,256]{2,1,0:T(8,128)(2,1)S(1)}, u32[]{:S(2)}, u32[]{:S(2)}) collective-permute-start(bf16[2,128,256]{2,1,0:T(8,128)(2,1)S(1)} %get-tuple-element.25), channel_id=1, source_target_pairs={{0,4},{1,17},{2,6},{3,19},{4,0},{5,21},{6,2},{7,23},{8,12},{9,25},... | collective-permute-start | bytes 393224 | tf_op jit(solution)/shard_map/ppermute | solution.py:30
  40.5 6.9 %collective-permute-start.1 = (bf16[2,128,256]{2,1,0:T(8,128)(2,1)S(1)}, bf16[2,128,256]{2,1,0:T(8,128)(2,1)S(1)}, u32[]{:S(2)}, u32[]{:S(2)}) collective-permute-start(bf16[2,128,256]{2,1,0:T(8,128)(2,1)S(1)} %get-tuple-element.25), channel_id=1, source_target_pairs={{0,6},{1,25},{2,0},{3,27},{4,2},{5,29},{6,4},{7,31},{8,14},{9,1},{... | collective-permute-start | bytes 393224 | tf_op jit(solution)/shard_map/ppermute | solution.py:30
  43.5 8.1 %collective-permute-start.3 = (bf16[2,128,256]{2,1,0:T(8,128)(2,1)S(1)}, bf16[2,128,256]{2,1,0:T(8,128)(2,1)S(1)}, u32[]{:S(2)}, u32[]{:S(2)}) collective-permute-start(bf16[2,128,256]{2,1,0:T(8,128)(2,1)S(1)} %get-tuple-element.25), channel_id=1, source_target_pairs={{0,2},{1,9},{2,4},{3,11},{4,6},{5,13},{6,0},{7,15},{8,10},{9,17},{... | collective-permute-start | bytes 393224 | tf_op jit(solution)/shard_map/ppermute | solution.py:30
  51.7 13.4 %collective-permute-start.5 = (bf16[4,2,128,256]{3,2,1,0:T(8,128)(2,1)S(1)}, bf16[4,2,128,256]{3,2,1,0:T(8,128)(2,1)S(1)}, u32[]{:S(2)}, u32[]{:S(2)}) collective-permute-start(bf16[4,2,128,256]{3,2,1,0:T(8,128)(2,1)S(1)} %get-tuple-element.20), channel_id=1, source_target_pairs={{0,16},{1,5},{2,18},{3,7},{4,20},{5,1},{6,22},{7,3},{8,24},{9,13},... | collective-permute-start | bytes 1572872 | tf_op jit(solution)/shard_map/ppermute | solution.py:30
  56.6 13.4 %collective-permute-start.4 = (bf16[4,2,128,256]{3,2,1,0:T(8,128)(2,1)S(1)}, bf16[4,2,128,256]{3,2,1,0:T(8,128)(2,1)S(1)}, u32[]{:S(2)}, u32[]{:S(2)}) collective-permute-start(bf16[4,2,128,256]{3,2,1,0:T(8,128)(2,1)S(1)} %get-tuple-element.20), channel_id=1, source_target_pairs={{0,24},{1,7},{2,26},{3,1},{4,28},{5,3},{6,30},{7,5},{8,0},{9,15},{... | collective-permute-start | bytes 1572872 | tf_op jit(solution)/shard_map/ppermute | solution.py:30
  59.7 12.3 %collective-permute-start.6 = (bf16[4,2,128,256]{3,2,1,0:T(8,128)(2,1)S(1)}, bf16[4,2,128,256]{3,2,1,0:T(8,128)(2,1)S(1)}, u32[]{:S(2)}, u32[]{:S(2)}) collective-permute-start(bf16[4,2,128,256]{3,2,1,0:T(8,128)(2,1)S(1)} %get-tuple-element.20), channel_id=1, source_target_pairs={{0,8},{1,3},{2,10},{3,5},{4,12},{5,7},{6,14},{7,1},{8,16},{9,11},{... | collective-permute-start | bytes 1572872 | tf_op jit(solution)/shard_map/ppermute | solution.py:30
  72.2 6.1 %collective-permute-start.7 = (bf16[4,4,2,128,256]{4,3,2,1,0:T(8,128)(2,1)S(1)}, bf16[4,4,2,128,256]{4,3,2,1,0:T(8,128)(2,1)S(1)}, u32[]{:S(2)}, u32[]{:S(2)}) collective-permute-start(bf16[4,4,2,128,256]{4,3,2,1,0:T(8,128)(2,1)S(1)} %pad_maximum_fusion.mine), channel_id=1, source_target_pairs={{0,1},{1,0},{2,3},{3,2},{4,5},{5,4},{6,7},{7,6},{8,9},{9,8},{10,11... | collective-permute-start | bytes 6291464 | tf_op jit(solution)/shard_map/ppermute | solution.py:20
  79.6 1.6 copy-start.1
  87.4 5.6 %copy-start.9 = (bf16[4,4,128,256]{3,2,1,0:T(8,128)(2,1)S(1)}, bf16[4,4,128,256]{3,2,1,0:T(8,128)(2,1)}, u32[]{:S(2)}) copy-start(bf16[4,4,128,256]{3,2,1,0:T(8,128)(2,1)} %copy-done.8) | copy-start | bytes 3145732
  87.4 44.9 %copy-start.4 = (bf16[4,4,128,256]{3,2,1,0:T(8,128)(2,1)S(1)}, bf16[4,4,128,256]{3,2,1,0:T(8,128)(2,1)}, u32[]{:S(2)}) copy-start(bf16[4,4,128,256]{3,2,1,0:T(8,128)(2,1)} %copy-done.3) | copy-start | bytes 3145732
  87.4 32.3 %all-to-all-start.1 = ((bf16[16,264,128]{2,1,0:T(8,128)(2,1)}), bf16[16,264,128]{2,1,0:T(8,128)(2,1)S(1)}, u32[]{:S(2)}, u32[]{:S(2)}) async-start(bf16[16,264,128]{2,1,0:T(8,128)(2,1)} %copy-done.2), calls=%async_computation.1 | async-start | bytes 2162688 | tf_op jit(solution)/shard_map/all_to_all | solution.py:227
  93.0 39.3 %collective-permute-start.9 = (bf16[4,4,128,256]{3,2,1,0:T(8,128)(2,1)S(1)}, bf16[4,4,128,256]{3,2,1,0:T(8,128)(2,1)}, u32[]{:S(2)}, u32[]{:S(2)}) collective-permute-start(bf16[4,4,128,256]{3,2,1,0:T(8,128)(2,1)S(1)} %copy-done.9), channel_id=1, source_target_pairs={{0,1},{1,0},{2,3},{3,2},{4,5},{5,4},{6,7},{7,6},{8,9},{9,8},{10,11... | collective-permute-start | bytes 3145736 | tf_op jit(solution)/shard_map/ppermute | solution.py:20
  120.7 45.6 %all-to-all-start.2 = ((bf16[4,2,264,128]{3,2,1,0:T(8,128)(2,1)}), bf16[4,2,264,128]{3,2,1,0:T(8,128)(2,1)S(1)}, u32[]{:S(2)}, u32[]{:S(2)}) async-start(bf16[4,2,264,128]{3,2,1,0:T(8,128)(2,1)} %shard_map.87), calls=%async_computation.2 | async-start | bytes 1081344 | tf_op jit(solution)/shard_map/all_to_all | solution.py:229
  133.9 9.5 %collective-permute-start.10 = (bf16[4,128,256]{2,1,0:T(8,128)(2,1)S(1)}, bf16[4,128,256]{2,1,0:T(8,128)(2,1)S(1)}, u32[]{:S(2)}, u32[]{:S(2)}) collective-permute-start(bf16[4,128,256]{2,1,0:T(8,128)(2,1)S(1)} %get-tuple-element.16), channel_id=1, source_target_pairs={{0,2},{1,9},{2,4},{3,11},{4,6},{5,13},{6,0},{7,15},{8,10},{9,17},{... | collective-permute-start | bytes 786440 | tf_op jit(solution)/shard_map/ppermute | solution.py:30
  135.8 11.9 %collective-permute-start.12 = (bf16[4,128,256]{2,1,0:T(8,128)(2,1)S(1)}, bf16[4,128,256]{2,1,0:T(8,128)(2,1)S(1)}, u32[]{:S(2)}, u32[]{:S(2)}) collective-permute-start(bf16[4,128,256]{2,1,0:T(8,128)(2,1)S(1)} %get-tuple-element.17), channel_id=1, source_target_pairs={{0,6},{1,25},{2,0},{3,27},{4,2},{5,29},{6,4},{7,31},{8,14},{9,1},{... | collective-permute-start | bytes 786440 | tf_op jit(solution)/shard_map/ppermute | solution.py:30
  141.0 9.8 %collective-permute-start.11 = (bf16[4,128,256]{2,1,0:T(8,128)(2,1)S(1)}, bf16[4,128,256]{2,1,0:T(8,128)(2,1)S(1)}, u32[]{:S(2)}, u32[]{:S(2)}) collective-permute-start(bf16[4,128,256]{2,1,0:T(8,128)(2,1)S(1)} %get-tuple-element.18), channel_id=1, source_target_pairs={{0,4},{1,17},{2,6},{3,19},{4,0},{5,21},{6,2},{7,23},{8,12},{9,25},... | collective-permute-start | bytes 786440 | tf_op jit(solution)/shard_map/ppermute | solution.py:30
  150.9 10.0 %collective-permute-start.13 = (bf16[128,256]{1,0:T(8,128)(2,1)S(1)}, bf16[128,256]{1,0:T(8,128)(2,1)S(1)}, u32[]{:S(2)}, u32[]{:S(2)}) collective-permute-start(bf16[128,256]{1,0:T(8,128)(2,1)S(1)} %get-tuple-element.21), channel_id=1, source_target_pairs={{0,8},{1,3},{2,10},{3,5},{4,12},{5,7},{6,14},{7,1},{8,16},{9,11},{... | collective-permute-start | bytes 196616 | tf_op jit(solution)/shard_map/ppermute | solution.py:30
  153.1 7.8 %collective-permute-start.15 = (bf16[128,256]{1,0:T(8,128)(2,1)S(1)}, bf16[128,256]{1,0:T(8,128)(2,1)S(1)}, u32[]{:S(2)}, u32[]{:S(2)}) collective-permute-start(bf16[128,256]{1,0:T(8,128)(2,1)S(1)} %get-tuple-element.22), channel_id=1, source_target_pairs={{0,24},{1,7},{2,26},{3,1},{4,28},{5,3},{6,30},{7,5},{8,0},{9,15},{... | collective-permute-start | bytes 196616 | tf_op jit(solution)/shard_map/ppermute | solution.py:30
  158.0 7.7 %collective-permute-start.14 = (bf16[128,256]{1,0:T(8,128)(2,1)S(1)}, bf16[128,256]{1,0:T(8,128)(2,1)S(1)}, u32[]{:S(2)}, u32[]{:S(2)}) collective-permute-start(bf16[128,256]{1,0:T(8,128)(2,1)S(1)} %get-tuple-element.23), channel_id=1, source_target_pairs={{0,16},{1,5},{2,18},{3,7},{4,20},{5,1},{6,22},{7,3},{8,24},{9,13},... | collective-permute-start | bytes 196616 | tf_op jit(solution)/shard_map/ppermute | solution.py:30
  (7 other events, 6.7 us)
where the time goes:
time: 168 us; the launch traced here: 167 us
  starting transfers between devices  81.8 us (49%)
  waiting for transfers between devices  67 us (40%)
  local copies, waits for them, and re-layouts  8.4 us (5%)
  Pallas kernels  6.51 us (4%)
  other arithmetic  2.72 us (2%)
    ppermute x12, starting transfers between devices, moved(): return lax.ppermute(value, PLANE, pairs)  40.4 us
    ppermute x12, waiting for transfers between devices, moved(): return lax.ppermute(value, PLANE, pairs)  27.4 us
    all_to_all x1, waiting for transfers between devices, per_device(): pieces = lax.all_to_all(pieces, ('zr', 'y'), 0, 0, tiled=True)  24.8 us
    ppermute x4, starting transfers between devices, swapped(): return lax.ppermute(value, axis, [(0, 1), (1, 0)])  14.9 us
    ppermute x4, waiting for transfers between devices, swapped(): return lax.ppermute(value, axis, [(0, 1), (1, 0)])  14.8 us
    all_to_all x1, starting transfers between devices, per_device(): quads = lax.all_to_all(quads, QUADS, 0, 0, tiled=True)  11.6 us
    all_to_all x1, starting transfers between devices, per_device(): chunks = lax.all_to_all(chunks, ('zr', 'y'), 0, 0, tiled=True)  9.34 us
    unnamed x24, local copies, waits for them, and re-layouts  8.33 us
  transfers between devices with their start and end apart: 19, of which 13 were waited for; matrix products, arithmetic and copies ran while one was open for 2% of the time, Pallas kernels for 1%

commit v1 on v0

v1 whole, which is shorter than its diff:
```python
import jax
import jax.numpy as jnp
from jax import lax
from jax.experimental import pallas as pl
from jax.experimental.pallas import tpu as pltpu
from jax.sharding import Mesh, PartitionSpec as P


BF = jnp.bfloat16
F32 = jnp.float32
NQ, NR, NY, NX, NC = 2, 4, 4, 4, 2
PLANE = ("y", "x", "c")
VM = pl.BlockSpec(memory_space=pltpu.VMEM)
NN = ((1,), (0,))
NT = ((1,), (1,))


def swapped(value):
    return lax.ppermute(value, "c", [(0, 1), (1, 0)])


def moved(value, k, x_core):
    pairs = []
    for y in range(NY):
        for x in range(NX):
            for c in range(NC):
                ty, tx = (y, (x + k) % NX) if c == x_core else ((y + k) % NY, x)
                pairs.append(((y * NX + x) * NC + c, (ty * NX + tx) * NC + c))
    return lax.ppermute(value, PLANE, pairs)


def line_gather(value, x_core):
    return [value] + [moved(value, -k, x_core) for k in (1, 2, 3)]


def line_sum(value, x_core):
    total = value[0].astype(F32)
    for k in (1, 2, 3):
        total = total + moved(value[k], k, x_core).astype(F32)
    return total.astype(BF)


def dot(a, b, dims):
    return lax.dot_general(a, b, (dims, ((), ())), preferred_element_type=F32)


def call(body, args, shapes, mib=8, far_in=0, far_out=False):
    single = not isinstance(shapes, (list, tuple))
    shapes = [shapes] if single else list(shapes)
    n, m = len(args), len(shapes)
    loads, stores = far_in, m if far_out else 0

    def whole(*refs):
        ins, outs, rest = list(refs[:n]), list(refs[n : n + m]), refs[n + m :]
        near_in, near_out = rest[:loads], rest[loads : loads + stores]
        if loads:
            sems = rest[loads + stores]
            copies = [pltpu.make_async_copy(ins[i], near_in[i], sems.at[i]) for i in range(loads)]
            for c in copies:
                c.start()
            for c in copies:
                c.wait()
        body(*near_in, *ins[loads:], *(near_out if stores else outs))
        if stores:
            sems = rest[-1]
            copies = [pltpu.make_async_copy(near_out[i], outs[i], sems.at[i]) for i in range(m)]
            for c in copies:
                c.start()
            for c in copies:
                c.wait()

    far = pl.BlockSpec(memory_space=pltpu.HBM)
    scratch = [pltpu.VMEM(a.shape, a.dtype) for a in args[:loads]]
    scratch += [pltpu.VMEM(a.shape, a.dtype) for a in shapes[:stores]]
    scratch += [pltpu.SemaphoreType.DMA((k,)) for k in (loads, stores) if k]
    out = pl.pallas_call(
        whole,
        in_specs=[far] * loads + [VM] * (n - loads),
        out_specs=[far if far_out else VM] * m,
        out_shape=shapes,
        scratch_shapes=scratch,
        compiler_params=pltpu.CompilerParams(vmem_limit_bytes=mib * 2**20),
    )(*args)
    return out[0] if single else out


def folded(value, cut):
    low = value[cut:]
    gap = jnp.zeros((2 * cut - value.shape[0], value.shape[1]), value.dtype)
    return jnp.concatenate([value[:cut], jnp.concatenate([low, gap], axis=0)], axis=1)


def unfolded(value, n):
    cut, width = value.shape
    return jnp.concatenate([value[:, : width // 2], value[: n - cut, width // 2 :]], axis=0)


def cut_of(n):
    return -(-n // 16) * 8


def pack_body(wg, wu, wd, out):
    hid = wd.shape[1] // NY
    tg = wg[...].astype(F32).T
    tu = wu[...].astype(F32).T
    td = wd[...].astype(F32).T
    for y in range(NY):
        s = slice(y * hid, (y + 1) * hid)
        part = jnp.concatenate([tg[s], tu[s], td[s]], axis=0)
        part = folded(part, out.shape[1]).astype(BF)
        for q in range(NQ):
            out[q * NY + y] = part


def spread_body(parts, out):
    n = out.shape[1]
    whole = jnp.concatenate(
        [unfolded(parts[i].astype(F32), n).astype(BF) for i in range(NQ * NY)], axis=1
    )
    for r in range(NR):
        out[r] = whole


def layer_body(mine, other, chunks, keep, send, pieces):
    core = lax.axis_index("c")
    x_here = lax.axis_index("x")
    hid = chunks.shape[1] // 3
    width = chunks.shape[2] // NQ

    def run(inputs, cotan, me):
        def in_block(k, c):
            return jnp.concatenate([inputs[j][k, c] for j in range(NY)], axis=0)

        def co_block(k, c):
            part = cotan[k][:, 1 - c]
            return part.reshape(NY * part.shape[1], part.shape[2])

        def place(k, c):
            x = (x_here + k) % NX
            return (x % 2) * NC + c, pl.ds(pl.multiple_of((x // 2) * width, width), width)

        blocks = [(k, c) for k in range(NX) for c in range(NC)]
        pre = None
        hid_grad = None
        for k, c in blocks:
            r, s = place(k, c)
            p = dot(chunks[r, : 2 * hid, s], in_block(k, c), NT)
            q = dot(chunks[r, 2 * hid :, s], co_block(k, c), NT)
            pre = p if pre is None else pre + p
            hid_grad = q if hid_grad is None else hid_grad + q
        gate = pre[:hid]
        up = pre[hid:]
        sig = jax.nn.sigmoid(gate)
        act = gate * sig
        hidden = (act * up).astype(BF)
        g_gate = hid_grad * up * sig * (1.0 + gate * (1.0 - sig))
        g_up = hid_grad * act
        g_both = jnp.concatenate([g_gate, g_up], axis=0)
        g_turned = g_both.T.astype(BF)
        g_both = g_both.astype(BF)
        for k, c in blocks:
            r, s = place(k, c)
            pieces[r, : 2 * hid, s] = dot(g_both, in_block(k, c), NN).astype(BF)
            pieces[r, 2 * hid :, s] = dot(hidden, co_block(k, c), NN).astype(BF)
            gi = dot(g_turned, chunks[r, : 2 * hid, s], NN).astype(BF)
            rows = gi.shape[0] // NY
            ref = keep if c == me else send
            for j in range(NY):
                piece = gi[j * rows : (j + 1) * rows]
                if c == 0:
                    ref[k, j] = piece
                else:
                    ref[j, k] = piece

    @pl.when(core == 0)
    def _():
        run(mine, other, 0)

    @pl.when(core == 1)
    def _():
        run(other, mine, 1)


def sum_body(pieces, out):
    total = pieces[0].astype(F32)
    for r in range(1, NR):
        total = total + pieces[r].astype(F32)
    width = total.shape[1] // (NQ * NY)
    for i in range(NQ * NY):
        part = folded(total[:, i * width : (i + 1) * width], out.shape[1]).astype(BF)
        for h in range(2):
            out[h * NQ * NY + i] = part


def last_body(parts, gg, gu, gd):
    hid = gg.shape[1] // NY
    by_y = []
    for y in range(NY):
        v = parts[y].astype(F32)
        for q in range(1, 4):
            v = v + parts[q * NY + y].astype(F32)
        by_y.append(unfolded(v, 3 * hid))
    gg[...] = jnp.concatenate([b[:hid] for b in by_y], axis=0).T
    gu[...] = jnp.concatenate([b[hid : 2 * hid] for b in by_y], axis=0).T
    gd[...] = jnp.concatenate([b[2 * hid :] for b in by_y], axis=0).T


def per_device(inputs, cotangent, gate_weight, up_weight, down_weight):
    S = jax.ShapeDtypeStruct
    rows_d, ff = gate_weight.shape
    hid = ff // NY
    cut = cut_of(3 * hid)
    rows, cols = inputs.shape

    first = lax.axis_index("c") == 0
    kept = jnp.where(first, inputs, cotangent)
    given = jnp.where(first, cotangent, inputs)
    got = swapped(given)
    block = jnp.stack([kept, got])

    packed = call(
        pack_body,
        (gate_weight, up_weight, down_weight.T),
        S((NQ * NY, cut, 2 * rows_d), BF),
        far_in=3,
    )
    packed = lax.all_to_all(packed, ("zq", "y"), 0, 0, tiled=True)
    chunks = call(spread_body, (packed,), S((NR, 3 * hid, NQ * NY * rows_d), BF))
    chunks = lax.all_to_all(chunks, "zr", 0, 0, tiled=True)

    line = jnp.stack(line_gather(block, 0))
    mine = line_gather(line, 1)
    other = [swapped(m) for m in mine]

    tiles = S((4, 4, rows, cols), BF)

    def body(*refs):
        layer_body(refs[:4], refs[4:8], *refs[8:])

    keep, send, pieces = call(
        body,
        (*mine, *other, chunks),
        [tiles, tiles, S(chunks.shape, BF)],
        28,
        far_in=8,
        far_out=True,
    )

    pieces = lax.all_to_all(pieces, "zr", 0, 0, tiled=True)
    ring = call(sum_body, (pieces,), S((2 * NQ * NY, cut, 2 * rows_d), BF))
    ring = lax.all_to_all(ring, ("zh", "zq", "y"), 0, 0, tiled=True)
    g_gate, g_up, g_down = call(last_body, (ring,), [S((rows_d, ff), F32)] * 3)

    theirs = swapped(send)
    chip = (keep.astype(F32) + theirs.astype(F32)).astype(BF)
    part = line_sum(chip, 0)
    done = line_sum(part, 1)
    return (done, g_gate, g_up, g_down.T)


def solution(mesh):
    fine = Mesh(mesh.devices.reshape(2, NQ, NR, NY, NX, NC), ("zh", "zq", "zr", "y", "x", "c"))
    tok, fs, tp = ("zh", "zq", "zr", "y"), ("zq", "zr", "y"), ("x", "c")

    return jax.shard_map(
        per_device,
        mesh=fine,
        in_specs=(P(tok, tp), P(tok, tp), P(fs, tp), P(fs, tp), P(tp, fs)),
        out_specs=(P(tok, tp), P(fs, tp), P(fs, tp), P(tp, fs)),
        check_vma=False,
    )
```

time: 168 us -> 178 us (1.060)
  the two profiles are of different devices: /device:TPU:32 before, /device:TPU:8 now
where the time goes in v1:
time: 178 us; the launch traced here: 177 us
  starting transfers between devices  74.4 us (42%)
  waiting for transfers between devices  46.7 us (26%)
  blocking collectives  30.4 us (17%)
  local copies, waits for them, and re-layouts  13.6 us (8%)
  Pallas kernels  8.2 us (5%)
  other arithmetic  2.44 us (1%)
    ppermute x12, starting transfers between devices, moved(): return lax.ppermute(value, PLANE, pairs)  39.4 us
    all_to_all x1, blocking collectives, per_device(): packed = lax.all_to_all(packed, ('zq', 'y'), 0, 0, tiled=True)  30.4 us
    all_to_all x1, waiting for transfers between devices, per_device(): pieces = lax.all_to_all(pieces, 'zr', 0, 0, tiled=True)  25 us
    ppermute x12, waiting for transfers between devices, moved(): return lax.ppermute(value, PLANE, pairs)  20.5 us
    all_to_all x1, starting transfers between devices, per_device(): ring = lax.all_to_all(ring, ('zh', 'zq', 'y'), 0, 0, tiled=True)  14.2 us
    unnamed x34, local copies, waits for them, and re-layouts  13.5 us
    ppermute x6, starting transfers between devices, swapped(): return lax.ppermute(value, 'c', [(0, 1), (1, 0)])  12.2 us
    pallas_call x5, Pallas kernels, call(): pl.pallas_call(whole, in_specs=[far] * loads + [VM] * (n - loads), out_sp...  8.2 us
  transfers between devices with their start and end apart: 21, of which 10 were waited for; matrix products, arithmetic and copies ran while one was open for 1% of the time, Pallas kernels for 1%

profile of v1, /device:TPU:8, one launch (start us, length us, event | category | flops | bytes accessed | tf_op | source)
XLA Modules:
  0.0 176.7 jit_solution(1095421444151198638)
XLA Ops:
  3.5 30.4 %all_to_all.20.refs_0_ = bf16[8,136,128]{2,1,0:T(8,128)(2,1)S(1)} all-to-all(bf16[8,136,128]{2,1,0:T(8,128)(2,1)S(1)} %shard_map.84), channel_id=1, replica_groups=mesh['zh'=2,'zq'=2,'zr'=4,'y'=4,'x'=4,'c'=2] {'zq','y'}, dimensions={0} | all-to-all | bytes 557056 | tf_op jit(solution)/shard_map/all_to_all | solution.py:227
  35.1 3.6 %all-to-all-start.1 = ((bf16[4,264,512]{2,1,0:T(8,128)(2,1)}), bf16[4,264,512]{2,1,0:T(8,128)(2,1)S(1)}, u32[]{:S(2)}, u32[]{:S(2)}) async-start(bf16[4,264,512]{2,1,0:T(8,128)(2,1)} %shard_map.85), calls=%async_computation.1 | async-start | bytes 2162688 | tf_op jit(solution)/shard_map/all_to_all | solution.py:229
  42.0 4.9 %collective-permute-start.2 = (bf16[2,128,256]{2,1,0:T(8,128)(2,1)S(1)}, bf16[2,128,256]{2,1,0:T(8,128)(2,1)S(1)}, u32[]{:S(2)}, u32[]{:S(2)}) collective-permute-start(bf16[2,128,256]{2,1,0:T(8,128)(2,1)S(1)} %get-tuple-element.23), channel_id=1, source_target_pairs={{0,4},{1,17},{2,6},{3,19},{4,0},{5,21},{6,2},{7,23},{8,12},{9,25},... | collective-permute-start | bytes 393224 | tf_op jit(solution)/shard_map/ppermute | solution.py:29
  47.0 3.0 %collective-permute-start.1 = (bf16[2,128,256]{2,1,0:T(8,128)(2,1)S(1)}, bf16[2,128,256]{2,1,0:T(8,128)(2,1)S(1)}, u32[]{:S(2)}, u32[]{:S(2)}) collective-permute-start(bf16[2,128,256]{2,1,0:T(8,128)(2,1)S(1)} %get-tuple-element.23), channel_id=1, source_target_pairs={{0,6},{1,25},{2,0},{3,27},{4,2},{5,29},{6,4},{7,31},{8,14},{9,1},{... | collective-permute-start | bytes 393224 | tf_op jit(solution)/shard_map/ppermute | solution.py:29
  50.0 2.8 %collective-permute-start.3 = (bf16[2,128,256]{2,1,0:T(8,128)(2,1)S(1)}, bf16[2,128,256]{2,1,0:T(8,128)(2,1)S(1)}, u32[]{:S(2)}, u32[]{:S(2)}) collective-permute-start(bf16[2,128,256]{2,1,0:T(8,128)(2,1)S(1)} %get-tuple-element.23), channel_id=1, source_target_pairs={{0,2},{1,9},{2,4},{3,11},{4,6},{5,13},{6,0},{7,15},{8,10},{9,17},{... | collective-permute-start | bytes 393224 | tf_op jit(solution)/shard_map/ppermute | solution.py:29
  53.8 4.3 %collective-permute-done.3 = bf16[2,128,256]{2,1,0:T(8,128)(2,1)S(1)} collective-permute-done((bf16[2,128,256]{2,1,0:T(8,128)(2,1)S(1)}, bf16[2,128,256]{2,1,0:T(8,128)(2,1)S(1)}, u32[]{:S(2)}, u32[]{:S(2)}) %collective-permute-start.3) | collective-permute-done | bytes 131104 | tf_op jit(solution)/shard_map/ppermute | solution.py:29
  58.2 2.5 %collective-permute-start.6 = (bf16[4,2,128,256]{3,2,1,0:T(8,128)(2,1)S(1)}, bf16[4,2,128,256]{3,2,1,0:T(8,128)(2,1)S(1)}, u32[]{:S(2)}, u32[]{:S(2)}) collective-permute-start(bf16[4,2,128,256]{3,2,1,0:T(8,128)(2,1)S(1)} %pad_maximum_fusion.refs_0_), channel_id=1, source_target_pairs={{0,8},{1,3},{2,10},{3,5},{4,12},{5,7},{6,14},{7,1},{8,16},{9,11},{... | collective-permute-start | bytes 1572872 | tf_op jit(solution)/shard_map/ppermute | solution.py:29
  60.6 4.9 %collective-permute-start.5 = (bf16[4,2,128,256]{3,2,1,0:T(8,128)(2,1)S(1)}, bf16[4,2,128,256]{3,2,1,0:T(8,128)(2,1)S(1)}, u32[]{:S(2)}, u32[]{:S(2)}) collective-permute-start(bf16[4,2,128,256]{3,2,1,0:T(8,128)(2,1)S(1)} %pad_maximum_fusion.refs_0_), channel_id=1, source_target_pairs={{0,16},{1,5},{2,18},{3,7},{4,20},{5,1},{6,22},{7,3},{8,24},{9,13},... | collective-permute-start | bytes 1572872 | tf_op jit(solution)/shard_map/ppermute | solution.py:29
  65.5 2.5 %collective-permute-start.4 = (bf16[4,2,128,256]{3,2,1,0:T(8,128)(2,1)S(1)}, bf16[4,2,128,256]{3,2,1,0:T(8,128)(2,1)S(1)}, u32[]{:S(2)}, u32[]{:S(2)}) collective-permute-start(bf16[4,2,128,256]{3,2,1,0:T(8,128)(2,1)S(1)} %pad_maximum_fusion.refs_0_), channel_id=1, source_target_pairs={{0,24},{1,7},{2,26},{3,1},{4,28},{5,3},{6,30},{7,5},{8,0},{9,15},{... | collective-permute-start | bytes 1572872 | tf_op jit(solution)/shard_map/ppermute | solution.py:29
  69.9 2.4 %collective-permute-start.10 = (bf16[4,2,128,256]{3,2,1,0:T(8,128)(2,1)S(1)}, bf16[4,2,128,256]{3,2,1,0:T(8,128)(2,1)S(1)}, u32[]{:S(2)}, u32[]{:S(2)}) collective-permute-start(bf16[4,2,128,256]{3,2,1,0:T(8,128)(2,1)S(1)} %collective-permute-done.6.refs_3_), channel_id=1, source_target_pairs={{0,1},{1,0},{2,3},{3,2},{4,5},{5,4},{6,7},{7,6},{8,9},{9,8},{10,11... | collective-permute-start | bytes 1572872 | tf_op jit(solution)/shard_map/ppermute | solution.py:19
  76.0 2.8 %collective-permute-done.4.refs_1_ = bf16[4,2,128,256]{3,2,1,0:T(8,128)(2,1)S(1)} collective-permute-done((bf16[4,2,128,256]{3,2,1,0:T(8,128)(2,1)S(1)}, bf16[4,2,128,256]{3,2,1,0:T(8,128)(2,1)S(1)}, u32[]{:S(2)}, u32[]{:S(2)}) %collective-permute-start.4) | collective-permute-done | bytes 524320 | tf_op jit(solution)/shard_map/ppermute | solution.py:29
  91.1 4.6 %shard_map.86 = (bf16[4,4,128,256]{3,2,1,0:T(8,128)(2,1)S(1)}, bf16[4,4,128,256]{3,2,1,0:T(8,128)(2,1)}, bf16[4,264,512]{2,1,0:T(8,128)(2,1)}) custom-call(bf16[4,2,128,256]{3,2,1,0:T(8,128)(2,1)S(1)} %pad_maximum_fusion.refs_0_, bf16[4,2,128,256]{3,2,1,0:T(8,128)(2,1)S(1)} %copy-done.3, bf16[4,2,128,256]{3,2,1,0:T(8,128)(2,1)S(1)} %copy-done.1, ...), custom_call_target="tpu_custom_call" | custom-call | tf_op jit(solution)/shard_map/pallas_call | solution.py:76
  95.6 5.0 %all-to-all-start.2 = ((bf16[4,264,512]{2,1,0:T(8,128)(2,1)}), bf16[4,264,512]{2,1,0:T(8,128)(2,1)S(1)}, u32[]{:S(2)}, u32[]{:S(2)}) async-start(bf16[4,264,512]{2,1,0:T(8,128)(2,1)} %get-tuple-element.12), calls=%async_computation.2 | async-start | bytes 2162688 | tf_op jit(solution)/shard_map/all_to_all | solution.py:249
  100.7 2.1 %collective-permute-start.11 = (bf16[4,4,128,256]{3,2,1,0:T(8,128)(2,1)}, bf16[4,4,128,256]{3,2,1,0:T(8,128)(2,1)}, u32[]{:S(2)}, u32[]{:S(2)}) collective-permute-start(bf16[4,4,128,256]{3,2,1,0:T(8,128)(2,1)} %get-tuple-element.11), channel_id=1, source_target_pairs={{0,1},{1,0},{2,3},{3,2},{4,5},{5,4},{6,7},{7,6},{8,9},{9,8},{10,11... | collective-permute-start | bytes 3145736 | tf_op jit(solution)/shard_map/ppermute | solution.py:19
  102.8 25.0 %all-to-all-done.2.refs_0_ = bf16[4,264,512]{2,1,0:T(8,128)(2,1)S(1)} async-done(((bf16[4,264,512]{2,1,0:T(8,128)(2,1)}), bf16[4,264,512]{2,1,0:T(8,128)(2,1)S(1)}, u32[]{:S(2)}, u32[]{:S(2)}) %all-to-all-start.2) | async-done | bytes 1081376 | tf_op jit(solution)/shard_map/all_to_all | solution.py:249
  128.8 14.2 %all-to-all-start.3 = ((bf16[16,136,128]{2,1,0:T(8,128)(2,1)}), bf16[16,136,128]{2,1,0:T(8,128)(2,1)S(1)}, u32[]{:S(2)}, u32[]{:S(2)}) async-start(bf16[16,136,128]{2,1,0:T(8,128)(2,1)} %shard_map.87), calls=%async_computation.3 | async-start | bytes 1114112 | tf_op jit(solution)/shard_map/all_to_all | solution.py:251
  146.5 5.1 %collective-permute-start.14 = (bf16[4,128,256]{2,1,0:T(8,128)(2,1)S(1)}, bf16[4,128,256]{2,1,0:T(8,128)(2,1)S(1)}, u32[]{:S(2)}, u32[]{:S(2)}) collective-permute-start(bf16[4,128,256]{2,1,0:T(8,128)(2,1)S(1)} %get-tuple-element.17), channel_id=1, source_target_pairs={{0,6},{1,25},{2,0},{3,27},{4,2},{5,29},{6,4},{7,31},{8,14},{9,1},{... | collective-permute-start | bytes 786440 | tf_op jit(solution)/shard_map/ppermute | solution.py:29
  151.6 1.9 %collective-permute-start.13 = (bf16[4,128,256]{2,1,0:T(8,128)(2,1)S(1)}, bf16[4,128,256]{2,1,0:T(8,128)(2,1)S(1)}, u32[]{:S(2)}, u32[]{:S(2)}) collective-permute-start(bf16[4,128,256]{2,1,0:T(8,128)(2,1)S(1)} %get-tuple-element.18), channel_id=1, source_target_pairs={{0,4},{1,17},{2,6},{3,19},{4,0},{5,21},{6,2},{7,23},{8,12},{9,25},... | collective-permute-start | bytes 786440 | tf_op jit(solution)/shard_map/ppermute | solution.py:29
  154.1 4.3 %collective-permute-done.14 = bf16[4,128,256]{2,1,0:T(8,128)(2,1)S(1)} collective-permute-done((bf16[4,128,256]{2,1,0:T(8,128)(2,1)S(1)}, bf16[4,128,256]{2,1,0:T(8,128)(2,1)S(1)}, u32[]{:S(2)}, u32[]{:S(2)}) %collective-permute-start.14) | collective-permute-done | bytes 262176 | tf_op jit(solution)/shard_map/ppermute | solution.py:29
  158.4 3.1 %collective-permute-done.13 = bf16[4,128,256]{2,1,0:T(8,128)(2,1)S(1)} collective-permute-done((bf16[4,128,256]{2,1,0:T(8,128)(2,1)S(1)}, bf16[4,128,256]{2,1,0:T(8,128)(2,1)S(1)}, u32[]{:S(2)}, u32[]{:S(2)}) %collective-permute-start.13) | collective-permute-done | bytes 262176 | tf_op jit(solution)/shard_map/ppermute | solution.py:29
  161.6 3.4 %collective-permute-start.15 = (bf16[128,256]{1,0:T(8,128)(2,1)S(1)}, bf16[128,256]{1,0:T(8,128)(2,1)S(1)}, u32[]{:S(2)}, u32[]{:S(2)}) collective-permute-start(bf16[128,256]{1,0:T(8,128)(2,1)S(1)} %get-tuple-element.19), channel_id=1, source_target_pairs={{0,8},{1,3},{2,10},{3,5},{4,12},{5,7},{6,14},{7,1},{8,16},{9,11},{... | collective-permute-start | bytes 196616 | tf_op jit(solution)/shard_map/ppermute | solution.py:29
  165.0 2.5 %collective-permute-start.17 = (bf16[128,256]{1,0:T(8,128)(2,1)S(1)}, bf16[128,256]{1,0:T(8,128)(2,1)S(1)}, u32[]{:S(2)}, u32[]{:S(2)}) collective-permute-start(bf16[128,256]{1,0:T(8,128)(2,1)S(1)} %get-tuple-element.20), channel_id=1, source_target_pairs={{0,24},{1,7},{2,26},{3,1},{4,28},{5,3},{6,30},{7,5},{8,0},{9,15},{... | collective-permute-start | bytes 196616 | tf_op jit(solution)/shard_map/ppermute | solution.py:29
  167.4 4.0 %collective-permute-start.16 = (bf16[128,256]{1,0:T(8,128)(2,1)S(1)}, bf16[128,256]{1,0:T(8,128)(2,1)S(1)}, u32[]{:S(2)}, u32[]{:S(2)}) collective-permute-start(bf16[128,256]{1,0:T(8,128)(2,1)S(1)} %get-tuple-element.21), channel_id=1, source_target_pairs={{0,16},{1,5},{2,18},{3,7},{4,20},{5,1},{6,22},{7,3},{8,24},{9,13},... | collective-permute-start | bytes 196616 | tf_op jit(solution)/shard_map/ppermute | solution.py:29
  171.4 3.7 %collective-permute-done.16 = bf16[128,256]{1,0:T(8,128)(2,1)S(1)} collective-permute-done((bf16[128,256]{1,0:T(8,128)(2,1)S(1)}, bf16[128,256]{1,0:T(8,128)(2,1)S(1)}, u32[]{:S(2)}, u32[]{:S(2)}) %collective-permute-start.16) | collective-permute-done | bytes 65568 | tf_op jit(solution)/shard_map/ppermute | solution.py:29
  (66 shorter events, 32.9 us)
Async XLA Ops:
  35.1 3.7 %copy-start.15 = (bf16[128,256]{1,0:T(8,128)(2,1)S(1)}, bf16[128,256]{1,0:T(8,128)(2,1)}, u32[]{:S(2)}) copy-start(bf16[128,256]{1,0:T(8,128)(2,1)} %param.5) | copy-start | bytes 196612
  35.1 3.7 %copy-start.16 = (bf16[128,256]{1,0:T(8,128)(2,1)S(1)}, bf16[128,256]{1,0:T(8,128)(2,1)}, u32[]{:S(2)}) copy-start(bf16[128,256]{1,0:T(8,128)(2,1)} %param.6) | copy-start | bytes 196612
  35.1 49.7 %all-to-all-start.1 = ((bf16[4,264,512]{2,1,0:T(8,128)(2,1)}), bf16[4,264,512]{2,1,0:T(8,128)(2,1)S(1)}, u32[]{:S(2)}, u32[]{:S(2)}) async-start(bf16[4,264,512]{2,1,0:T(8,128)(2,1)} %shard_map.85), calls=%async_computation.1 | async-start | bytes 2162688 | tf_op jit(solution)/shard_map/all_to_all | solution.py:229
  38.9 3.1 %collective-permute-start = (bf16[128,256]{1,0:T(8,128)(2,1)S(1)}, bf16[128,256]{1,0:T(8,128)(2,1)S(1)}, u32[]{:S(2)}, u32[]{:S(2)}) collective-permute-start(bf16[128,256]{1,0:T(8,128)(2,1)S(1)} %get-tuple-element.25), channel_id=1, source_target_pairs={{0,1},{1,0},{2,3},{3,2},{4,5},{5,4},{6,7},{7,6},{8,9},{9,8},{10,11... | collective-permute-start | bytes 196616 | tf_op jit(solution)/shard_map/ppermute | solution.py:19
  42.0 10.8 %collective-permute-start.2 = (bf16[2,128,256]{2,1,0:T(8,128)(2,1)S(1)}, bf16[2,128,256]{2,1,0:T(8,128)(2,1)S(1)}, u32[]{:S(2)}, u32[]{:S(2)}) collective-permute-start(bf16[2,128,256]{2,1,0:T(8,128)(2,1)S(1)} %get-tuple-element.23), channel_id=1, source_target_pairs={{0,4},{1,17},{2,6},{3,19},{4,0},{5,21},{6,2},{7,23},{8,12},{9,25},... | collective-permute-start | bytes 393224 | tf_op jit(solution)/shard_map/ppermute | solution.py:29
  47.0 6.9 %collective-permute-start.1 = (bf16[2,128,256]{2,1,0:T(8,128)(2,1)S(1)}, bf16[2,128,256]{2,1,0:T(8,128)(2,1)S(1)}, u32[]{:S(2)}, u32[]{:S(2)}) collective-permute-start(bf16[2,128,256]{2,1,0:T(8,128)(2,1)S(1)} %get-tuple-element.23), channel_id=1, source_target_pairs={{0,6},{1,25},{2,0},{3,27},{4,2},{5,29},{6,4},{7,31},{8,14},{9,1},{... | collective-permute-start | bytes 393224 | tf_op jit(solution)/shard_map/ppermute | solution.py:29
  50.0 8.1 %collective-permute-start.3 = (bf16[2,128,256]{2,1,0:T(8,128)(2,1)S(1)}, bf16[2,128,256]{2,1,0:T(8,128)(2,1)S(1)}, u32[]{:S(2)}, u32[]{:S(2)}) collective-permute-start(bf16[2,128,256]{2,1,0:T(8,128)(2,1)S(1)} %get-tuple-element.23), channel_id=1, source_target_pairs={{0,2},{1,9},{2,4},{3,11},{4,6},{5,13},{6,0},{7,15},{8,10},{9,17},{... | collective-permute-start | bytes 393224 | tf_op jit(solution)/shard_map/ppermute | solution.py:29
  58.2 11.8 %collective-permute-start.6 = (bf16[4,2,128,256]{3,2,1,0:T(8,128)(2,1)S(1)}, bf16[4,2,128,256]{3,2,1,0:T(8,128)(2,1)S(1)}, u32[]{:S(2)}, u32[]{:S(2)}) collective-permute-start(bf16[4,2,128,256]{3,2,1,0:T(8,128)(2,1)S(1)} %pad_maximum_fusion.refs_0_), channel_id=1, source_target_pairs={{0,8},{1,3},{2,10},{3,5},{4,12},{5,7},{6,14},{7,1},{8,16},{9,11},{... | collective-permute-start | bytes 1572872 | tf_op jit(solution)/shard_map/ppermute | solution.py:29
  60.6 12.7 %collective-permute-start.5 = (bf16[4,2,128,256]{3,2,1,0:T(8,128)(2,1)S(1)}, bf16[4,2,128,256]{3,2,1,0:T(8,128)(2,1)S(1)}, u32[]{:S(2)}, u32[]{:S(2)}) collective-permute-start(bf16[4,2,128,256]{3,2,1,0:T(8,128)(2,1)S(1)} %pad_maximum_fusion.refs_0_), channel_id=1, source_target_pairs={{0,16},{1,5},{2,18},{3,7},{4,20},{5,1},{6,22},{7,3},{8,24},{9,13},... | collective-permute-start | bytes 1572872 | tf_op jit(solution)/shard_map/ppermute | solution.py:29
  65.5 13.3 %collective-permute-start.4 = (bf16[4,2,128,256]{3,2,1,0:T(8,128)(2,1)S(1)}, bf16[4,2,128,256]{3,2,1,0:T(8,128)(2,1)S(1)}, u32[]{:S(2)}, u32[]{:S(2)}) collective-permute-start(bf16[4,2,128,256]{3,2,1,0:T(8,128)(2,1)S(1)} %pad_maximum_fusion.refs_0_), channel_id=1, source_target_pairs={{0,24},{1,7},{2,26},{3,1},{4,28},{5,3},{6,30},{7,5},{8,0},{9,15},{... | collective-permute-start | bytes 1572872 | tf_op jit(solution)/shard_map/ppermute | solution.py:29
  68.0 13.6 %collective-permute-start.7 = (bf16[4,2,128,256]{3,2,1,0:T(8,128)(2,1)S(1)}, bf16[4,2,128,256]{3,2,1,0:T(8,128)(2,1)S(1)}, u32[]{:S(2)}, u32[]{:S(2)}) collective-permute-start(bf16[4,2,128,256]{3,2,1,0:T(8,128)(2,1)S(1)} %pad_maximum_fusion.refs_0_), channel_id=1, source_target_pairs={{0,1},{1,0},{2,3},{3,2},{4,5},{5,4},{6,7},{7,6},{8,9},{9,8},{10,11... | collective-permute-start | bytes 1572872 | tf_op jit(solution)/shard_map/ppermute | solution.py:19
  69.9 12.4 %collective-permute-start.10 = (bf16[4,2,128,256]{3,2,1,0:T(8,128)(2,1)S(1)}, bf16[4,2,128,256]{3,2,1,0:T(8,128)(2,1)S(1)}, u32[]{:S(2)}, u32[]{:S(2)}) collective-permute-start(bf16[4,2,128,256]{3,2,1,0:T(8,128)(2,1)S(1)} %collective-permute-done.6.refs_3_), channel_id=1, source_target_pairs={{0,1},{1,0},{2,3},{3,2},{4,5},{5,4},{6,7},{7,6},{8,9},{9,8},{10,11... | collective-permute-start | bytes 1572872 | tf_op jit(solution)/shard_map/ppermute | solution.py:19
  73.3 9.9 %collective-permute-start.9 = (bf16[4,2,128,256]{3,2,1,0:T(8,128)(2,1)S(1)}, bf16[4,2,128,256]{3,2,1,0:T(8,128)(2,1)S(1)}, u32[]{:S(2)}, u32[]{:S(2)}) collective-permute-start(bf16[4,2,128,256]{3,2,1,0:T(8,128)(2,1)S(1)} %collective-permute-done.5.refs_2_), channel_id=1, source_target_pairs={{0,1},{1,0},{2,3},{3,2},{4,5},{5,4},{6,7},{7,6},{8,9},{9,8},{10,11... | collective-permute-start | bytes 1572872 | tf_op jit(solution)/shard_map/ppermute | solution.py:19
  78.8 5.2 %collective-permute-start.8 = (bf16[4,2,128,256]{3,2,1,0:T(8,128)(2,1)S(1)}, bf16[4,2,128,256]{3,2,1,0:T(8,128)(2,1)S(1)}, u32[]{:S(2)}, u32[]{:S(2)}) collective-permute-start(bf16[4,2,128,256]{3,2,1,0:T(8,128)(2,1)S(1)} %collective-permute-done.4.refs_1_), channel_id=1, source_target_pairs={{0,1},{1,0},{2,3},{3,2},{4,5},{5,4},{6,7},{7,6},{8,9},{9,8},{10,11... | collective-permute-start | bytes 1572872 | tf_op jit(solution)/shard_map/ppermute | solution.py:19
  84.8 1.0 copy-start.1
  95.6 32.1 %all-to-all-start.2 = ((bf16[4,264,512]{2,1,0:T(8,128)(2,1)}), bf16[4,264,512]{2,1,0:T(8,128)(2,1)S(1)}, u32[]{:S(2)}, u32[]{:S(2)}) async-start(bf16[4,264,512]{2,1,0:T(8,128)(2,1)} %get-tuple-element.12), calls=%async_computation.2 | async-start | bytes 2162688 | tf_op jit(solution)/shard_map/all_to_all | solution.py:249
  100.7 42.3 %collective-permute-start.11 = (bf16[4,4,128,256]{3,2,1,0:T(8,128)(2,1)}, bf16[4,4,128,256]{3,2,1,0:T(8,128)(2,1)}, u32[]{:S(2)}, u32[]{:S(2)}) collective-permute-start(bf16[4,4,128,256]{3,2,1,0:T(8,128)(2,1)} %get-tuple-element.11), channel_id=1, source_target_pairs={{0,1},{1,0},{2,3},{3,2},{4,5},{5,4},{6,7},{7,6},{8,9},{9,8},{10,11... | collective-permute-start | bytes 3145736 | tf_op jit(solution)/shard_map/ppermute | solution.py:19
  128.8 47.0 %all-to-all-start.3 = ((bf16[16,136,128]{2,1,0:T(8,128)(2,1)}), bf16[16,136,128]{2,1,0:T(8,128)(2,1)S(1)}, u32[]{:S(2)}, u32[]{:S(2)}) async-start(bf16[16,136,128]{2,1,0:T(8,128)(2,1)} %shard_map.87), calls=%async_computation.3 | async-start | bytes 1114112 | tf_op jit(solution)/shard_map/all_to_all | solution.py:251
  144.6 9.5 %collective-permute-start.12 = (bf16[4,128,256]{2,1,0:T(8,128)(2,1)S(1)}, bf16[4,128,256]{2,1,0:T(8,128)(2,1)S(1)}, u32[]{:S(2)}, u32[]{:S(2)}) collective-permute-start(bf16[4,128,256]{2,1,0:T(8,128)(2,1)S(1)} %get-tuple-element.16), channel_id=1, source_target_pairs={{0,2},{1,9},{2,4},{3,11},{4,6},{5,13},{6,0},{7,15},{8,10},{9,17},{... | collective-permute-start | bytes 786440 | tf_op jit(solution)/shard_map/ppermute | solution.py:29
  146.5 11.9 %collective-permute-start.14 = (bf16[4,128,256]{2,1,0:T(8,128)(2,1)S(1)}, bf16[4,128,256]{2,1,0:T(8,128)(2,1)S(1)}, u32[]{:S(2)}, u32[]{:S(2)}) collective-permute-start(bf16[4,128,256]{2,1,0:T(8,128)(2,1)S(1)} %get-tuple-element.17), channel_id=1, source_target_pairs={{0,6},{1,25},{2,0},{3,27},{4,2},{5,29},{6,4},{7,31},{8,14},{9,1},{... | collective-permute-start | bytes 786440 | tf_op jit(solution)/shard_map/ppermute | solution.py:29
  151.6 9.8 %collective-permute-start.13 = (bf16[4,128,256]{2,1,0:T(8,128)(2,1)S(1)}, bf16[4,128,256]{2,1,0:T(8,128)(2,1)S(1)}, u32[]{:S(2)}, u32[]{:S(2)}) collective-permute-start(bf16[4,128,256]{2,1,0:T(8,128)(2,1)S(1)} %get-tuple-element.18), channel_id=1, source_target_pairs={{0,4},{1,17},{2,6},{3,19},{4,0},{5,21},{6,2},{7,23},{8,12},{9,25},... | collective-permute-start | bytes 786440 | tf_op jit(solution)/shard_map/ppermute | solution.py:29
  161.6 9.8 %collective-permute-start.15 = (bf16[128,256]{1,0:T(8,128)(2,1)S(1)}, bf16[128,256]{1,0:T(8,128)(2,1)S(1)}, u32[]{:S(2)}, u32[]{:S(2)}) collective-permute-start(bf16[128,256]{1,0:T(8,128)(2,1)S(1)} %get-tuple-element.19), channel_id=1, source_target_pairs={{0,8},{1,3},{2,10},{3,5},{4,12},{5,7},{6,14},{7,1},{8,16},{9,11},{... | collective-permute-start | bytes 196616 | tf_op jit(solution)/shard_map/ppermute | solution.py:29
  165.0 6.5 %collective-permute-start.17 = (bf16[128,256]{1,0:T(8,128)(2,1)S(1)}, bf16[128,256]{1,0:T(8,128)(2,1)S(1)}, u32[]{:S(2)}, u32[]{:S(2)}) collective-permute-start(bf16[128,256]{1,0:T(8,128)(2,1)S(1)} %get-tuple-element.20), channel_id=1, source_target_pairs={{0,24},{1,7},{2,26},{3,1},{4,28},{5,3},{6,30},{7,5},{8,0},{9,15},{... | collective-permute-start | bytes 196616 | tf_op jit(solution)/shard_map/ppermute | solution.py:29
  167.4 7.7 %collective-permute-start.16 = (bf16[128,256]{1,0:T(8,128)(2,1)S(1)}, bf16[128,256]{1,0:T(8,128)(2,1)S(1)}, u32[]{:S(2)}, u32[]{:S(2)}) collective-permute-start(bf16[128,256]{1,0:T(8,128)(2,1)S(1)} %get-tuple-element.21), channel_id=1, source_target_pairs={{0,16},{1,5},{2,18},{3,7},{4,20},{5,1},{6,22},{7,3},{8,24},{9,13},... | collective-permute-start | bytes 196616 | tf_op jit(solution)/shard_map/ppermute | solution.py:29
  (14 other events, 12.5 us)

commit v2 on v1

v2 whole, which is shorter than its diff:
```python
import jax
import jax.numpy as jnp
from jax import lax
from jax.experimental import pallas as pl
from jax.experimental.pallas import tpu as pltpu
from jax.sharding import Mesh, PartitionSpec as P


BF = jnp.bfloat16
F32 = jnp.float32
NQ, NR, NY, NX, NC = 2, 4, 4, 4, 2
PLANE = ("y", "x", "c")
VM = pl.BlockSpec(memory_space=pltpu.VMEM)
NN = ((1,), (0,))
NT = ((1,), (1,))


def swapped(value):
    return lax.ppermute(value, "c", [(0, 1), (1, 0)])


def moved(value, k, x_core):
    pairs = []
    for y in range(NY):
        for x in range(NX):
            for c in range(NC):
                ty, tx = (y, (x + k) % NX) if c == x_core else ((y + k) % NY, x)
                pairs.append(((y * NX + x) * NC + c, (ty * NX + tx) * NC + c))
    return lax.ppermute(value, PLANE, pairs)


def line_gather(value, x_core):
    return [value] + [moved(value, -k, x_core) for k in (1, 2, 3)]


def line_sum(value, x_core):
    total = value[0].astype(F32)
    for k in (1, 2, 3):
        total = total + moved(value[k], k, x_core).astype(F32)
    return total.astype(BF)


def dot(a, b, dims):
    return lax.dot_general(a, b, (dims, ((), ())), preferred_element_type=F32)


def call(body, args, shapes, mib=8, far_in=0, far_out=False, own=()):
    single = not isinstance(shapes, (list, tuple))
    shapes = [shapes] if single else list(shapes)
    n, m = len(args), len(shapes)
    loads, stores = far_in, m if far_out else 0

    def whole(*refs):
        ins, outs, rest = list(refs[:n]), list(refs[n : n + m]), refs[n + m :]
        mid = loads + stores
        near_in, near_out = rest[:loads], rest[loads:mid]
        held, rest = rest[mid : mid + len(own)], rest[mid + len(own) :]
        if loads:
            sems = rest[0]
            copies = [pltpu.make_async_copy(ins[i], near_in[i], sems.at[i]) for i in range(loads)]
            for c in copies:
                c.start()
            for c in copies:
                c.wait()
        body(*near_in, *ins[loads:], *(near_out if stores else outs), *held)
        if stores:
            sems = rest[-1]
            copies = [pltpu.make_async_copy(near_out[i], outs[i], sems.at[i]) for i in range(m)]
            for c in copies:
                c.start()
            for c in copies:
                c.wait()

    far = pl.BlockSpec(memory_space=pltpu.HBM)
    scratch = [pltpu.VMEM(a.shape, a.dtype) for a in args[:loads]]
    scratch += [pltpu.VMEM(a.shape, a.dtype) for a in shapes[:stores]]
    scratch += list(own)
    scratch += [pltpu.SemaphoreType.DMA((k,)) for k in (loads, stores) if k]
    out = pl.pallas_call(
        whole,
        in_specs=[far] * loads + [VM] * (n - loads),
        out_specs=[far if far_out else VM] * m,
        out_shape=shapes,
        scratch_shapes=scratch,
        compiler_params=pltpu.CompilerParams(vmem_limit_bytes=mib * 2**20),
    )(*args)
    return out[0] if single else out


def sides(a, b):
    return jnp.concatenate([a, b], axis=1)


def pack_body(wg, wu, wd, out):
    hid = wd.shape[1] // NY
    tg = wg[...].astype(F32).T
    tu = wu[...].astype(F32).T
    td = wd[...].astype(F32).T
    parts = []
    for y in range(NY):
        s = slice(y * hid, (y + 1) * hid)
        parts.append(jnp.concatenate([tg[s], tu[s], td[s]], axis=0))
    out[0] = sides(parts[0], parts[2]).astype(BF)
    out[1] = sides(parts[1], parts[3]).astype(BF)


def spread_body(own, far, out):
    half = own.shape[2] // 2
    for i in range(2):
        o, f = own[i].astype(F32), far[i].astype(F32)
        low = sides(o[:, :half], f[:, :half]).astype(BF)
        high = sides(o[:, half:], f[:, half:]).astype(BF)
        for r in range(NR):
            out[r * NY + i] = low
            out[r * NY + i + 2] = high


def layer_body(mine, other, chunks, keep, send, pieces, wt, made):
    core = lax.axis_index("c")
    x_here = lax.axis_index("x")
    zq = lax.axis_index("zq")
    hid = chunks.shape[1] // 3
    half = chunks.shape[2] // 2

    for r in range(NR):
        for side in range(NQ):
            cut = slice(side * half, (side + 1) * half)
            wt[NQ * r + side] = jnp.concatenate(
                [chunks[r * NY + y][:, cut] for y in range(NY)], axis=1
            )

    def run(even, odd, me):
        def block(k, c, which):
            if c == 0:
                return jnp.concatenate([even[j][k, which] for j in range(NY)], axis=0)
            part = odd[k][:, which]
            return part.reshape(NY * part.shape[1], part.shape[2])

        def place(k, c):
            x = (x_here + k) % NX
            return NQ * ((x % 2) * NC + c) + (x // 2 + zq) % NQ

        blocks = [(k, c) for k in range(NX) for c in range(NC)]
        pre = None
        hid_grad = None
        for k, c in blocks:
            i = place(k, c)
            p = dot(wt[i, : 2 * hid, :], block(k, c, 0), NT)
            q = dot(wt[i, 2 * hid :, :], block(k, c, 1), NT)
            pre = p if pre is None else pre + p
            hid_grad = q if hid_grad is None else hid_grad + q
        gate = pre[:hid]
        up = pre[hid:]
        sig = jax.nn.sigmoid(gate)
        act = gate * sig
        hidden = (act * up).astype(BF)
        g_gate = hid_grad * up * sig * (1.0 + gate * (1.0 - sig))
        g_up = hid_grad * act
        g_both = jnp.concatenate([g_gate, g_up], axis=0)
        g_turned = g_both.T.astype(BF)
        g_both = g_both.astype(BF)
        for k, c in blocks:
            i = place(k, c)
            made[i, : 2 * hid, :] = dot(g_both, block(k, c, 0), NN).astype(BF)
            made[i, 2 * hid :, :] = dot(hidden, block(k, c, 1), NN).astype(BF)
            gi = dot(g_turned, wt[i, : 2 * hid, :], NN).astype(BF)
            rows = gi.shape[0] // NY
            ref = keep if c == me else send
            for j in range(NY):
                piece = gi[j * rows : (j + 1) * rows]
                if c == 0:
                    ref[k, j] = piece
                else:
                    ref[j, k] = piece

    @pl.when(core == 0)
    def _():
        run(mine, other, 0)

    @pl.when(core == 1)
    def _():
        run(other, mine, 1)

    for r in range(NR):
        for y in range(NY):
            s = slice(y * half, (y + 1) * half)
            pieces[r * NY + y] = sides(made[NQ * r, :, s], made[NQ * r + 1, :, s])


def sum_body(pieces, out):
    zq = lax.axis_index("zq")
    half = pieces.shape[2] // 2

    def total(y):
        s = pieces[y].astype(F32)
        for r in range(1, NR):
            s = s + pieces[r * NY + y].astype(F32)
        return s

    for i in range(2):
        low, high = total(i), total(i + 2)
        own = sides(low[:, :half], high[:, :half]).astype(BF)
        far = sides(low[:, half:], high[:, half:]).astype(BF)
        for h in range(2):
            out[2 * h + zq, i] = own
            out[2 * h + 1 - zq, i] = far


def last_body(parts, gg, gu, gd):
    hid = parts.shape[2] // 3
    half = parts.shape[3] // 2
    s = []
    for i in range(2):
        v = parts[0, i].astype(F32)
        for q in range(1, 4):
            v = v + parts[q, i].astype(F32)
        s.append(v)
    by_y = [s[0][:, :half], s[1][:, :half], s[0][:, half:], s[1][:, half:]]
    gg[...] = jnp.concatenate([b[:hid] for b in by_y], axis=0).T
    gu[...] = jnp.concatenate([b[hid : 2 * hid] for b in by_y], axis=0).T
    gd[...] = jnp.concatenate([b[2 * hid :] for b in by_y], axis=0).T


def per_device(inputs, cotangent, gate_weight, up_weight, down_weight):
    S = jax.ShapeDtypeStruct
    rows_d, ff = gate_weight.shape
    hid = ff // NY
    rows, cols = inputs.shape

    packed = call(
        pack_body,
        (gate_weight, up_weight, down_weight.T),
        S((2, 3 * hid, 2 * rows_d), BF),
        60,
        far_in=3,
    )
    far = lax.ppermute(packed, "zq", [(0, 1), (1, 0)])
    chunks = call(spread_body, (packed, far), S((NR * NY, 3 * hid, 2 * rows_d), BF))
    chunks = lax.all_to_all(chunks, ("zr", "y"), 0, 0, tiled=True)

    block = jnp.stack([inputs, cotangent])
    line = jnp.stack(line_gather(block, 0))
    mine = line_gather(line, 1)
    other = [swapped(m) for m in mine]

    tiles = S((4, 4, rows, cols), BF)

    def body(*refs):
        layer_body(refs[:4], refs[4:8], *refs[8:])

    blocks = pltpu.VMEM((NQ * NR, 3 * hid, NY * rows_d), BF)
    keep, send, pieces = call(
        body,
        (*mine, *other, chunks),
        [tiles, tiles, S(chunks.shape, BF)],
        60,
        far_in=9,
        far_out=True,
        own=[blocks, blocks],
    )

    pieces = lax.all_to_all(pieces, ("zr", "y"), 0, 0, tiled=True)
    ring = call(sum_body, (pieces,), S((4, 2, 3 * hid, 2 * rows_d), BF))
    ring = lax.all_to_all(ring, ("zh", "zq"), 0, 0, tiled=True)
    g_gate, g_up, g_down = call(last_body, (ring,), [S((rows_d, ff), F32)] * 3)

    theirs = swapped(send)
    chip = (keep.astype(F32) + theirs.astype(F32)).astype(BF)
    part = line_sum(chip, 0)
    done = line_sum(part, 1)
    return (done, g_gate, g_up, g_down.T)


def solution(mesh):
    fine = Mesh(mesh.devices.reshape(2, NQ, NR, NY, NX, NC), ("zh", "zq", "zr", "y", "x", "c"))
    tok, fs, tp = ("zh", "zq", "zr", "y"), ("zq", "zr", "y"), ("x", "c")

    return jax.shard_map(
        per_device,
        mesh=fine,
        in_specs=(P(tok, tp), P(tok, tp), P(fs, tp), P(fs, tp), P(tp, fs)),
        out_specs=(P(tok, tp), P(fs, tp), P(fs, tp), P(tp, fs)),
        check_vma=False,
    )
```

time: 178 us -> 165 us (0.927)
  the two profiles are of different devices: /device:TPU:8 before, /device:TPU:32 now
where the time goes in v2:
time: 165 us; the launch traced here: 164 us
  starting transfers between devices  88.7 us (54%)
  waiting for transfers between devices  57.2 us (35%)
  Pallas kernels  12.3 us (7%)
  local copies, waits for them, and re-layouts  3.79 us (2%)
    ppermute x12, starting transfers between devices, moved(): return lax.ppermute(value, PLANE, pairs)  41.2 us
    all_to_all x1, waiting for transfers between devices, per_device(): pieces = lax.all_to_all(pieces, ('zr', 'y'), 0, 0, tiled=True)  24.8 us
    ppermute x12, waiting for transfers between devices, moved(): return lax.ppermute(value, PLANE, pairs)  22.7 us
    pallas_call x5, Pallas kernels, call(): pl.pallas_call(whole, in_specs=[far] * loads + [VM] * (n - loads), out_sp...  12.3 us
    all_to_all x1, starting transfers between devices, per_device(): ring = lax.all_to_all(ring, ('zh', 'zq'), 0, 0, tiled=True)  11.1 us
    ppermute x5, starting transfers between devices, swapped(): return lax.ppermute(value, 'c', [(0, 1), (1, 0)])  10.3 us
    ppermute x1, waiting for transfers between devices, per_device(): far = lax.ppermute(packed, 'zq', [(0, 1), (1, 0)])  9.67 us
    all_to_all x1, starting transfers between devices, per_device(): chunks = lax.all_to_all(chunks, ('zr', 'y'), 0, 0, tiled=True)  9.57 us
  transfers between devices with their start and end apart: 21, of which 10 were waited for; matrix products, arithmetic and copies ran while one was open for 1% of the time, Pallas kernels for 1%

profile of v2, /device:TPU:32, one launch (start us, length us, event | category | flops | bytes accessed | tf_op | source)
XLA Modules:
  0.0 164.2 jit_solution(5456593574549754465)
XLA Ops:
  2.4 9.1 %collective-permute-start.10 = (bf16[2,264,128]{2,1,0:T(8,128)(2,1)}, bf16[2,264,128]{2,1,0:T(8,128)(2,1)S(1)}, u32[]{:S(2)}, u32[]{:S(2)}) collective-permute-start(bf16[2,264,128]{2,1,0:T(8,128)(2,1)} %shard_map.84.refs_0_), channel_id=1, source_target_pairs={{0,128},{128,0},{1,129},{129,1},{2,130},{130,2},{3,131},{131,3},{4... | collective-permute-start | bytes 405512 | tf_op jit(solution)/shard_map/ppermute | solution.py:237
  11.5 9.7 %collective-permute-done.10.refs_1_ = bf16[2,264,128]{2,1,0:T(8,128)(2,1)S(1)} collective-permute-done((bf16[2,264,128]{2,1,0:T(8,128)(2,1)}, bf16[2,264,128]{2,1,0:T(8,128)(2,1)S(1)}, u32[]{:S(2)}, u32[]{:S(2)}) %collective-permute-start.10) | collective-permute-done | bytes 135200 | tf_op jit(solution)/shard_map/ppermute | solution.py:237
  23.2 9.6 %all-to-all-start = ((bf16[16,264,128]{2,1,0:T(8,128)(2,1)}), bf16[16,264,128]{2,1,0:T(8,128)(2,1)S(1)}, u32[]{:S(2)}, u32[]{:S(2)}) async-start(bf16[16,264,128]{2,1,0:T(8,128)(2,1)} %shard_map.85), calls=%async_computation | async-start | bytes 2162688 | tf_op jit(solution)/shard_map/all_to_all | solution.py:239
  32.9 4.9 %collective-permute-start.1 = (bf16[2,128,256]{2,1,0:T(8,128)(2,1)S(1)}, bf16[2,128,256]{2,1,0:T(8,128)(2,1)S(1)}, u32[]{:S(2)}, u32[]{:S(2)}) collective-permute-start(bf16[2,128,256]{2,1,0:T(8,128)(2,1)S(1)} %get-tuple-element.23), channel_id=1, source_target_pairs={{0,4},{1,17},{2,6},{3,19},{4,0},{5,21},{6,2},{7,23},{8,12},{9,25},... | collective-permute-start | bytes 393224 | tf_op jit(solution)/shard_map/ppermute | solution.py:29
  37.8 3.0 %collective-permute-start = (bf16[2,128,256]{2,1,0:T(8,128)(2,1)S(1)}, bf16[2,128,256]{2,1,0:T(8,128)(2,1)S(1)}, u32[]{:S(2)}, u32[]{:S(2)}) collective-permute-start(bf16[2,128,256]{2,1,0:T(8,128)(2,1)S(1)} %get-tuple-element.23), channel_id=1, source_target_pairs={{0,6},{1,25},{2,0},{3,27},{4,2},{5,29},{6,4},{7,31},{8,14},{9,1},{... | collective-permute-start | bytes 393224 | tf_op jit(solution)/shard_map/ppermute | solution.py:29
  40.9 2.8 %collective-permute-start.2 = (bf16[2,128,256]{2,1,0:T(8,128)(2,1)S(1)}, bf16[2,128,256]{2,1,0:T(8,128)(2,1)S(1)}, u32[]{:S(2)}, u32[]{:S(2)}) collective-permute-start(bf16[2,128,256]{2,1,0:T(8,128)(2,1)S(1)} %get-tuple-element.23), channel_id=1, source_target_pairs={{0,2},{1,9},{2,4},{3,11},{4,6},{5,13},{6,0},{7,15},{8,10},{9,17},{... | collective-permute-start | bytes 393224 | tf_op jit(solution)/shard_map/ppermute | solution.py:29
  44.7 4.3 %collective-permute-done.2 = bf16[2,128,256]{2,1,0:T(8,128)(2,1)S(1)} collective-permute-done((bf16[2,128,256]{2,1,0:T(8,128)(2,1)S(1)}, bf16[2,128,256]{2,1,0:T(8,128)(2,1)S(1)}, u32[]{:S(2)}, u32[]{:S(2)}) %collective-permute-start.2) | collective-permute-done | bytes 131104 | tf_op jit(solution)/shard_map/ppermute | solution.py:29
  49.0 3.4 %collective-permute-start.5 = (bf16[4,2,128,256]{3,2,1,0:T(8,128)(2,1)S(1)}, bf16[4,2,128,256]{3,2,1,0:T(8,128)(2,1)S(1)}, u32[]{:S(2)}, u32[]{:S(2)}) collective-permute-start(bf16[4,2,128,256]{3,2,1,0:T(8,128)(2,1)S(1)} %pad_maximum_fusion.refs_0_), channel_id=1, source_target_pairs={{0,8},{1,3},{2,10},{3,5},{4,12},{5,7},{6,14},{7,1},{8,16},{9,11},{... | collective-permute-start | bytes 1572872 | tf_op jit(solution)/shard_map/ppermute | solution.py:29
  52.4 4.6 %collective-permute-start.4 = (bf16[4,2,128,256]{3,2,1,0:T(8,128)(2,1)S(1)}, bf16[4,2,128,256]{3,2,1,0:T(8,128)(2,1)S(1)}, u32[]{:S(2)}, u32[]{:S(2)}) collective-permute-start(bf16[4,2,128,256]{3,2,1,0:T(8,128)(2,1)S(1)} %pad_maximum_fusion.refs_0_), channel_id=1, source_target_pairs={{0,16},{1,5},{2,18},{3,7},{4,20},{5,1},{6,22},{7,3},{8,24},{9,13},... | collective-permute-start | bytes 1572872 | tf_op jit(solution)/shard_map/ppermute | solution.py:29
  57.0 3.4 %collective-permute-start.3 = (bf16[4,2,128,256]{3,2,1,0:T(8,128)(2,1)S(1)}, bf16[4,2,128,256]{3,2,1,0:T(8,128)(2,1)S(1)}, u32[]{:S(2)}, u32[]{:S(2)}) collective-permute-start(bf16[4,2,128,256]{3,2,1,0:T(8,128)(2,1)S(1)} %pad_maximum_fusion.refs_0_), channel_id=1, source_target_pairs={{0,24},{1,7},{2,26},{3,1},{4,28},{5,3},{6,30},{7,5},{8,0},{9,15},{... | collective-permute-start | bytes 1572872 | tf_op jit(solution)/shard_map/ppermute | solution.py:29
  64.7 4.5 %collective-permute-done.4.refs_2_ = bf16[4,2,128,256]{3,2,1,0:T(8,128)(2,1)S(1)} collective-permute-done((bf16[4,2,128,256]{3,2,1,0:T(8,128)(2,1)S(1)}, bf16[4,2,128,256]{3,2,1,0:T(8,128)(2,1)S(1)}, u32[]{:S(2)}, u32[]{:S(2)}) %collective-permute-start.4) | collective-permute-done | bytes 524320 | tf_op jit(solution)/shard_map/ppermute | solution.py:29
  71.2 2.4 %collective-permute-start.7 = (bf16[4,2,128,256]{3,2,1,0:T(8,128)(2,1)S(1)}, bf16[4,2,128,256]{3,2,1,0:T(8,128)(2,1)}, u32[]{:S(2)}, u32[]{:S(2)}) collective-permute-start(bf16[4,2,128,256]{3,2,1,0:T(8,128)(2,1)S(1)} %collective-permute-done.3.refs_1_), channel_id=1, source_target_pairs={{0,1},{1,0},{2,3},{3,2},{4,5},{5,4},{6,7},{7,6},{8,9},{9,8},{10,11... | collective-permute-start | bytes 1572872 | tf_op jit(solution)/shard_map/ppermute | solution.py:19
  76.5 7.4 %shard_map.86 = (bf16[4,4,128,256]{3,2,1,0:T(8,128)(2,1)}, bf16[4,4,128,256]{3,2,1,0:T(8,128)(2,1)}, bf16[16,264,128]{2,1,0:T(8,128)(2,1)}) custom-call(bf16[4,2,128,256]{3,2,1,0:T(8,128)(2,1)} %copy-done.2, bf16[4,2,128,256]{3,2,1,0:T(8,128)(2,1)} %copy-done.6, bf16[4,2,128,256]{3,2,1,0:T(8,128)(2,1)} %copy-done.5, bf16[4,2,128,256]{3,2,1,0:T(8,128)(2,1)} %copy-done.4, ...), custom_call_target="tpu_custom_call" | custom-call | tf_op jit(solution)/shard_map/pallas_call | solution.py:79
  83.9 7.5 %all-to-all-start.1 = ((bf16[16,264,128]{2,1,0:T(8,128)(2,1)}), bf16[16,264,128]{2,1,0:T(8,128)(2,1)S(1)}, u32[]{:S(2)}, u32[]{:S(2)}) async-start(bf16[16,264,128]{2,1,0:T(8,128)(2,1)} %get-tuple-element.12), calls=%async_computation.1 | async-start | bytes 2162688 | tf_op jit(solution)/shard_map/all_to_all | solution.py:262
  91.4 2.1 %collective-permute-start.11 = (bf16[4,4,128,256]{3,2,1,0:T(8,128)(2,1)}, bf16[4,4,128,256]{3,2,1,0:T(8,128)(2,1)S(1)}, u32[]{:S(2)}, u32[]{:S(2)}) collective-permute-start(bf16[4,4,128,256]{3,2,1,0:T(8,128)(2,1)} %get-tuple-element.11), channel_id=1, source_target_pairs={{0,1},{1,0},{2,3},{3,2},{4,5},{5,4},{6,7},{7,6},{8,9},{9,8},{10,11... | collective-permute-start | bytes 3145736 | tf_op jit(solution)/shard_map/ppermute | solution.py:19
  93.5 24.8 %all-to-all-done.1.refs_0_ = bf16[16,264,128]{2,1,0:T(8,128)(2,1)S(1)} async-done(((bf16[16,264,128]{2,1,0:T(8,128)(2,1)}), bf16[16,264,128]{2,1,0:T(8,128)(2,1)S(1)}, u32[]{:S(2)}, u32[]{:S(2)}) %all-to-all-start.1) | async-done | bytes 1081376 | tf_op jit(solution)/shard_map/all_to_all | solution.py:262
  119.3 11.1 %all-to-all-start.2 = ((bf16[4,2,264,128]{3,2,1,0:T(8,128)(2,1)}), bf16[4,2,264,128]{3,2,1,0:T(8,128)(2,1)S(1)}, u32[]{:S(2)}, u32[]{:S(2)}) async-start(bf16[4,2,264,128]{3,2,1,0:T(8,128)(2,1)} %shard_map.87), calls=%async_computation.2 | async-start | bytes 1081344 | tf_op jit(solution)/shard_map/all_to_all | solution.py:264
  132.8 5.0 %collective-permute-start.14 = (bf16[4,128,256]{2,1,0:T(8,128)(2,1)S(1)}, bf16[4,128,256]{2,1,0:T(8,128)(2,1)S(1)}, u32[]{:S(2)}, u32[]{:S(2)}) collective-permute-start(bf16[4,128,256]{2,1,0:T(8,128)(2,1)S(1)} %get-tuple-element.17), channel_id=1, source_target_pairs={{0,6},{1,25},{2,0},{3,27},{4,2},{5,29},{6,4},{7,31},{8,14},{9,1},{... | collective-permute-start | bytes 786440 | tf_op jit(solution)/shard_map/ppermute | solution.py:29
  140.3 4.3 %collective-permute-done.14 = bf16[4,128,256]{2,1,0:T(8,128)(2,1)S(1)} collective-permute-done((bf16[4,128,256]{2,1,0:T(8,128)(2,1)S(1)}, bf16[4,128,256]{2,1,0:T(8,128)(2,1)S(1)}, u32[]{:S(2)}, u32[]{:S(2)}) %collective-permute-start.14) | collective-permute-done | bytes 262176 | tf_op jit(solution)/shard_map/ppermute | solution.py:29
  144.6 3.1 %collective-permute-done.13 = bf16[4,128,256]{2,1,0:T(8,128)(2,1)S(1)} collective-permute-done((bf16[4,128,256]{2,1,0:T(8,128)(2,1)S(1)}, bf16[4,128,256]{2,1,0:T(8,128)(2,1)S(1)}, u32[]{:S(2)}, u32[]{:S(2)}) %collective-permute-start.13) | collective-permute-done | bytes 262176 | tf_op jit(solution)/shard_map/ppermute | solution.py:29
  147.8 2.2 %collective-permute-start.15 = (bf16[128,256]{1,0:T(8,128)(2,1)S(1)}, bf16[128,256]{1,0:T(8,128)(2,1)S(1)}, u32[]{:S(2)}, u32[]{:S(2)}) collective-permute-start(bf16[128,256]{1,0:T(8,128)(2,1)S(1)} %get-tuple-element.19), channel_id=1, source_target_pairs={{0,8},{1,3},{2,10},{3,5},{4,12},{5,7},{6,14},{7,1},{8,16},{9,11},{... | collective-permute-start | bytes 196616 | tf_op jit(solution)/shard_map/ppermute | solution.py:29
  150.0 4.9 %collective-permute-start.17 = (bf16[128,256]{1,0:T(8,128)(2,1)S(1)}, bf16[128,256]{1,0:T(8,128)(2,1)S(1)}, u32[]{:S(2)}, u32[]{:S(2)}) collective-permute-start(bf16[128,256]{1,0:T(8,128)(2,1)S(1)} %get-tuple-element.20), channel_id=1, source_target_pairs={{0,24},{1,7},{2,26},{3,1},{4,28},{5,3},{6,30},{7,5},{8,0},{9,15},{... | collective-permute-start | bytes 196616 | tf_op jit(solution)/shard_map/ppermute | solution.py:29
  154.9 3.0 %collective-permute-start.16 = (bf16[128,256]{1,0:T(8,128)(2,1)S(1)}, bf16[128,256]{1,0:T(8,128)(2,1)S(1)}, u32[]{:S(2)}, u32[]{:S(2)}) collective-permute-start(bf16[128,256]{1,0:T(8,128)(2,1)S(1)} %get-tuple-element.21), channel_id=1, source_target_pairs={{0,16},{1,5},{2,18},{3,7},{4,20},{5,1},{6,22},{7,3},{8,24},{9,13},... | collective-permute-start | bytes 196616 | tf_op jit(solution)/shard_map/ppermute | solution.py:29
  158.0 4.6 %collective-permute-done.16 = bf16[128,256]{1,0:T(8,128)(2,1)S(1)} collective-permute-done((bf16[128,256]{1,0:T(8,128)(2,1)S(1)}, bf16[128,256]{1,0:T(8,128)(2,1)S(1)}, u32[]{:S(2)}, u32[]{:S(2)}) %collective-permute-start.16) | collective-permute-done | bytes 65568 | tf_op jit(solution)/shard_map/ppermute | solution.py:29
  (54 shorter events, 21.5 us)
Async XLA Ops:
  2.4 18.8 %collective-permute-start.10 = (bf16[2,264,128]{2,1,0:T(8,128)(2,1)}, bf16[2,264,128]{2,1,0:T(8,128)(2,1)S(1)}, u32[]{:S(2)}, u32[]{:S(2)}) collective-permute-start(bf16[2,264,128]{2,1,0:T(8,128)(2,1)} %shard_map.84.refs_0_), channel_id=1, source_target_pairs={{0,128},{128,0},{1,129},{129,1},{2,130},{130,2},{3,131},{131,3},{4... | collective-permute-start | bytes 405512 | tf_op jit(solution)/shard_map/ppermute | solution.py:237
  23.2 52.2 %all-to-all-start = ((bf16[16,264,128]{2,1,0:T(8,128)(2,1)}), bf16[16,264,128]{2,1,0:T(8,128)(2,1)S(1)}, u32[]{:S(2)}, u32[]{:S(2)}) async-start(bf16[16,264,128]{2,1,0:T(8,128)(2,1)} %shard_map.85), calls=%async_computation | async-start | bytes 2162688 | tf_op jit(solution)/shard_map/all_to_all | solution.py:239
  32.9 10.8 %collective-permute-start.1 = (bf16[2,128,256]{2,1,0:T(8,128)(2,1)S(1)}, bf16[2,128,256]{2,1,0:T(8,128)(2,1)S(1)}, u32[]{:S(2)}, u32[]{:S(2)}) collective-permute-start(bf16[2,128,256]{2,1,0:T(8,128)(2,1)S(1)} %get-tuple-element.23), channel_id=1, source_target_pairs={{0,4},{1,17},{2,6},{3,19},{4,0},{5,21},{6,2},{7,23},{8,12},{9,25},... | collective-permute-start | bytes 393224 | tf_op jit(solution)/shard_map/ppermute | solution.py:29
  37.8 6.9 %collective-permute-start = (bf16[2,128,256]{2,1,0:T(8,128)(2,1)S(1)}, bf16[2,128,256]{2,1,0:T(8,128)(2,1)S(1)}, u32[]{:S(2)}, u32[]{:S(2)}) collective-permute-start(bf16[2,128,256]{2,1,0:T(8,128)(2,1)S(1)} %get-tuple-element.23), channel_id=1, source_target_pairs={{0,6},{1,25},{2,0},{3,27},{4,2},{5,29},{6,4},{7,31},{8,14},{9,1},{... | collective-permute-start | bytes 393224 | tf_op jit(solution)/shard_map/ppermute | solution.py:29
  40.9 8.1 %collective-permute-start.2 = (bf16[2,128,256]{2,1,0:T(8,128)(2,1)S(1)}, bf16[2,128,256]{2,1,0:T(8,128)(2,1)S(1)}, u32[]{:S(2)}, u32[]{:S(2)}) collective-permute-start(bf16[2,128,256]{2,1,0:T(8,128)(2,1)S(1)} %get-tuple-element.23), channel_id=1, source_target_pairs={{0,2},{1,9},{2,4},{3,11},{4,6},{5,13},{6,0},{7,15},{8,10},{9,17},{... | collective-permute-start | bytes 393224 | tf_op jit(solution)/shard_map/ppermute | solution.py:29
  49.0 26.5 %copy-start.2 = (bf16[4,2,128,256]{3,2,1,0:T(8,128)(2,1)}, bf16[4,2,128,256]{3,2,1,0:T(8,128)(2,1)S(1)}, u32[]{:S(2)}) copy-start(bf16[4,2,128,256]{3,2,1,0:T(8,128)(2,1)S(1)} %pad_maximum_fusion.refs_0_) | copy-start | bytes 1572868
  49.0 13.7 %collective-permute-start.5 = (bf16[4,2,128,256]{3,2,1,0:T(8,128)(2,1)S(1)}, bf16[4,2,128,256]{3,2,1,0:T(8,128)(2,1)S(1)}, u32[]{:S(2)}, u32[]{:S(2)}) collective-permute-start(bf16[4,2,128,256]{3,2,1,0:T(8,128)(2,1)S(1)} %pad_maximum_fusion.refs_0_), channel_id=1, source_target_pairs={{0,8},{1,3},{2,10},{3,5},{4,12},{5,7},{6,14},{7,1},{8,16},{9,11},{... | collective-permute-start | bytes 1572872 | tf_op jit(solution)/shard_map/ppermute | solution.py:29
  52.4 16.9 %collective-permute-start.4 = (bf16[4,2,128,256]{3,2,1,0:T(8,128)(2,1)S(1)}, bf16[4,2,128,256]{3,2,1,0:T(8,128)(2,1)S(1)}, u32[]{:S(2)}, u32[]{:S(2)}) collective-permute-start(bf16[4,2,128,256]{3,2,1,0:T(8,128)(2,1)S(1)} %pad_maximum_fusion.refs_0_), channel_id=1, source_target_pairs={{0,16},{1,5},{2,18},{3,7},{4,20},{5,1},{6,22},{7,3},{8,24},{9,13},... | collective-permute-start | bytes 1572872 | tf_op jit(solution)/shard_map/ppermute | solution.py:29
  57.0 14.2 %collective-permute-start.3 = (bf16[4,2,128,256]{3,2,1,0:T(8,128)(2,1)S(1)}, bf16[4,2,128,256]{3,2,1,0:T(8,128)(2,1)S(1)}, u32[]{:S(2)}, u32[]{:S(2)}) collective-permute-start(bf16[4,2,128,256]{3,2,1,0:T(8,128)(2,1)S(1)} %pad_maximum_fusion.refs_0_), channel_id=1, source_target_pairs={{0,24},{1,7},{2,26},{3,1},{4,28},{5,3},{6,30},{7,5},{8,0},{9,15},{... | collective-permute-start | bytes 1572872 | tf_op jit(solution)/shard_map/ppermute | solution.py:29
  60.4 13.3 %collective-permute-start.6 = (bf16[4,2,128,256]{3,2,1,0:T(8,128)(2,1)S(1)}, bf16[4,2,128,256]{3,2,1,0:T(8,128)(2,1)S(1)}, u32[]{:S(2)}, u32[]{:S(2)}) collective-permute-start(bf16[4,2,128,256]{3,2,1,0:T(8,128)(2,1)S(1)} %pad_maximum_fusion.refs_0_), channel_id=1, source_target_pairs={{0,1},{1,0},{2,3},{3,2},{4,5},{5,4},{6,7},{7,6},{8,9},{9,8},{10,11... | collective-permute-start | bytes 1572872 | tf_op jit(solution)/shard_map/ppermute | solution.py:19
  62.7 12.7 %copy-start.4 = (bf16[4,2,128,256]{3,2,1,0:T(8,128)(2,1)}, bf16[4,2,128,256]{3,2,1,0:T(8,128)(2,1)S(1)}, u32[]{:S(2)}) copy-start(bf16[4,2,128,256]{3,2,1,0:T(8,128)(2,1)S(1)} %collective-permute-done.5.refs_3_) | copy-start | bytes 1572868
  62.7 10.9 %collective-permute-start.9 = (bf16[4,2,128,256]{3,2,1,0:T(8,128)(2,1)S(1)}, bf16[4,2,128,256]{3,2,1,0:T(8,128)(2,1)S(1)}, u32[]{:S(2)}, u32[]{:S(2)}) collective-permute-start(bf16[4,2,128,256]{3,2,1,0:T(8,128)(2,1)S(1)} %collective-permute-done.5.refs_3_), channel_id=1, source_target_pairs={{0,1},{1,0},{2,3},{3,2},{4,5},{5,4},{6,7},{7,6},{8,9},{9,8},{10,11... | collective-permute-start | bytes 1572872 | tf_op jit(solution)/shard_map/ppermute | solution.py:19
  69.3 4.4 %collective-permute-start.8 = (bf16[4,2,128,256]{3,2,1,0:T(8,128)(2,1)S(1)}, bf16[4,2,128,256]{3,2,1,0:T(8,128)(2,1)S(1)}, u32[]{:S(2)}, u32[]{:S(2)}) collective-permute-start(bf16[4,2,128,256]{3,2,1,0:T(8,128)(2,1)S(1)} %collective-permute-done.4.refs_2_), channel_id=1, source_target_pairs={{0,1},{1,0},{2,3},{3,2},{4,5},{5,4},{6,7},{7,6},{8,9},{9,8},{10,11... | collective-permute-start | bytes 1572872 | tf_op jit(solution)/shard_map/ppermute | solution.py:19
  71.2 4.3 %collective-permute-start.7 = (bf16[4,2,128,256]{3,2,1,0:T(8,128)(2,1)S(1)}, bf16[4,2,128,256]{3,2,1,0:T(8,128)(2,1)}, u32[]{:S(2)}, u32[]{:S(2)}) collective-permute-start(bf16[4,2,128,256]{3,2,1,0:T(8,128)(2,1)S(1)} %collective-permute-done.3.refs_1_), channel_id=1, source_target_pairs={{0,1},{1,0},{2,3},{3,2},{4,5},{5,4},{6,7},{7,6},{8,9},{9,8},{10,11... | collective-permute-start | bytes 1572872 | tf_op jit(solution)/shard_map/ppermute | solution.py:19
  83.9 34.4 %all-to-all-start.1 = ((bf16[16,264,128]{2,1,0:T(8,128)(2,1)}), bf16[16,264,128]{2,1,0:T(8,128)(2,1)S(1)}, u32[]{:S(2)}, u32[]{:S(2)}) async-start(bf16[16,264,128]{2,1,0:T(8,128)(2,1)} %get-tuple-element.12), calls=%async_computation.1 | async-start | bytes 2162688 | tf_op jit(solution)/shard_map/all_to_all | solution.py:262
  91.4 39.0 %copy-start.3 = (bf16[4,4,128,256]{3,2,1,0:T(8,128)(2,1)S(1)}, bf16[4,4,128,256]{3,2,1,0:T(8,128)(2,1)}, u32[]{:S(2)}) copy-start(bf16[4,4,128,256]{3,2,1,0:T(8,128)(2,1)} %get-tuple-element.10) | copy-start | bytes 3145732
  91.4 39.0 %collective-permute-start.11 = (bf16[4,4,128,256]{3,2,1,0:T(8,128)(2,1)}, bf16[4,4,128,256]{3,2,1,0:T(8,128)(2,1)S(1)}, u32[]{:S(2)}, u32[]{:S(2)}) collective-permute-start(bf16[4,4,128,256]{3,2,1,0:T(8,128)(2,1)} %get-tuple-element.11), channel_id=1, source_target_pairs={{0,1},{1,0},{2,3},{3,2},{4,5},{5,4},{6,7},{7,6},{8,9},{9,8},{10,11... | collective-permute-start | bytes 3145736 | tf_op jit(solution)/shard_map/ppermute | solution.py:19
  119.3 43.9 %all-to-all-start.2 = ((bf16[4,2,264,128]{3,2,1,0:T(8,128)(2,1)}), bf16[4,2,264,128]{3,2,1,0:T(8,128)(2,1)S(1)}, u32[]{:S(2)}, u32[]{:S(2)}) async-start(bf16[4,2,264,128]{3,2,1,0:T(8,128)(2,1)} %shard_map.87), calls=%async_computation.2 | async-start | bytes 1081344 | tf_op jit(solution)/shard_map/all_to_all | solution.py:264
  130.8 9.5 %collective-permute-start.12 = (bf16[4,128,256]{2,1,0:T(8,128)(2,1)S(1)}, bf16[4,128,256]{2,1,0:T(8,128)(2,1)S(1)}, u32[]{:S(2)}, u32[]{:S(2)}) collective-permute-start(bf16[4,128,256]{2,1,0:T(8,128)(2,1)S(1)} %get-tuple-element.16), channel_id=1, source_target_pairs={{0,2},{1,9},{2,4},{3,11},{4,6},{5,13},{6,0},{7,15},{8,10},{9,17},{... | collective-permute-start | bytes 786440 | tf_op jit(solution)/shard_map/ppermute | solution.py:29
  132.8 11.8 %collective-permute-start.14 = (bf16[4,128,256]{2,1,0:T(8,128)(2,1)S(1)}, bf16[4,128,256]{2,1,0:T(8,128)(2,1)S(1)}, u32[]{:S(2)}, u32[]{:S(2)}) collective-permute-start(bf16[4,128,256]{2,1,0:T(8,128)(2,1)S(1)} %get-tuple-element.17), channel_id=1, source_target_pairs={{0,6},{1,25},{2,0},{3,27},{4,2},{5,29},{6,4},{7,31},{8,14},{9,1},{... | collective-permute-start | bytes 786440 | tf_op jit(solution)/shard_map/ppermute | solution.py:29
  137.9 9.8 %collective-permute-start.13 = (bf16[4,128,256]{2,1,0:T(8,128)(2,1)S(1)}, bf16[4,128,256]{2,1,0:T(8,128)(2,1)S(1)}, u32[]{:S(2)}, u32[]{:S(2)}) collective-permute-start(bf16[4,128,256]{2,1,0:T(8,128)(2,1)S(1)} %get-tuple-element.18), channel_id=1, source_target_pairs={{0,4},{1,17},{2,6},{3,19},{4,0},{5,21},{6,2},{7,23},{8,12},{9,25},... | collective-permute-start | bytes 786440 | tf_op jit(solution)/shard_map/ppermute | solution.py:29
  147.8 10.1 %collective-permute-start.15 = (bf16[128,256]{1,0:T(8,128)(2,1)S(1)}, bf16[128,256]{1,0:T(8,128)(2,1)S(1)}, u32[]{:S(2)}, u32[]{:S(2)}) collective-permute-start(bf16[128,256]{1,0:T(8,128)(2,1)S(1)} %get-tuple-element.19), channel_id=1, source_target_pairs={{0,8},{1,3},{2,10},{3,5},{4,12},{5,7},{6,14},{7,1},{8,16},{9,11},{... | collective-permute-start | bytes 196616 | tf_op jit(solution)/shard_map/ppermute | solution.py:29
  150.0 8.0 %collective-permute-start.17 = (bf16[128,256]{1,0:T(8,128)(2,1)S(1)}, bf16[128,256]{1,0:T(8,128)(2,1)S(1)}, u32[]{:S(2)}, u32[]{:S(2)}) collective-permute-start(bf16[128,256]{1,0:T(8,128)(2,1)S(1)} %get-tuple-element.20), channel_id=1, source_target_pairs={{0,24},{1,7},{2,26},{3,1},{4,28},{5,3},{6,30},{7,5},{8,0},{9,15},{... | collective-permute-start | bytes 196616 | tf_op jit(solution)/shard_map/ppermute | solution.py:29
  154.9 7.7 %collective-permute-start.16 = (bf16[128,256]{1,0:T(8,128)(2,1)S(1)}, bf16[128,256]{1,0:T(8,128)(2,1)S(1)}, u32[]{:S(2)}, u32[]{:S(2)}) collective-permute-start(bf16[128,256]{1,0:T(8,128)(2,1)S(1)} %get-tuple-element.21), channel_id=1, source_target_pairs={{0,16},{1,5},{2,18},{3,7},{4,20},{5,1},{6,22},{7,3},{8,24},{9,13},... | collective-permute-start | bytes 196616 | tf_op jit(solution)/shard_map/ppermute | solution.py:29
  (9 other events, 34.2 us)

commit v3 on v2

--- a/solution.py
+++ b/solution.py
@@ -115,40 +115,57 @@
             out[r * NY + i + 2] = high
 
 
-def layer_body(mine, other, chunks, keep, send, pieces, wt, made):
+def weights_into(wt, chunks, r, rows):
+    half = chunks.shape[2] // 2
+    for side in range(NQ):
+        cut = slice(side * half, (side + 1) * half)
+        wt[NQ * r + side] = jnp.concatenate(
+            [chunks[r * NY + y][:rows, cut] for y in range(NY)], axis=1
+        )
+
+
+def near_x(side, r, zq, x_here):
+    return (2 * ((side + zq) % NQ) + r // NC + NX - x_here) % NX
+
+
+def layer_body(refs):
+    mine, other, chunks_far = refs[:4], refs[4:8], refs[8]
+    pieces_far, turned_far = refs[9:11]
+    one, two, chunks, pieces, turned, wt, sems = refs[11:]
     core = lax.axis_index("c")
     x_here = lax.axis_index("x")
     zq = lax.axis_index("zq")
     hid = chunks.shape[1] // 3
     half = chunks.shape[2] // 2
 
+    first = pltpu.make_async_copy(chunks_far, chunks, sems.at[8])
+    first.start()
+    loads = []
+    for i in range(4):
+        loads.append(pltpu.make_async_copy(mine[i], one.at[i], sems.at[i]))
+        loads.append(pltpu.make_async_copy(other[i], two.at[i], sems.at[4 + i]))
+    for c in loads:
+        c.start()
+    first.wait()
     for r in range(NR):
-        for side in range(NQ):
-            cut = slice(side * half, (side + 1) * half)
-            wt[NQ * r + side] = jnp.concatenate(
-                [chunks[r * NY + y][:, cut] for y in range(NY)], axis=1
-            )
-
-    def run(even, odd, me):
-        def block(k, c, which):
-            if c == 0:
-                return jnp.concatenate([even[j][k, which] for j in range(NY)], axis=0)
-            part = odd[k][:, which]
+        weights_into(wt, chunks, r, 3 * hid)
+    for c in loads:
+        c.wait()
+
+    def run(even, odd):
+        def block(side, r, which):
+            k = near_x(side, r, zq, x_here)
+            part = even[:, k, which] if r % NC == 0 else odd[k, :, which]
             return part.reshape(NY * part.shape[1], part.shape[2])
 
-        def place(k, c):
-            x = (x_here + k) % NX
-            return NQ * ((x % 2) * NC + c) + (x // 2 + zq) % NQ
-
-        blocks = [(k, c) for k in range(NX) for c in range(NC)]
         pre = None
         hid_grad = None
-        for k, c in blocks:
-            i = place(k, c)
-            p = dot(wt[i, : 2 * hid, :], block(k, c, 0), NT)
-            q = dot(wt[i, 2 * hid :, :], block(k, c, 1), NT)
-            pre = p if pre is None else pre + p
-            hid_grad = q if hid_grad is None else hid_grad + q
+        for r in range(NR):
+            for side in range(NQ):
+                p = dot(wt[NQ * r + side, : 2 * hid, :], block(side, r, 0), NT)
+                q = dot(wt[NQ * r + side, 2 * hid :, :], block(side, r, 1), NT)
+                pre = p if pre is None else pre + p
+                hid_grad = q if hid_grad is None else hid_grad + q
         gate = pre[:hid]
         up = pre[hid:]
         sig = jax.nn.sigmoid(gate)
@@ -157,34 +174,62 @@
         g_gate = hid_grad * up * sig * (1.0 + gate * (1.0 - sig))
         g_up = hid_grad * act
         g_both = jnp.concatenate([g_gate, g_up], axis=0)
-        g_turned = g_both.T.astype(BF)
+        turned[...] = g_both.T.astype(BF)
         g_both = g_both.astype(BF)
-        for k, c in blocks:
-            i = place(k, c)
-            made[i, : 2 * hid, :] = dot(g_both, block(k, c, 0), NN).astype(BF)
-            made[i, 2 * hid :, :] = dot(hidden, block(k, c, 1), NN).astype(BF)
-            gi = dot(g_turned, wt[i, : 2 * hid, :], NN).astype(BF)
-            rows = gi.shape[0] // NY
-            ref = keep if c == me else send
-            for j in range(NY):
-                piece = gi[j * rows : (j + 1) * rows]
-                if c == 0:
-                    ref[k, j] = piece
-                else:
-                    ref[j, k] = piece
+        stores = [pltpu.make_async_copy(turned, turned_far, sems.at[4])]
+        stores[0].start()
+        for r in range(NR):
+            made = []
+            for side in range(NQ):
+                pw = dot(g_both, block(side, r, 0), NN)
+                pd = dot(hidden, block(side, r, 1), NN)
+                made.append(jnp.concatenate([pw, pd], axis=0).astype(BF))
+            for y in range(NY):
+                s = slice(y * half, (y + 1) * half)
+                pieces[r * NY + y] = sides(made[0][:, s], made[1][:, s])
+            part = pl.ds(r * NY, NY)
+            stores.append(pltpu.make_async_copy(pieces.at[part], pieces_far.at[part], sems.at[r]))
+            stores[-1].start()
+        for c in stores:
+            c.wait()
 
     @pl.when(core == 0)
     def _():
-        run(mine, other, 0)
+        run(one, two)
 
     @pl.when(core == 1)
     def _():
-        run(other, mine, 1)
-
+        run(two, one)
+
+
+def back_body(turned, chunks, keep, send, wt):
+    core = lax.axis_index("c")
+    x_here = lax.axis_index("x")
+    zq = lax.axis_index("zq")
+    rows = turned.shape[0] // NY
     for r in range(NR):
-        for y in range(NY):
-            s = slice(y * half, (y + 1) * half)
-            pieces[r * NY + y] = sides(made[NQ * r, :, s], made[NQ * r + 1, :, s])
+        weights_into(wt, chunks, r, wt.shape[1])
+
+    def run(me):
+        for r in range(NR):
+            for side in range(NQ):
+                k = near_x(side, r, zq, x_here)
+                gi = dot(turned[...], wt[NQ * r + side], NN).astype(BF)
+                ref = keep if r % NC == me else send
+                for j in range(NY):
+                    piece = gi[j * rows : (j + 1) * rows]
+                    if r % NC == 0:
+                        ref[k, j] = piece
+                    else:
+                        ref[j, k] = piece
+
+    @pl.when(core == 0)
+    def _():
+        run(0)
+
+    @pl.when(core == 1)
+    def _():
+        run(1)
 
 
 def sum_body(pieces, out):
@@ -235,7 +280,7 @@
         far_in=3,
     )
     far = lax.ppermute(packed, "zq", [(0, 1), (1, 0)])
-    chunks = call(spread_body, (packed, far), S((NR * NY, 3 * hid, 2 * rows_d), BF))
+    chunks = call(spread_body, (packed, far), S((NR * NY, 3 * hid, 2 * rows_d), BF), 60, far_in=2)
     chunks = lax.all_to_all(chunks, ("zr", "y"), 0, 0, tiled=True)
 
     block = jnp.stack([inputs, cotangent])
@@ -244,26 +289,36 @@
     other = [swapped(m) for m in mine]
 
     tiles = S((4, 4, rows, cols), BF)
-
-    def body(*refs):
-        layer_body(refs[:4], refs[4:8], *refs[8:])
-
-    blocks = pltpu.VMEM((NQ * NR, 3 * hid, NY * rows_d), BF)
-    keep, send, pieces = call(
-        body,
-        (*mine, *other, chunks),
-        [tiles, tiles, S(chunks.shape, BF)],
-        60,
-        far_in=9,
-        far_out=True,
-        own=[blocks, blocks],
-    )
+    turned = S((NY * rows, 2 * hid), BF)
+    joint = (4, *mine[0].shape)
+    made = [S(chunks.shape, BF), turned]
+    far = pl.BlockSpec(memory_space=pltpu.HBM)
+    shapes = (joint, joint, chunks.shape, chunks.shape, turned.shape)
+    shapes += ((NQ * NR, 3 * hid, NY * rows_d),)
+    pieces, turned = pl.pallas_call(
+        lambda *refs: layer_body(refs),
+        in_specs=[far] * 9,
+        out_specs=[far] * 2,
+        out_shape=made,
+        scratch_shapes=[pltpu.VMEM(s, BF) for s in shapes] + [pltpu.SemaphoreType.DMA((9,))],
+        compiler_params=pltpu.CompilerParams(vmem_limit_bytes=60 * 2**20),
+        name="layer",
+    )(*mine, *other, chunks)
 
     pieces = lax.all_to_all(pieces, ("zr", "y"), 0, 0, tiled=True)
     ring = call(sum_body, (pieces,), S((4, 2, 3 * hid, 2 * rows_d), BF))
     ring = lax.all_to_all(ring, ("zh", "zq"), 0, 0, tiled=True)
     g_gate, g_up, g_down = call(last_body, (ring,), [S((rows_d, ff), F32)] * 3)
 
+    keep, send = call(
+        back_body,
+        (turned, chunks),
+        [tiles, tiles],
+        60,
+        far_in=2,
+        far_out=True,
+        own=[pltpu.VMEM((NQ * NR, 2 * hid, NY * rows_d), BF)],
+    )
     theirs = swapped(send)
     chip = (keep.astype(F32) + theirs.astype(F32)).astype(BF)
     part = line_sum(chip, 0)

time: 165 us -> 164 us (level)
  waiting for transfers between devices: 57.2 us -> 53.4 us
  Pallas kernels: 12.3 us -> 15.1 us
    pallas_call x0 -> x1, Pallas kernels: none -> 5.52 us  [per_device(): pl.pallas_call(lambda *refs: layer_body(refs), in_specs=[far] * 9, out_sp...]
    all_to_all x1, waiting for transfers between devices: 24.8 us -> 21.1 us  [per_device(): pieces = lax.all_to_all(pieces, ('zr', 'y'), 0, 0, tiled=True)]
    pallas_call x5, Pallas kernels: 12.3 us -> 9.56 us  [call(): pl.pallas_call(whole, in_specs=[far] * loads + [VM] * (n - loads), out_sp...]
  transfers between devices with their start and end apart: 21 -> 21, of which waited for: 10 -> 10; matrix products, arithmetic and copies ran while one was open for 1% -> 1% of each run, Pallas kernels for 1% -> 3%
where the time goes in v3:
time: 164 us; the launch traced here: 163 us
  starting transfers between devices  88.7 us (54%)
  waiting for transfers between devices  53.4 us (33%)
  Pallas kernels  15.1 us (9%)
  local copies, waits for them, and re-layouts  3.52 us (2%)
    ppermute x12, starting transfers between devices, moved(): return lax.ppermute(value, PLANE, pairs)  41.2 us
    ppermute x12, waiting for transfers between devices, moved(): return lax.ppermute(value, PLANE, pairs)  22.7 us
    all_to_all x1, waiting for transfers between devices, per_device(): pieces = lax.all_to_all(pieces, ('zr', 'y'), 0, 0, tiled=True)  21.1 us
    all_to_all x1, starting transfers between devices, per_device(): ring = lax.all_to_all(ring, ('zh', 'zq'), 0, 0, tiled=True)  11.1 us
    ppermute x5, starting transfers between devices, swapped(): return lax.ppermute(value, 'c', [(0, 1), (1, 0)])  10.3 us
    ppermute x1, waiting for transfers between devices, per_device(): far = lax.ppermute(packed, 'zq', [(0, 1), (1, 0)])  9.67 us
    all_to_all x1, starting transfers between devices, per_device(): chunks = lax.all_to_all(chunks, ('zr', 'y'), 0, 0, tiled=True)  9.59 us
    pallas_call x5, Pallas kernels, call(): pl.pallas_call(whole, in_specs=[far] * loads + [VM] * (n - loads), out_sp...  9.56 us
  transfers between devices with their start and end apart: 21, of which 10 were waited for; matrix products, arithmetic and copies ran while one was open for 1% of the time, Pallas kernels for 3%

profile of v3, /device:TPU:32, one launch (start us, length us, event | category | flops | bytes accessed | tf_op | source)
XLA Modules:
  0.0 163.0 jit_solution(15795373184318468885)
XLA Ops:
  2.4 9.1 %collective-permute-start.10 = (bf16[2,264,128]{2,1,0:T(8,128)(2,1)}, bf16[2,264,128]{2,1,0:T(8,128)(2,1)S(1)}, u32[]{:S(2)}, u32[]{:S(2)}) collective-permute-start(bf16[2,264,128]{2,1,0:T(8,128)(2,1)} %shard_map.84.refs_0_), channel_id=1, source_target_pairs={{0,128},{128,0},{1,129},{129,1},{2,130},{130,2},{3,131},{131,3},{4... | collective-permute-start | bytes 405512 | tf_op jit(solution)/shard_map/ppermute | solution.py:282
  11.5 9.7 %collective-permute-done.10.refs_1_ = bf16[2,264,128]{2,1,0:T(8,128)(2,1)S(1)} collective-permute-done((bf16[2,264,128]{2,1,0:T(8,128)(2,1)}, bf16[2,264,128]{2,1,0:T(8,128)(2,1)S(1)}, u32[]{:S(2)}, u32[]{:S(2)}) %collective-permute-start.10) | collective-permute-done | bytes 135200 | tf_op jit(solution)/shard_map/ppermute | solution.py:282
  24.0 9.6 %all-to-all-start = ((bf16[16,264,128]{2,1,0:T(8,128)(2,1)}), bf16[16,264,128]{2,1,0:T(8,128)(2,1)S(1)}, u32[]{:S(2)}, u32[]{:S(2)}) async-start(bf16[16,264,128]{2,1,0:T(8,128)(2,1)} %shard_map.85), calls=%async_computation | async-start | bytes 2162688 | tf_op jit(solution)/shard_map/all_to_all | solution.py:284
  33.6 4.9 %collective-permute-start.1 = (bf16[2,128,256]{2,1,0:T(8,128)(2,1)S(1)}, bf16[2,128,256]{2,1,0:T(8,128)(2,1)S(1)}, u32[]{:S(2)}, u32[]{:S(2)}) collective-permute-start(bf16[2,128,256]{2,1,0:T(8,128)(2,1)S(1)} %get-tuple-element.25), channel_id=1, source_target_pairs={{0,4},{1,17},{2,6},{3,19},{4,0},{5,21},{6,2},{7,23},{8,12},{9,25},... | collective-permute-start | bytes 393224 | tf_op jit(solution)/shard_map/ppermute | solution.py:29
  38.6 3.0 %collective-permute-start = (bf16[2,128,256]{2,1,0:T(8,128)(2,1)S(1)}, bf16[2,128,256]{2,1,0:T(8,128)(2,1)S(1)}, u32[]{:S(2)}, u32[]{:S(2)}) collective-permute-start(bf16[2,128,256]{2,1,0:T(8,128)(2,1)S(1)} %get-tuple-element.25), channel_id=1, source_target_pairs={{0,6},{1,25},{2,0},{3,27},{4,2},{5,29},{6,4},{7,31},{8,14},{9,1},{... | collective-permute-start | bytes 393224 | tf_op jit(solution)/shard_map/ppermute | solution.py:29
  41.6 2.8 %collective-permute-start.2 = (bf16[2,128,256]{2,1,0:T(8,128)(2,1)S(1)}, bf16[2,128,256]{2,1,0:T(8,128)(2,1)S(1)}, u32[]{:S(2)}, u32[]{:S(2)}) collective-permute-start(bf16[2,128,256]{2,1,0:T(8,128)(2,1)S(1)} %get-tuple-element.25), channel_id=1, source_target_pairs={{0,2},{1,9},{2,4},{3,11},{4,6},{5,13},{6,0},{7,15},{8,10},{9,17},{... | collective-permute-start | bytes 393224 | tf_op jit(solution)/shard_map/ppermute | solution.py:29
  45.4 4.3 %collective-permute-done.2 = bf16[2,128,256]{2,1,0:T(8,128)(2,1)S(1)} collective-permute-done((bf16[2,128,256]{2,1,0:T(8,128)(2,1)S(1)}, bf16[2,128,256]{2,1,0:T(8,128)(2,1)S(1)}, u32[]{:S(2)}, u32[]{:S(2)}) %collective-permute-start.2) | collective-permute-done | bytes 131104 | tf_op jit(solution)/shard_map/ppermute | solution.py:29
  49.8 3.4 %collective-permute-start.5 = (bf16[4,2,128,256]{3,2,1,0:T(8,128)(2,1)S(1)}, bf16[4,2,128,256]{3,2,1,0:T(8,128)(2,1)S(1)}, u32[]{:S(2)}, u32[]{:S(2)}) collective-permute-start(bf16[4,2,128,256]{3,2,1,0:T(8,128)(2,1)S(1)} %pad_maximum_fusion.refs_0_), channel_id=1, source_target_pairs={{0,8},{1,3},{2,10},{3,5},{4,12},{5,7},{6,14},{7,1},{8,16},{9,11},{... | collective-permute-start | bytes 1572872 | tf_op jit(solution)/shard_map/ppermute | solution.py:29
  53.2 4.6 %collective-permute-start.4 = (bf16[4,2,128,256]{3,2,1,0:T(8,128)(2,1)S(1)}, bf16[4,2,128,256]{3,2,1,0:T(8,128)(2,1)S(1)}, u32[]{:S(2)}, u32[]{:S(2)}) collective-permute-start(bf16[4,2,128,256]{3,2,1,0:T(8,128)(2,1)S(1)} %pad_maximum_fusion.refs_0_), channel_id=1, source_target_pairs={{0,16},{1,5},{2,18},{3,7},{4,20},{5,1},{6,22},{7,3},{8,24},{9,13},... | collective-permute-start | bytes 1572872 | tf_op jit(solution)/shard_map/ppermute | solution.py:29
  57.8 3.4 %collective-permute-start.3 = (bf16[4,2,128,256]{3,2,1,0:T(8,128)(2,1)S(1)}, bf16[4,2,128,256]{3,2,1,0:T(8,128)(2,1)S(1)}, u32[]{:S(2)}, u32[]{:S(2)}) collective-permute-start(bf16[4,2,128,256]{3,2,1,0:T(8,128)(2,1)S(1)} %pad_maximum_fusion.refs_0_), channel_id=1, source_target_pairs={{0,24},{1,7},{2,26},{3,1},{4,28},{5,3},{6,30},{7,5},{8,0},{9,15},{... | collective-permute-start | bytes 1572872 | tf_op jit(solution)/shard_map/ppermute | solution.py:29
  65.5 4.5 %collective-permute-done.4.refs_2_ = bf16[4,2,128,256]{3,2,1,0:T(8,128)(2,1)S(1)} collective-permute-done((bf16[4,2,128,256]{3,2,1,0:T(8,128)(2,1)S(1)}, bf16[4,2,128,256]{3,2,1,0:T(8,128)(2,1)S(1)}, u32[]{:S(2)}, u32[]{:S(2)}) %collective-permute-start.4) | collective-permute-done | bytes 524320 | tf_op jit(solution)/shard_map/ppermute | solution.py:29
  72.0 2.4 %collective-permute-start.7 = (bf16[4,2,128,256]{3,2,1,0:T(8,128)(2,1)S(1)}, bf16[4,2,128,256]{3,2,1,0:T(8,128)(2,1)}, u32[]{:S(2)}, u32[]{:S(2)}) collective-permute-start(bf16[4,2,128,256]{3,2,1,0:T(8,128)(2,1)S(1)} %collective-permute-done.3.refs_1_), channel_id=1, source_target_pairs={{0,1},{1,0},{2,3},{3,2},{4,5},{5,4},{6,7},{7,6},{8,9},{9,8},{10,11... | collective-permute-start | bytes 1572872 | tf_op jit(solution)/shard_map/ppermute | solution.py:19
  77.2 5.5 %layer.1 = (bf16[16,264,128]{2,1,0:T(8,128)(2,1)}, bf16[512,176]{1,0:T(8,128)(2,1)}) custom-call(bf16[4,2,128,256]{3,2,1,0:T(8,128)(2,1)} %copy-done.1, bf16[4,2,128,256]{3,2,1,0:T(8,128)(2,1)} %copy-done.5, bf16[4,2,128,256]{3,2,1,0:T(8,128)(2,1)} %copy-done.4, bf16[4,2,128,256]{3,2,1,0:T(8,128)(2,1)} %copy-done.3, bf16[4,2,128,256]{3,2,1,0:T(8,128)(2,1)} %copy-done.6, ...), custom_call_target="tpu_custom_call" | custom-call | tf_op jit(solution)/shard_map/layer/pallas_call | solution.py:298
  82.8 7.5 %all-to-all-start.1 = ((bf16[16,264,128]{2,1,0:T(8,128)(2,1)}), bf16[16,264,128]{2,1,0:T(8,128)(2,1)S(1)}, u32[]{:S(2)}, u32[]{:S(2)}) async-start(bf16[16,264,128]{2,1,0:T(8,128)(2,1)} %get-tuple-element.14), calls=%async_computation.1 | async-start | bytes 2162688 | tf_op jit(solution)/shard_map/all_to_all | solution.py:308
  90.3 3.7 %shard_map.86 = (bf16[4,4,128,256]{3,2,1,0:T(8,128)(2,1)}, bf16[4,4,128,256]{3,2,1,0:T(8,128)(2,1)}) custom-call(bf16[512,176]{1,0:T(8,128)(2,1)} %get-tuple-element.11.refs_0_, bf16[16,264,128]{2,1,0:T(8,128)(2,1)} %copy-done), custom_call_target="tpu_custom_call" | custom-call | tf_op jit(solution)/shard_map/pallas_call | solution.py:79
  96.1 21.1 %all-to-all-done.1.refs_0_ = bf16[16,264,128]{2,1,0:T(8,128)(2,1)S(1)} async-done(((bf16[16,264,128]{2,1,0:T(8,128)(2,1)}), bf16[16,264,128]{2,1,0:T(8,128)(2,1)S(1)}, u32[]{:S(2)}, u32[]{:S(2)}) %all-to-all-start.1) | async-done | bytes 1081376 | tf_op jit(solution)/shard_map/all_to_all | solution.py:308
  118.1 11.1 %all-to-all-start.2 = ((bf16[4,2,264,128]{3,2,1,0:T(8,128)(2,1)}), bf16[4,2,264,128]{3,2,1,0:T(8,128)(2,1)S(1)}, u32[]{:S(2)}, u32[]{:S(2)}) async-start(bf16[4,2,264,128]{3,2,1,0:T(8,128)(2,1)} %shard_map.87), calls=%async_computation.2 | async-start | bytes 1081344 | tf_op jit(solution)/shard_map/all_to_all | solution.py:310
  131.7 5.0 %collective-permute-start.14 = (bf16[4,128,256]{2,1,0:T(8,128)(2,1)S(1)}, bf16[4,128,256]{2,1,0:T(8,128)(2,1)S(1)}, u32[]{:S(2)}, u32[]{:S(2)}) collective-permute-start(bf16[4,128,256]{2,1,0:T(8,128)(2,1)S(1)} %get-tuple-element.19), channel_id=1, source_target_pairs={{0,6},{1,25},{2,0},{3,27},{4,2},{5,29},{6,4},{7,31},{8,14},{9,1},{... | collective-permute-start | bytes 786440 | tf_op jit(solution)/shard_map/ppermute | solution.py:29
  139.1 4.3 %collective-permute-done.14 = bf16[4,128,256]{2,1,0:T(8,128)(2,1)S(1)} collective-permute-done((bf16[4,128,256]{2,1,0:T(8,128)(2,1)S(1)}, bf16[4,128,256]{2,1,0:T(8,128)(2,1)S(1)}, u32[]{:S(2)}, u32[]{:S(2)}) %collective-permute-start.14) | collective-permute-done | bytes 262176 | tf_op jit(solution)/shard_map/ppermute | solution.py:29
  143.4 3.1 %collective-permute-done.13 = bf16[4,128,256]{2,1,0:T(8,128)(2,1)S(1)} collective-permute-done((bf16[4,128,256]{2,1,0:T(8,128)(2,1)S(1)}, bf16[4,128,256]{2,1,0:T(8,128)(2,1)S(1)}, u32[]{:S(2)}, u32[]{:S(2)}) %collective-permute-start.13) | collective-permute-done | bytes 262176 | tf_op jit(solution)/shard_map/ppermute | solution.py:29
  146.6 2.2 %collective-permute-start.15 = (bf16[128,256]{1,0:T(8,128)(2,1)S(1)}, bf16[128,256]{1,0:T(8,128)(2,1)S(1)}, u32[]{:S(2)}, u32[]{:S(2)}) collective-permute-start(bf16[128,256]{1,0:T(8,128)(2,1)S(1)} %get-tuple-element.21), channel_id=1, source_target_pairs={{0,8},{1,3},{2,10},{3,5},{4,12},{5,7},{6,14},{7,1},{8,16},{9,11},{... | collective-permute-start | bytes 196616 | tf_op jit(solution)/shard_map/ppermute | solution.py:29
  148.8 4.9 %collective-permute-start.17 = (bf16[128,256]{1,0:T(8,128)(2,1)S(1)}, bf16[128,256]{1,0:T(8,128)(2,1)S(1)}, u32[]{:S(2)}, u32[]{:S(2)}) collective-permute-start(bf16[128,256]{1,0:T(8,128)(2,1)S(1)} %get-tuple-element.22), channel_id=1, source_target_pairs={{0,24},{1,7},{2,26},{3,1},{4,28},{5,3},{6,30},{7,5},{8,0},{9,15},{... | collective-permute-start | bytes 196616 | tf_op jit(solution)/shard_map/ppermute | solution.py:29
  153.7 3.1 %collective-permute-start.16 = (bf16[128,256]{1,0:T(8,128)(2,1)S(1)}, bf16[128,256]{1,0:T(8,128)(2,1)S(1)}, u32[]{:S(2)}, u32[]{:S(2)}) collective-permute-start(bf16[128,256]{1,0:T(8,128)(2,1)S(1)} %get-tuple-element.23), channel_id=1, source_target_pairs={{0,16},{1,5},{2,18},{3,7},{4,20},{5,1},{6,22},{7,3},{8,24},{9,13},... | collective-permute-start | bytes 196616 | tf_op jit(solution)/shard_map/ppermute | solution.py:29
  156.8 4.6 %collective-permute-done.16 = bf16[128,256]{1,0:T(8,128)(2,1)S(1)} collective-permute-done((bf16[128,256]{1,0:T(8,128)(2,1)S(1)}, bf16[128,256]{1,0:T(8,128)(2,1)S(1)}, u32[]{:S(2)}, u32[]{:S(2)}) %collective-permute-start.16) | collective-permute-done | bytes 65568 | tf_op jit(solution)/shard_map/ppermute | solution.py:29
  (55 shorter events, 24.3 us)
Async XLA Ops:
  2.4 18.8 %collective-permute-start.10 = (bf16[2,264,128]{2,1,0:T(8,128)(2,1)}, bf16[2,264,128]{2,1,0:T(8,128)(2,1)S(1)}, u32[]{:S(2)}, u32[]{:S(2)}) collective-permute-start(bf16[2,264,128]{2,1,0:T(8,128)(2,1)} %shard_map.84.refs_0_), channel_id=1, source_target_pairs={{0,128},{128,0},{1,129},{129,1},{2,130},{130,2},{3,131},{131,3},{4... | collective-permute-start | bytes 405512 | tf_op jit(solution)/shard_map/ppermute | solution.py:282
  24.0 52.2 %all-to-all-start = ((bf16[16,264,128]{2,1,0:T(8,128)(2,1)}), bf16[16,264,128]{2,1,0:T(8,128)(2,1)S(1)}, u32[]{:S(2)}, u32[]{:S(2)}) async-start(bf16[16,264,128]{2,1,0:T(8,128)(2,1)} %shard_map.85), calls=%async_computation | async-start | bytes 2162688 | tf_op jit(solution)/shard_map/all_to_all | solution.py:284
  33.6 10.8 %collective-permute-start.1 = (bf16[2,128,256]{2,1,0:T(8,128)(2,1)S(1)}, bf16[2,128,256]{2,1,0:T(8,128)(2,1)S(1)}, u32[]{:S(2)}, u32[]{:S(2)}) collective-permute-start(bf16[2,128,256]{2,1,0:T(8,128)(2,1)S(1)} %get-tuple-element.25), channel_id=1, source_target_pairs={{0,4},{1,17},{2,6},{3,19},{4,0},{5,21},{6,2},{7,23},{8,12},{9,25},... | collective-permute-start | bytes 393224 | tf_op jit(solution)/shard_map/ppermute | solution.py:29
  38.6 6.9 %collective-permute-start = (bf16[2,128,256]{2,1,0:T(8,128)(2,1)S(1)}, bf16[2,128,256]{2,1,0:T(8,128)(2,1)S(1)}, u32[]{:S(2)}, u32[]{:S(2)}) collective-permute-start(bf16[2,128,256]{2,1,0:T(8,128)(2,1)S(1)} %get-tuple-element.25), channel_id=1, source_target_pairs={{0,6},{1,25},{2,0},{3,27},{4,2},{5,29},{6,4},{7,31},{8,14},{9,1},{... | collective-permute-start | bytes 393224 | tf_op jit(solution)/shard_map/ppermute | solution.py:29
  41.6 8.1 %collective-permute-start.2 = (bf16[2,128,256]{2,1,0:T(8,128)(2,1)S(1)}, bf16[2,128,256]{2,1,0:T(8,128)(2,1)S(1)}, u32[]{:S(2)}, u32[]{:S(2)}) collective-permute-start(bf16[2,128,256]{2,1,0:T(8,128)(2,1)S(1)} %get-tuple-element.25), channel_id=1, source_target_pairs={{0,2},{1,9},{2,4},{3,11},{4,6},{5,13},{6,0},{7,15},{8,10},{9,17},{... | collective-permute-start | bytes 393224 | tf_op jit(solution)/shard_map/ppermute | solution.py:29
  49.8 26.4 %copy-start.1 = (bf16[4,2,128,256]{3,2,1,0:T(8,128)(2,1)}, bf16[4,2,128,256]{3,2,1,0:T(8,128)(2,1)S(1)}, u32[]{:S(2)}) copy-start(bf16[4,2,128,256]{3,2,1,0:T(8,128)(2,1)S(1)} %pad_maximum_fusion.refs_0_) | copy-start | bytes 1572868
  49.8 13.7 %collective-permute-start.5 = (bf16[4,2,128,256]{3,2,1,0:T(8,128)(2,1)S(1)}, bf16[4,2,128,256]{3,2,1,0:T(8,128)(2,1)S(1)}, u32[]{:S(2)}, u32[]{:S(2)}) collective-permute-start(bf16[4,2,128,256]{3,2,1,0:T(8,128)(2,1)S(1)} %pad_maximum_fusion.refs_0_), channel_id=1, source_target_pairs={{0,8},{1,3},{2,10},{3,5},{4,12},{5,7},{6,14},{7,1},{8,16},{9,11},{... | collective-permute-start | bytes 1572872 | tf_op jit(solution)/shard_map/ppermute | solution.py:29
  53.2 16.9 %collective-permute-start.4 = (bf16[4,2,128,256]{3,2,1,0:T(8,128)(2,1)S(1)}, bf16[4,2,128,256]{3,2,1,0:T(8,128)(2,1)S(1)}, u32[]{:S(2)}, u32[]{:S(2)}) collective-permute-start(bf16[4,2,128,256]{3,2,1,0:T(8,128)(2,1)S(1)} %pad_maximum_fusion.refs_0_), channel_id=1, source_target_pairs={{0,16},{1,5},{2,18},{3,7},{4,20},{5,1},{6,22},{7,3},{8,24},{9,13},... | collective-permute-start | bytes 1572872 | tf_op jit(solution)/shard_map/ppermute | solution.py:29
  57.8 14.2 %collective-permute-start.3 = (bf16[4,2,128,256]{3,2,1,0:T(8,128)(2,1)S(1)}, bf16[4,2,128,256]{3,2,1,0:T(8,128)(2,1)S(1)}, u32[]{:S(2)}, u32[]{:S(2)}) collective-permute-start(bf16[4,2,128,256]{3,2,1,0:T(8,128)(2,1)S(1)} %pad_maximum_fusion.refs_0_), channel_id=1, source_target_pairs={{0,24},{1,7},{2,26},{3,1},{4,28},{5,3},{6,30},{7,5},{8,0},{9,15},{... | collective-permute-start | bytes 1572872 | tf_op jit(solution)/shard_map/ppermute | solution.py:29
  61.1 13.3 %collective-permute-start.6 = (bf16[4,2,128,256]{3,2,1,0:T(8,128)(2,1)S(1)}, bf16[4,2,128,256]{3,2,1,0:T(8,128)(2,1)S(1)}, u32[]{:S(2)}, u32[]{:S(2)}) collective-permute-start(bf16[4,2,128,256]{3,2,1,0:T(8,128)(2,1)S(1)} %pad_maximum_fusion.refs_0_), channel_id=1, source_target_pairs={{0,1},{1,0},{2,3},{3,2},{4,5},{5,4},{6,7},{7,6},{8,9},{9,8},{10,11... | collective-permute-start | bytes 1572872 | tf_op jit(solution)/shard_map/ppermute | solution.py:19
  63.5 12.7 %copy-start.3 = (bf16[4,2,128,256]{3,2,1,0:T(8,128)(2,1)}, bf16[4,2,128,256]{3,2,1,0:T(8,128)(2,1)S(1)}, u32[]{:S(2)}) copy-start(bf16[4,2,128,256]{3,2,1,0:T(8,128)(2,1)S(1)} %collective-permute-done.5.refs_3_) | copy-start | bytes 1572868
  63.5 10.9 %collective-permute-start.9 = (bf16[4,2,128,256]{3,2,1,0:T(8,128)(2,1)S(1)}, bf16[4,2,128,256]{3,2,1,0:T(8,128)(2,1)S(1)}, u32[]{:S(2)}, u32[]{:S(2)}) collective-permute-start(bf16[4,2,128,256]{3,2,1,0:T(8,128)(2,1)S(1)} %collective-permute-done.5.refs_3_), channel_id=1, source_target_pairs={{0,1},{1,0},{2,3},{3,2},{4,5},{5,4},{6,7},{7,6},{8,9},{9,8},{10,11... | collective-permute-start | bytes 1572872 | tf_op jit(solution)/shard_map/ppermute | solution.py:19
  70.0 4.4 %collective-permute-start.8 = (bf16[4,2,128,256]{3,2,1,0:T(8,128)(2,1)S(1)}, bf16[4,2,128,256]{3,2,1,0:T(8,128)(2,1)S(1)}, u32[]{:S(2)}, u32[]{:S(2)}) collective-permute-start(bf16[4,2,128,256]{3,2,1,0:T(8,128)(2,1)S(1)} %collective-permute-done.4.refs_2_), channel_id=1, source_target_pairs={{0,1},{1,0},{2,3},{3,2},{4,5},{5,4},{6,7},{7,6},{8,9},{9,8},{10,11... | collective-permute-start | bytes 1572872 | tf_op jit(solution)/shard_map/ppermute | solution.py:19
  72.0 4.2 %collective-permute-start.7 = (bf16[4,2,128,256]{3,2,1,0:T(8,128)(2,1)S(1)}, bf16[4,2,128,256]{3,2,1,0:T(8,128)(2,1)}, u32[]{:S(2)}, u32[]{:S(2)}) collective-permute-start(bf16[4,2,128,256]{3,2,1,0:T(8,128)(2,1)S(1)} %collective-permute-done.3.refs_1_), channel_id=1, source_target_pairs={{0,1},{1,0},{2,3},{3,2},{4,5},{5,4},{6,7},{7,6},{8,9},{9,8},{10,11... | collective-permute-start | bytes 1572872 | tf_op jit(solution)/shard_map/ppermute | solution.py:19
  82.8 34.4 %all-to-all-start.1 = ((bf16[16,264,128]{2,1,0:T(8,128)(2,1)}), bf16[16,264,128]{2,1,0:T(8,128)(2,1)S(1)}, u32[]{:S(2)}, u32[]{:S(2)}) async-start(bf16[16,264,128]{2,1,0:T(8,128)(2,1)} %get-tuple-element.14), calls=%async_computation.1 | async-start | bytes 2162688 | tf_op jit(solution)/shard_map/all_to_all | solution.py:308
  94.0 35.2 %copy-start.2 = (bf16[4,4,128,256]{3,2,1,0:T(8,128)(2,1)S(1)}, bf16[4,4,128,256]{3,2,1,0:T(8,128)(2,1)}, u32[]{:S(2)}) copy-start(bf16[4,4,128,256]{3,2,1,0:T(8,128)(2,1)} %get-tuple-element.12) | copy-start | bytes 3145732
  94.0 35.2 %collective-permute-start.11 = (bf16[4,4,128,256]{3,2,1,0:T(8,128)(2,1)}, bf16[4,4,128,256]{3,2,1,0:T(8,128)(2,1)S(1)}, u32[]{:S(2)}, u32[]{:S(2)}) collective-permute-start(bf16[4,4,128,256]{3,2,1,0:T(8,128)(2,1)} %get-tuple-element.13), channel_id=1, source_target_pairs={{0,1},{1,0},{2,3},{3,2},{4,5},{5,4},{6,7},{7,6},{8,9},{9,8},{10,11... | collective-permute-start | bytes 3145736 | tf_op jit(solution)/shard_map/ppermute | solution.py:19
  118.1 43.9 %all-to-all-start.2 = ((bf16[4,2,264,128]{3,2,1,0:T(8,128)(2,1)}), bf16[4,2,264,128]{3,2,1,0:T(8,128)(2,1)S(1)}, u32[]{:S(2)}, u32[]{:S(2)}) async-start(bf16[4,2,264,128]{3,2,1,0:T(8,128)(2,1)} %shard_map.87), calls=%async_computation.2 | async-start | bytes 1081344 | tf_op jit(solution)/shard_map/all_to_all | solution.py:310
  129.6 9.5 %collective-permute-start.12 = (bf16[4,128,256]{2,1,0:T(8,128)(2,1)S(1)}, bf16[4,128,256]{2,1,0:T(8,128)(2,1)S(1)}, u32[]{:S(2)}, u32[]{:S(2)}) collective-permute-start(bf16[4,128,256]{2,1,0:T(8,128)(2,1)S(1)} %get-tuple-element.18), channel_id=1, source_target_pairs={{0,2},{1,9},{2,4},{3,11},{4,6},{5,13},{6,0},{7,15},{8,10},{9,17},{... | collective-permute-start | bytes 786440 | tf_op jit(solution)/shard_map/ppermute | solution.py:29
  131.7 11.8 %collective-permute-start.14 = (bf16[4,128,256]{2,1,0:T(8,128)(2,1)S(1)}, bf16[4,128,256]{2,1,0:T(8,128)(2,1)S(1)}, u32[]{:S(2)}, u32[]{:S(2)}) collective-permute-start(bf16[4,128,256]{2,1,0:T(8,128)(2,1)S(1)} %get-tuple-element.19), channel_id=1, source_target_pairs={{0,6},{1,25},{2,0},{3,27},{4,2},{5,29},{6,4},{7,31},{8,14},{9,1},{... | collective-permute-start | bytes 786440 | tf_op jit(solution)/shard_map/ppermute | solution.py:29
  136.7 9.8 %collective-permute-start.13 = (bf16[4,128,256]{2,1,0:T(8,128)(2,1)S(1)}, bf16[4,128,256]{2,1,0:T(8,128)(2,1)S(1)}, u32[]{:S(2)}, u32[]{:S(2)}) collective-permute-start(bf16[4,128,256]{2,1,0:T(8,128)(2,1)S(1)} %get-tuple-element.20), channel_id=1, source_target_pairs={{0,4},{1,17},{2,6},{3,19},{4,0},{5,21},{6,2},{7,23},{8,12},{9,25},... | collective-permute-start | bytes 786440 | tf_op jit(solution)/shard_map/ppermute | solution.py:29
  146.6 10.1 %collective-permute-start.15 = (bf16[128,256]{1,0:T(8,128)(2,1)S(1)}, bf16[128,256]{1,0:T(8,128)(2,1)S(1)}, u32[]{:S(2)}, u32[]{:S(2)}) collective-permute-start(bf16[128,256]{1,0:T(8,128)(2,1)S(1)} %get-tuple-element.21), channel_id=1, source_target_pairs={{0,8},{1,3},{2,10},{3,5},{4,12},{5,7},{6,14},{7,1},{8,16},{9,11},{... | collective-permute-start | bytes 196616 | tf_op jit(solution)/shard_map/ppermute | solution.py:29
  148.8 8.0 %collective-permute-start.17 = (bf16[128,256]{1,0:T(8,128)(2,1)S(1)}, bf16[128,256]{1,0:T(8,128)(2,1)S(1)}, u32[]{:S(2)}, u32[]{:S(2)}) collective-permute-start(bf16[128,256]{1,0:T(8,128)(2,1)S(1)} %get-tuple-element.22), channel_id=1, source_target_pairs={{0,24},{1,7},{2,26},{3,1},{4,28},{5,3},{6,30},{7,5},{8,0},{9,15},{... | collective-permute-start | bytes 196616 | tf_op jit(solution)/shard_map/ppermute | solution.py:29
  153.7 7.7 %collective-permute-start.16 = (bf16[128,256]{1,0:T(8,128)(2,1)S(1)}, bf16[128,256]{1,0:T(8,128)(2,1)S(1)}, u32[]{:S(2)}, u32[]{:S(2)}) collective-permute-start(bf16[128,256]{1,0:T(8,128)(2,1)S(1)} %get-tuple-element.23), channel_id=1, source_target_pairs={{0,16},{1,5},{2,18},{3,7},{4,20},{5,1},{6,22},{7,3},{8,24},{9,13},... | collective-permute-start | bytes 196616 | tf_op jit(solution)/shard_map/ppermute | solution.py:29
  (9 other events, 33.9 us)

commit v4 on v3

--- a/solution.py
+++ b/solution.py
@@ -19,24 +19,29 @@
     return lax.ppermute(value, "c", [(0, 1), (1, 0)])
 
 
-def moved(value, k, x_core):
+def moved(value, mask, x_core):
     pairs = []
     for y in range(NY):
         for x in range(NX):
             for c in range(NC):
-                ty, tx = (y, (x + k) % NX) if c == x_core else ((y + k) % NY, x)
+                ty, tx = (y, x ^ mask) if c == x_core else (y ^ mask, x)
                 pairs.append(((y * NX + x) * NC + c, (ty * NX + tx) * NC + c))
     return lax.ppermute(value, PLANE, pairs)
 
 
+def line_double(value, x_core):
+    two = jnp.stack([value, moved(value, 1, x_core)])
+    return jnp.concatenate([two, moved(two, 2, x_core)], axis=0)
+
+
 def line_gather(value, x_core):
-    return [value] + [moved(value, -k, x_core) for k in (1, 2, 3)]
+    return [value] + [moved(value, m, x_core) for m in (1, 2, 3)]
 
 
 def line_sum(value, x_core):
     total = value[0].astype(F32)
-    for k in (1, 2, 3):
-        total = total + moved(value[k], k, x_core).astype(F32)
+    for m in (1, 2, 3):
+        total = total + moved(value[m], m, x_core).astype(F32)
     return total.astype(BF)
 
 
@@ -125,7 +130,7 @@
 
 
 def near_x(side, r, zq, x_here):
-    return (2 * ((side + zq) % NQ) + r // NC + NX - x_here) % NX
+    return (2 * ((side + zq) % NQ) + r // NC) ^ x_here
 
 
 def layer_body(refs):
@@ -280,11 +285,11 @@
         far_in=3,
     )
     far = lax.ppermute(packed, "zq", [(0, 1), (1, 0)])
-    chunks = call(spread_body, (packed, far), S((NR * NY, 3 * hid, 2 * rows_d), BF), 60, far_in=2)
+    chunks = call(spread_body, (packed, far), S((NR * NY, 3 * hid, 2 * rows_d), BF))
     chunks = lax.all_to_all(chunks, ("zr", "y"), 0, 0, tiled=True)
 
     block = jnp.stack([inputs, cotangent])
-    line = jnp.stack(line_gather(block, 0))
+    line = line_double(block, 0)
     mine = line_gather(line, 1)
     other = [swapped(m) for m in mine]
 

time: 164 us -> 166 us (1.012)
  starting transfers between devices: 88.7 us -> 91.1 us
    ppermute x5, starting transfers between devices: 10.3 us -> 15.3 us  [swapped(): return lax.ppermute(value, 'c', [(0, 1), (1, 0)])]
    ppermute x12 -> x11, starting transfers between devices: 41.2 us -> 37.9 us  [moved(): return lax.ppermute(value, PLANE, pairs)]
    ppermute x12 -> x11, waiting for transfers between devices: 22.7 us -> 23.2 us  [moved(): return lax.ppermute(value, PLANE, pairs)]
  transfers between devices with their start and end apart: 21 -> 20, of which waited for: 10 -> 8; matrix products, arithmetic and copies ran while one was open for 1% -> 1% of each run, Pallas kernels for 3% -> 3%
where the time goes in v4:
time: 166 us; the launch traced here: 165 us
  starting transfers between devices  91.1 us (55%)
  waiting for transfers between devices  53.9 us (32%)
  Pallas kernels  14.1 us (8%)
  local copies, waits for them, and re-layouts  3.75 us (2%)
    ppermute x11, starting transfers between devices, moved(): return lax.ppermute(value, PLANE, pairs)  37.9 us
    ppermute x11, waiting for transfers between devices, moved(): return lax.ppermute(value, PLANE, pairs)  23.2 us
    all_to_all x1, waiting for transfers between devices, per_device(): pieces = lax.all_to_all(pieces, ('zr', 'y'), 0, 0, tiled=True)  21 us
    ppermute x5, starting transfers between devices, swapped(): return lax.ppermute(value, 'c', [(0, 1), (1, 0)])  15.3 us
    all_to_all x1, starting transfers between devices, per_device(): ring = lax.all_to_all(ring, ('zh', 'zq'), 0, 0, tiled=True)  11.4 us
    ppermute x1, waiting for transfers between devices, per_device(): far = lax.ppermute(packed, 'zq', [(0, 1), (1, 0)])  9.67 us
    all_to_all x1, starting transfers between devices, per_device(): chunks = lax.all_to_all(chunks, ('zr', 'y'), 0, 0, tiled=True)  9.57 us
    ppermute x1, starting transfers between devices, per_device(): far = lax.ppermute(packed, 'zq', [(0, 1), (1, 0)])  9.1 us
  transfers between devices with their start and end apart: 20, of which 8 were waited for; matrix products, arithmetic and copies ran while one was open for 1% of the time, Pallas kernels for 3%

profile of v4, /device:TPU:32, one launch (start us, length us, event | category | flops | bytes accessed | tf_op | source)
XLA Modules:
  0.0 165.0 jit_solution(12148650387149033619)
XLA Ops:
  2.4 9.1 %collective-permute-start.9 = (bf16[2,264,128]{2,1,0:T(8,128)(2,1)}, bf16[2,264,128]{2,1,0:T(8,128)(2,1)S(1)}, u32[]{:S(2)}, u32[]{:S(2)}) collective-permute-start(bf16[2,264,128]{2,1,0:T(8,128)(2,1)} %shard_map.84.refs_0_), channel_id=1, source_target_pairs={{0,128},{128,0},{1,129},{129,1},{2,130},{130,2},{3,131},{131,3},{4... | collective-permute-start | bytes 405512 | tf_op jit(solution)/shard_map/ppermute | solution.py:287
  11.5 9.7 %collective-permute-done.9.refs_1_ = bf16[2,264,128]{2,1,0:T(8,128)(2,1)S(1)} collective-permute-done((bf16[2,264,128]{2,1,0:T(8,128)(2,1)}, bf16[2,264,128]{2,1,0:T(8,128)(2,1)S(1)}, u32[]{:S(2)}, u32[]{:S(2)}) %collective-permute-start.9) | collective-permute-done | bytes 135200 | tf_op jit(solution)/shard_map/ppermute | solution.py:287
  23.2 9.6 %all-to-all-start = ((bf16[16,264,128]{2,1,0:T(8,128)(2,1)}), bf16[16,264,128]{2,1,0:T(8,128)(2,1)S(1)}, u32[]{:S(2)}, u32[]{:S(2)}) async-start(bf16[16,264,128]{2,1,0:T(8,128)(2,1)} %shard_map.85), calls=%async_computation | async-start | bytes 2162688 | tf_op jit(solution)/shard_map/all_to_all | solution.py:289
  32.9 3.4 %collective-permute-start = (bf16[2,128,256]{2,1,0:T(8,128)(2,1)S(1)}, bf16[2,128,256]{2,1,0:T(8,128)(2,1)S(1)}, u32[]{:S(2)}, u32[]{:S(2)}) collective-permute-start(bf16[2,128,256]{2,1,0:T(8,128)(2,1)S(1)} %get-tuple-element.25), channel_id=1, source_target_pairs={{0,2},{1,9},{2,0},{3,11},{4,6},{5,13},{6,4},{7,15},{8,10},{9,1},{1... | collective-permute-start | bytes 393224 | tf_op jit(solution)/shard_map/ppermute | solution.py:29
  36.3 3.5 %collective-permute-done = bf16[2,128,256]{2,1,0:T(8,128)(2,1)S(1)} collective-permute-done((bf16[2,128,256]{2,1,0:T(8,128)(2,1)S(1)}, bf16[2,128,256]{2,1,0:T(8,128)(2,1)S(1)}, u32[]{:S(2)}, u32[]{:S(2)}) %collective-permute-start) | collective-permute-done | bytes 131104 | tf_op jit(solution)/shard_map/ppermute | solution.py:29
  39.7 4.9 %collective-permute-start.1 = (bf16[2,2,128,256]{3,2,1,0:T(8,128)(2,1)S(1)}, bf16[2,2,128,256]{3,2,1,0:T(8,128)(2,1)S(1)}, u32[]{:S(2)}, u32[]{:S(2)}) collective-permute-start(bf16[2,2,128,256]{3,2,1,0:T(8,128)(2,1)S(1)} %pad_maximum_fusion.1), channel_id=1, source_target_pairs={{0,4},{1,17},{2,6},{3,19},{4,0},{5,21},{6,2},{7,23},{8,12},{9,25},... | collective-permute-start | bytes 786440 | tf_op jit(solution)/shard_map/ppermute | solution.py:29
  44.7 4.8 %collective-permute-done.1 = bf16[2,2,128,256]{3,2,1,0:T(8,128)(2,1)S(1)} collective-permute-done((bf16[2,2,128,256]{3,2,1,0:T(8,128)(2,1)S(1)}, bf16[2,2,128,256]{3,2,1,0:T(8,128)(2,1)S(1)}, u32[]{:S(2)}, u32[]{:S(2)}) %collective-permute-start.1) | collective-permute-done | bytes 262176 | tf_op jit(solution)/shard_map/ppermute | solution.py:29
  49.6 4.6 %collective-permute-start.4 = (bf16[4,2,128,256]{3,2,1,0:T(8,128)(2,1)S(1)}, bf16[4,2,128,256]{3,2,1,0:T(8,128)(2,1)S(1)}, u32[]{:S(2)}, u32[]{:S(2)}) collective-permute-start(bf16[4,2,128,256]{3,2,1,0:T(8,128)(2,1)S(1)} %pad_maximum_fusion.refs_0_), channel_id=1, source_target_pairs={{0,24},{1,7},{2,26},{3,5},{4,28},{5,3},{6,30},{7,1},{8,16},{9,15},... | collective-permute-start | bytes 1572872 | tf_op jit(solution)/shard_map/ppermute | solution.py:29
  54.2 2.8 %collective-permute-start.3 = (bf16[4,2,128,256]{3,2,1,0:T(8,128)(2,1)S(1)}, bf16[4,2,128,256]{3,2,1,0:T(8,128)(2,1)S(1)}, u32[]{:S(2)}, u32[]{:S(2)}) collective-permute-start(bf16[4,2,128,256]{3,2,1,0:T(8,128)(2,1)S(1)} %pad_maximum_fusion.refs_0_), channel_id=1, source_target_pairs={{0,16},{1,5},{2,18},{3,7},{4,20},{5,1},{6,22},{7,3},{8,24},{9,13},... | collective-permute-start | bytes 1572872 | tf_op jit(solution)/shard_map/ppermute | solution.py:29
  59.4 5.3 %collective-permute-start.5 = (bf16[4,2,128,256]{3,2,1,0:T(8,128)(2,1)S(1)}, bf16[4,2,128,256]{3,2,1,0:T(8,128)(2,1)S(1)}, u32[]{:S(2)}, u32[]{:S(2)}) collective-permute-start(bf16[4,2,128,256]{3,2,1,0:T(8,128)(2,1)S(1)} %pad_maximum_fusion.refs_0_), channel_id=1, source_target_pairs={{0,1},{1,0},{2,3},{3,2},{4,5},{5,4},{6,7},{7,6},{8,9},{9,8},{10,11... | collective-permute-start | bytes 1572872 | tf_op jit(solution)/shard_map/ppermute | solution.py:19
  64.8 4.2 %collective-permute-done.4.refs_3_ = bf16[4,2,128,256]{3,2,1,0:T(8,128)(2,1)S(1)} collective-permute-done((bf16[4,2,128,256]{3,2,1,0:T(8,128)(2,1)S(1)}, bf16[4,2,128,256]{3,2,1,0:T(8,128)(2,1)S(1)}, u32[]{:S(2)}, u32[]{:S(2)}) %collective-permute-start.4) | collective-permute-done | bytes 524320 | tf_op jit(solution)/shard_map/ppermute | solution.py:29
  68.9 3.6 %collective-permute-start.8 = (bf16[4,2,128,256]{3,2,1,0:T(8,128)(2,1)S(1)}, bf16[4,2,128,256]{3,2,1,0:T(8,128)(2,1)S(1)}, u32[]{:S(2)}, u32[]{:S(2)}) collective-permute-start(bf16[4,2,128,256]{3,2,1,0:T(8,128)(2,1)S(1)} %collective-permute-done.4.refs_3_), channel_id=1, source_target_pairs={{0,1},{1,0},{2,3},{3,2},{4,5},{5,4},{6,7},{7,6},{8,9},{9,8},{10,11... | collective-permute-start | bytes 1572872 | tf_op jit(solution)/shard_map/ppermute | solution.py:19
  79.7 5.5 %layer.1 = (bf16[16,264,128]{2,1,0:T(8,128)(2,1)}, bf16[512,176]{1,0:T(8,128)(2,1)}) custom-call(bf16[4,2,128,256]{3,2,1,0:T(8,128)(2,1)} %copy-done.2, bf16[4,2,128,256]{3,2,1,0:T(8,128)(2,1)} %copy-done.6, bf16[4,2,128,256]{3,2,1,0:T(8,128)(2,1)} %copy-done.5, bf16[4,2,128,256]{3,2,1,0:T(8,128)(2,1)} %copy-done.4, bf16[4,2,128,256]{3,2,1,0:T(8,128)(2,1)} %copy-done.7, ...), custom_call_target="tpu_custom_call" | custom-call | tf_op jit(solution)/shard_map/layer/pallas_call | solution.py:303
  85.3 7.8 %all-to-all-start.1 = ((bf16[16,264,128]{2,1,0:T(8,128)(2,1)}), bf16[16,264,128]{2,1,0:T(8,128)(2,1)S(1)}, u32[]{:S(2)}, u32[]{:S(2)}) async-start(bf16[16,264,128]{2,1,0:T(8,128)(2,1)} %get-tuple-element.14), calls=%async_computation.1 | async-start | bytes 2162688 | tf_op jit(solution)/shard_map/all_to_all | solution.py:313
  93.0 3.7 %shard_map.86 = (bf16[4,4,128,256]{3,2,1,0:T(8,128)(2,1)}, bf16[4,4,128,256]{3,2,1,0:T(8,128)(2,1)}) custom-call(bf16[512,176]{1,0:T(8,128)(2,1)} %get-tuple-element.11.refs_0_, bf16[16,264,128]{2,1,0:T(8,128)(2,1)} %copy-done.1), custom_call_target="tpu_custom_call" | custom-call | tf_op jit(solution)/shard_map/pallas_call | solution.py:84
  98.9 21.0 %all-to-all-done.1.refs_0_ = bf16[16,264,128]{2,1,0:T(8,128)(2,1)S(1)} async-done(((bf16[16,264,128]{2,1,0:T(8,128)(2,1)}), bf16[16,264,128]{2,1,0:T(8,128)(2,1)S(1)}, u32[]{:S(2)}, u32[]{:S(2)}) %all-to-all-start.1) | async-done | bytes 1081376 | tf_op jit(solution)/shard_map/all_to_all | solution.py:313
  120.8 11.4 %all-to-all-start.2 = ((bf16[4,2,264,128]{3,2,1,0:T(8,128)(2,1)}), bf16[4,2,264,128]{3,2,1,0:T(8,128)(2,1)S(1)}, u32[]{:S(2)}, u32[]{:S(2)}) async-start(bf16[4,2,264,128]{3,2,1,0:T(8,128)(2,1)} %shard_map.87), calls=%async_computation.2 | async-start | bytes 1081344 | tf_op jit(solution)/shard_map/all_to_all | solution.py:315
  132.6 2.5 %collective-permute-start.11 = (bf16[4,128,256]{2,1,0:T(8,128)(2,1)S(1)}, bf16[4,128,256]{2,1,0:T(8,128)(2,1)S(1)}, u32[]{:S(2)}, u32[]{:S(2)}) collective-permute-start(bf16[4,128,256]{2,1,0:T(8,128)(2,1)S(1)} %get-tuple-element.18), channel_id=1, source_target_pairs={{0,2},{1,9},{2,0},{3,11},{4,6},{5,13},{6,4},{7,15},{8,10},{9,1},{1... | collective-permute-start | bytes 786440 | tf_op jit(solution)/shard_map/ppermute | solution.py:29
  135.1 4.1 %collective-permute-start.13 = (bf16[4,128,256]{2,1,0:T(8,128)(2,1)S(1)}, bf16[4,128,256]{2,1,0:T(8,128)(2,1)S(1)}, u32[]{:S(2)}, u32[]{:S(2)}) collective-permute-start(bf16[4,128,256]{2,1,0:T(8,128)(2,1)S(1)} %get-tuple-element.19), channel_id=1, source_target_pairs={{0,6},{1,25},{2,4},{3,27},{4,2},{5,29},{6,0},{7,31},{8,14},{9,17},... | collective-permute-start | bytes 786440 | tf_op jit(solution)/shard_map/ppermute | solution.py:29
  139.3 3.4 %collective-permute-start.12 = (bf16[4,128,256]{2,1,0:T(8,128)(2,1)S(1)}, bf16[4,128,256]{2,1,0:T(8,128)(2,1)S(1)}, u32[]{:S(2)}, u32[]{:S(2)}) collective-permute-start(bf16[4,128,256]{2,1,0:T(8,128)(2,1)S(1)} %get-tuple-element.20), channel_id=1, source_target_pairs={{0,4},{1,17},{2,6},{3,19},{4,0},{5,21},{6,2},{7,23},{8,12},{9,25},... | collective-permute-start | bytes 786440 | tf_op jit(solution)/shard_map/ppermute | solution.py:29
  144.6 4.4 %collective-permute-done.12 = bf16[4,128,256]{2,1,0:T(8,128)(2,1)S(1)} collective-permute-done((bf16[4,128,256]{2,1,0:T(8,128)(2,1)S(1)}, bf16[4,128,256]{2,1,0:T(8,128)(2,1)S(1)}, u32[]{:S(2)}, u32[]{:S(2)}) %collective-permute-start.12) | collective-permute-done | bytes 262176 | tf_op jit(solution)/shard_map/ppermute | solution.py:29
  151.4 4.4 %collective-permute-start.16 = (bf16[128,256]{1,0:T(8,128)(2,1)S(1)}, bf16[128,256]{1,0:T(8,128)(2,1)S(1)}, u32[]{:S(2)}, u32[]{:S(2)}) collective-permute-start(bf16[128,256]{1,0:T(8,128)(2,1)S(1)} %get-tuple-element.22), channel_id=1, source_target_pairs={{0,24},{1,7},{2,26},{3,5},{4,28},{5,3},{6,30},{7,1},{8,16},{9,15},... | collective-permute-start | bytes 196616 | tf_op jit(solution)/shard_map/ppermute | solution.py:29
  155.8 3.3 %collective-permute-start.15 = (bf16[128,256]{1,0:T(8,128)(2,1)S(1)}, bf16[128,256]{1,0:T(8,128)(2,1)S(1)}, u32[]{:S(2)}, u32[]{:S(2)}) collective-permute-start(bf16[128,256]{1,0:T(8,128)(2,1)S(1)} %get-tuple-element.23), channel_id=1, source_target_pairs={{0,16},{1,5},{2,18},{3,7},{4,20},{5,1},{6,22},{7,3},{8,24},{9,13},... | collective-permute-start | bytes 196616 | tf_op jit(solution)/shard_map/ppermute | solution.py:29
  159.1 4.4 %collective-permute-done.15 = bf16[128,256]{1,0:T(8,128)(2,1)S(1)} collective-permute-done((bf16[128,256]{1,0:T(8,128)(2,1)S(1)}, bf16[128,256]{1,0:T(8,128)(2,1)S(1)}, u32[]{:S(2)}, u32[]{:S(2)}) %collective-permute-start.15) | collective-permute-done | bytes 65568 | tf_op jit(solution)/shard_map/ppermute | solution.py:29
  (54 shorter events, 22.8 us)
Async XLA Ops:
  2.4 18.8 %collective-permute-start.9 = (bf16[2,264,128]{2,1,0:T(8,128)(2,1)}, bf16[2,264,128]{2,1,0:T(8,128)(2,1)S(1)}, u32[]{:S(2)}, u32[]{:S(2)}) collective-permute-start(bf16[2,264,128]{2,1,0:T(8,128)(2,1)} %shard_map.84.refs_0_), channel_id=1, source_target_pairs={{0,128},{128,0},{1,129},{129,1},{2,130},{130,2},{3,131},{131,3},{4... | collective-permute-start | bytes 405512 | tf_op jit(solution)/shard_map/ppermute | solution.py:287
  23.2 9.6 %copy-start.11 = (bf16[128,256]{1,0:T(8,128)(2,1)S(1)}, bf16[128,256]{1,0:T(8,128)(2,1)}, u32[]{:S(2)}) copy-start(bf16[128,256]{1,0:T(8,128)(2,1)} %param.5) | copy-start | bytes 196612
  23.2 55.5 %all-to-all-start = ((bf16[16,264,128]{2,1,0:T(8,128)(2,1)}), bf16[16,264,128]{2,1,0:T(8,128)(2,1)S(1)}, u32[]{:S(2)}, u32[]{:S(2)}) async-start(bf16[16,264,128]{2,1,0:T(8,128)(2,1)} %shard_map.85), calls=%async_computation | async-start | bytes 2162688 | tf_op jit(solution)/shard_map/all_to_all | solution.py:289
  32.9 6.9 %collective-permute-start = (bf16[2,128,256]{2,1,0:T(8,128)(2,1)S(1)}, bf16[2,128,256]{2,1,0:T(8,128)(2,1)S(1)}, u32[]{:S(2)}, u32[]{:S(2)}) collective-permute-start(bf16[2,128,256]{2,1,0:T(8,128)(2,1)S(1)} %get-tuple-element.25), channel_id=1, source_target_pairs={{0,2},{1,9},{2,0},{3,11},{4,6},{5,13},{6,4},{7,15},{8,10},{9,1},{1... | collective-permute-start | bytes 393224 | tf_op jit(solution)/shard_map/ppermute | solution.py:29
  39.7 9.8 %collective-permute-start.1 = (bf16[2,2,128,256]{3,2,1,0:T(8,128)(2,1)S(1)}, bf16[2,2,128,256]{3,2,1,0:T(8,128)(2,1)S(1)}, u32[]{:S(2)}, u32[]{:S(2)}) collective-permute-start(bf16[2,2,128,256]{3,2,1,0:T(8,128)(2,1)S(1)} %pad_maximum_fusion.1), channel_id=1, source_target_pairs={{0,4},{1,17},{2,6},{3,19},{4,0},{5,21},{6,2},{7,23},{8,12},{9,25},... | collective-permute-start | bytes 786440 | tf_op jit(solution)/shard_map/ppermute | solution.py:29
  49.6 29.1 %copy-start.2 = (bf16[4,2,128,256]{3,2,1,0:T(8,128)(2,1)}, bf16[4,2,128,256]{3,2,1,0:T(8,128)(2,1)S(1)}, u32[]{:S(2)}) copy-start(bf16[4,2,128,256]{3,2,1,0:T(8,128)(2,1)S(1)} %pad_maximum_fusion.refs_0_) | copy-start | bytes 1572868
  49.6 19.3 %collective-permute-start.4 = (bf16[4,2,128,256]{3,2,1,0:T(8,128)(2,1)S(1)}, bf16[4,2,128,256]{3,2,1,0:T(8,128)(2,1)S(1)}, u32[]{:S(2)}, u32[]{:S(2)}) collective-permute-start(bf16[4,2,128,256]{3,2,1,0:T(8,128)(2,1)S(1)} %pad_maximum_fusion.refs_0_), channel_id=1, source_target_pairs={{0,24},{1,7},{2,26},{3,5},{4,28},{5,3},{6,30},{7,1},{8,16},{9,15},... | collective-permute-start | bytes 1572872 | tf_op jit(solution)/shard_map/ppermute | solution.py:29
  54.2 18.3 %collective-permute-start.3 = (bf16[4,2,128,256]{3,2,1,0:T(8,128)(2,1)S(1)}, bf16[4,2,128,256]{3,2,1,0:T(8,128)(2,1)S(1)}, u32[]{:S(2)}, u32[]{:S(2)}) collective-permute-start(bf16[4,2,128,256]{3,2,1,0:T(8,128)(2,1)S(1)} %pad_maximum_fusion.refs_0_), channel_id=1, source_target_pairs={{0,16},{1,5},{2,18},{3,7},{4,20},{5,1},{6,22},{7,3},{8,24},{9,13},... | collective-permute-start | bytes 1572872 | tf_op jit(solution)/shard_map/ppermute | solution.py:29
  56.9 17.5 %collective-permute-start.2 = (bf16[4,2,128,256]{3,2,1,0:T(8,128)(2,1)S(1)}, bf16[4,2,128,256]{3,2,1,0:T(8,128)(2,1)S(1)}, u32[]{:S(2)}, u32[]{:S(2)}) collective-permute-start(bf16[4,2,128,256]{3,2,1,0:T(8,128)(2,1)S(1)} %pad_maximum_fusion.refs_0_), channel_id=1, source_target_pairs={{0,8},{1,3},{2,10},{3,1},{4,12},{5,7},{6,14},{7,5},{8,0},{9,11},{1... | collective-permute-start | bytes 1572872 | tf_op jit(solution)/shard_map/ppermute | solution.py:29
  59.4 17.5 %collective-permute-start.5 = (bf16[4,2,128,256]{3,2,1,0:T(8,128)(2,1)S(1)}, bf16[4,2,128,256]{3,2,1,0:T(8,128)(2,1)S(1)}, u32[]{:S(2)}, u32[]{:S(2)}) collective-permute-start(bf16[4,2,128,256]{3,2,1,0:T(8,128)(2,1)S(1)} %pad_maximum_fusion.refs_0_), channel_id=1, source_target_pairs={{0,1},{1,0},{2,3},{3,2},{4,5},{5,4},{6,7},{7,6},{8,9},{9,8},{10,11... | collective-permute-start | bytes 1572872 | tf_op jit(solution)/shard_map/ppermute | solution.py:19
  68.9 9.8 %copy-start.4 = (bf16[4,2,128,256]{3,2,1,0:T(8,128)(2,1)}, bf16[4,2,128,256]{3,2,1,0:T(8,128)(2,1)S(1)}, u32[]{:S(2)}) copy-start(bf16[4,2,128,256]{3,2,1,0:T(8,128)(2,1)S(1)} %collective-permute-done.4.refs_3_) | copy-start | bytes 1572868
  68.9 8.0 %collective-permute-start.8 = (bf16[4,2,128,256]{3,2,1,0:T(8,128)(2,1)S(1)}, bf16[4,2,128,256]{3,2,1,0:T(8,128)(2,1)S(1)}, u32[]{:S(2)}, u32[]{:S(2)}) collective-permute-start(bf16[4,2,128,256]{3,2,1,0:T(8,128)(2,1)S(1)} %collective-permute-done.4.refs_3_), channel_id=1, source_target_pairs={{0,1},{1,0},{2,3},{3,2},{4,5},{5,4},{6,7},{7,6},{8,9},{9,8},{10,11... | collective-permute-start | bytes 1572872 | tf_op jit(solution)/shard_map/ppermute | solution.py:19
  72.5 4.4 %collective-permute-start.7 = (bf16[4,2,128,256]{3,2,1,0:T(8,128)(2,1)S(1)}, bf16[4,2,128,256]{3,2,1,0:T(8,128)(2,1)S(1)}, u32[]{:S(2)}, u32[]{:S(2)}) collective-permute-start(bf16[4,2,128,256]{3,2,1,0:T(8,128)(2,1)S(1)} %collective-permute-done.3.refs_2_), channel_id=1, source_target_pairs={{0,1},{1,0},{2,3},{3,2},{4,5},{5,4},{6,7},{7,6},{8,9},{9,8},{10,11... | collective-permute-start | bytes 1572872 | tf_op jit(solution)/shard_map/ppermute | solution.py:19
  74.5 4.2 %collective-permute-start.6 = (bf16[4,2,128,256]{3,2,1,0:T(8,128)(2,1)S(1)}, bf16[4,2,128,256]{3,2,1,0:T(8,128)(2,1)}, u32[]{:S(2)}, u32[]{:S(2)}) collective-permute-start(bf16[4,2,128,256]{3,2,1,0:T(8,128)(2,1)S(1)} %collective-permute-done.2.refs_1_), channel_id=1, source_target_pairs={{0,1},{1,0},{2,3},{3,2},{4,5},{5,4},{6,7},{7,6},{8,9},{9,8},{10,11... | collective-permute-start | bytes 1572872 | tf_op jit(solution)/shard_map/ppermute | solution.py:19
  85.3 34.5 %all-to-all-start.1 = ((bf16[16,264,128]{2,1,0:T(8,128)(2,1)}), bf16[16,264,128]{2,1,0:T(8,128)(2,1)S(1)}, u32[]{:S(2)}, u32[]{:S(2)}) async-start(bf16[16,264,128]{2,1,0:T(8,128)(2,1)} %get-tuple-element.14), calls=%async_computation.1 | async-start | bytes 2162688 | tf_op jit(solution)/shard_map/all_to_all | solution.py:313
  96.8 35.5 %copy-start.3 = (bf16[4,4,128,256]{3,2,1,0:T(8,128)(2,1)S(1)}, bf16[4,4,128,256]{3,2,1,0:T(8,128)(2,1)}, u32[]{:S(2)}) copy-start(bf16[4,4,128,256]{3,2,1,0:T(8,128)(2,1)} %get-tuple-element.12) | copy-start | bytes 3145732
  96.8 35.5 %collective-permute-start.10 = (bf16[4,4,128,256]{3,2,1,0:T(8,128)(2,1)}, bf16[4,4,128,256]{3,2,1,0:T(8,128)(2,1)S(1)}, u32[]{:S(2)}, u32[]{:S(2)}) collective-permute-start(bf16[4,4,128,256]{3,2,1,0:T(8,128)(2,1)} %get-tuple-element.13), channel_id=1, source_target_pairs={{0,1},{1,0},{2,3},{3,2},{4,5},{5,4},{6,7},{7,6},{8,9},{9,8},{10,11... | collective-permute-start | bytes 3145736 | tf_op jit(solution)/shard_map/ppermute | solution.py:19
  120.8 43.3 %all-to-all-start.2 = ((bf16[4,2,264,128]{3,2,1,0:T(8,128)(2,1)}), bf16[4,2,264,128]{3,2,1,0:T(8,128)(2,1)S(1)}, u32[]{:S(2)}, u32[]{:S(2)}) async-start(bf16[4,2,264,128]{3,2,1,0:T(8,128)(2,1)} %shard_map.87), calls=%async_computation.2 | async-start | bytes 1081344 | tf_op jit(solution)/shard_map/all_to_all | solution.py:315
  132.6 10.0 %collective-permute-start.11 = (bf16[4,128,256]{2,1,0:T(8,128)(2,1)S(1)}, bf16[4,128,256]{2,1,0:T(8,128)(2,1)S(1)}, u32[]{:S(2)}, u32[]{:S(2)}) collective-permute-start(bf16[4,128,256]{2,1,0:T(8,128)(2,1)S(1)} %get-tuple-element.18), channel_id=1, source_target_pairs={{0,2},{1,9},{2,0},{3,11},{4,6},{5,13},{6,4},{7,15},{8,10},{9,1},{1... | collective-permute-start | bytes 786440 | tf_op jit(solution)/shard_map/ppermute | solution.py:29
  135.1 9.5 %collective-permute-start.13 = (bf16[4,128,256]{2,1,0:T(8,128)(2,1)S(1)}, bf16[4,128,256]{2,1,0:T(8,128)(2,1)S(1)}, u32[]{:S(2)}, u32[]{:S(2)}) collective-permute-start(bf16[4,128,256]{2,1,0:T(8,128)(2,1)S(1)} %get-tuple-element.19), channel_id=1, source_target_pairs={{0,6},{1,25},{2,4},{3,27},{4,2},{5,29},{6,0},{7,31},{8,14},{9,17},... | collective-permute-start | bytes 786440 | tf_op jit(solution)/shard_map/ppermute | solution.py:29
  139.3 9.8 %collective-permute-start.12 = (bf16[4,128,256]{2,1,0:T(8,128)(2,1)S(1)}, bf16[4,128,256]{2,1,0:T(8,128)(2,1)S(1)}, u32[]{:S(2)}, u32[]{:S(2)}) collective-permute-start(bf16[4,128,256]{2,1,0:T(8,128)(2,1)S(1)} %get-tuple-element.20), channel_id=1, source_target_pairs={{0,4},{1,17},{2,6},{3,19},{4,0},{5,21},{6,2},{7,23},{8,12},{9,25},... | collective-permute-start | bytes 786440 | tf_op jit(solution)/shard_map/ppermute | solution.py:29
  149.2 9.8 %collective-permute-start.14 = (bf16[128,256]{1,0:T(8,128)(2,1)S(1)}, bf16[128,256]{1,0:T(8,128)(2,1)S(1)}, u32[]{:S(2)}, u32[]{:S(2)}) collective-permute-start(bf16[128,256]{1,0:T(8,128)(2,1)S(1)} %get-tuple-element.21), channel_id=1, source_target_pairs={{0,8},{1,3},{2,10},{3,1},{4,12},{5,7},{6,14},{7,5},{8,0},{9,11},{1... | collective-permute-start | bytes 196616 | tf_op jit(solution)/shard_map/ppermute | solution.py:29
  151.4 7.7 %collective-permute-start.16 = (bf16[128,256]{1,0:T(8,128)(2,1)S(1)}, bf16[128,256]{1,0:T(8,128)(2,1)S(1)}, u32[]{:S(2)}, u32[]{:S(2)}) collective-permute-start(bf16[128,256]{1,0:T(8,128)(2,1)S(1)} %get-tuple-element.22), channel_id=1, source_target_pairs={{0,24},{1,7},{2,26},{3,5},{4,28},{5,3},{6,30},{7,1},{8,16},{9,15},... | collective-permute-start | bytes 196616 | tf_op jit(solution)/shard_map/ppermute | solution.py:29
  155.8 7.7 %collective-permute-start.15 = (bf16[128,256]{1,0:T(8,128)(2,1)S(1)}, bf16[128,256]{1,0:T(8,128)(2,1)S(1)}, u32[]{:S(2)}, u32[]{:S(2)}) collective-permute-start(bf16[128,256]{1,0:T(8,128)(2,1)S(1)} %get-tuple-element.23), channel_id=1, source_target_pairs={{0,16},{1,5},{2,18},{3,7},{4,20},{5,1},{6,22},{7,3},{8,24},{9,13},... | collective-permute-start | bytes 196616 | tf_op jit(solution)/shard_map/ppermute | solution.py:29
  (8 other events, 24.5 us)

commit v5 on v4

--- a/solution.py
+++ b/solution.py
@@ -96,37 +96,37 @@
     return jnp.concatenate([a, b], axis=1)
 
 
-def pack_body(wg, wu, wd, out):
+def cut_of(n):
+    return -(-n // 32) * 16
+
+
+def pack_body(wg, wu, wd, out, every):
     hid = wd.shape[1] // NY
+    cut = out.shape[1]
     tg = wg[...].astype(F32).T
     tu = wu[...].astype(F32).T
     td = wd[...].astype(F32).T
-    parts = []
     for y in range(NY):
         s = slice(y * hid, (y + 1) * hid)
-        parts.append(jnp.concatenate([tg[s], tu[s], td[s]], axis=0))
-    out[0] = sides(parts[0], parts[2]).astype(BF)
-    out[1] = sides(parts[1], parts[3]).astype(BF)
-
-
-def spread_body(own, far, out):
-    half = own.shape[2] // 2
-    for i in range(2):
-        o, f = own[i].astype(F32), far[i].astype(F32)
-        low = sides(o[:, :half], f[:, :half]).astype(BF)
-        high = sides(o[:, half:], f[:, half:]).astype(BF)
-        for r in range(NR):
-            out[r * NY + i] = low
-            out[r * NY + i + 2] = high
-
-
-def weights_into(wt, chunks, r, rows):
-    half = chunks.shape[2] // 2
-    for side in range(NQ):
-        cut = slice(side * half, (side + 1) * half)
-        wt[NQ * r + side] = jnp.concatenate(
-            [chunks[r * NY + y][:rows, cut] for y in range(NY)], axis=1
-        )
+        part = jnp.concatenate([tg[s], tu[s], td[s]], axis=0)
+        gap = jnp.zeros((2 * cut - part.shape[0], part.shape[1]), F32)
+        low = jnp.concatenate([part[cut:], gap], axis=0)
+        part = sides(part[:cut], low).astype(BF)
+        out[y] = part
+        for r in range(NR):
+            every[r * NY + y] = part
+
+
+def weights_into(wt, chunks, r, side, rows):
+    n, width = chunks.shape[1:]
+    half = width // 2
+
+    def whole(chunk):
+        if rows <= n:
+            return chunk[:rows, :half]
+        return jnp.concatenate([chunk[:, :half], chunk[: rows - n, half:]], axis=0)
+
+    wt[NQ * r + side] = jnp.concatenate([whole(chunks[r * NY + y]) for y in range(NY)], axis=1)
 
 
 def near_x(side, r, zq, x_here):
@@ -134,26 +134,30 @@
 
 
 def layer_body(refs):
-    mine, other, chunks_far = refs[:4], refs[4:8], refs[8]
-    pieces_far, turned_far = refs[9:11]
-    one, two, chunks, pieces, turned, wt, sems = refs[11:]
+    mine, other, chunks_far = refs[:4], refs[4:8], refs[8:10]
+    pieces_far, turned_far = refs[10:12]
+    one, two, near, far, pieces, turned, wt, sems = refs[12:]
     core = lax.axis_index("c")
     x_here = lax.axis_index("x")
     zq = lax.axis_index("zq")
-    hid = chunks.shape[1] // 3
-    half = chunks.shape[2] // 2
-
-    first = pltpu.make_async_copy(chunks_far, chunks, sems.at[8])
-    first.start()
+    hid = wt.shape[1] // 3
+    half = pieces.shape[2] // 2
+
+    first = [
+        pltpu.make_async_copy(chunks_far[i], v, sems.at[8 + i]) for i, v in enumerate((near, far))
+    ]
+    for c in first:
+        c.start()
     loads = []
     for i in range(4):
         loads.append(pltpu.make_async_copy(mine[i], one.at[i], sems.at[i]))
         loads.append(pltpu.make_async_copy(other[i], two.at[i], sems.at[4 + i]))
     for c in loads:
         c.start()
-    first.wait()
-    for r in range(NR):
-        weights_into(wt, chunks, r, 3 * hid)
+    for side, v in enumerate((near, far)):
+        first[side].wait()
+        for r in range(NR):
+            weights_into(wt, v, r, side, 3 * hid)
     for c in loads:
         c.wait()
 
@@ -207,13 +211,14 @@
         run(two, one)
 
 
-def back_body(turned, chunks, keep, send, wt):
+def back_body(turned, near, far, keep, send, wt):
     core = lax.axis_index("c")
     x_here = lax.axis_index("x")
     zq = lax.axis_index("zq")
     rows = turned.shape[0] // NY
-    for r in range(NR):
-        weights_into(wt, chunks, r, wt.shape[1])
+    for side, v in enumerate((near, far)):
+        for r in range(NR):
+            weights_into(wt, v, r, side, wt.shape[1])
 
     def run(me):
         for r in range(NR):
@@ -277,16 +282,18 @@
     hid = ff // NY
     rows, cols = inputs.shape
 
-    packed = call(
+    cut = cut_of(3 * hid)
+    packed, near = call(
         pack_body,
         (gate_weight, up_weight, down_weight.T),
-        S((2, 3 * hid, 2 * rows_d), BF),
+        [S((NY, cut, 2 * rows_d), BF), S((NR * NY, cut, 2 * rows_d), BF)],
         60,
         far_in=3,
     )
     far = lax.ppermute(packed, "zq", [(0, 1), (1, 0)])
-    chunks = call(spread_body, (packed, far), S((NR * NY, 3 * hid, 2 * rows_d), BF))
-    chunks = lax.all_to_all(chunks, ("zr", "y"), 0, 0, tiled=True)
+    near = lax.all_to_all(near, ("zr", "y"), 0, 0, tiled=True)
+    far = jnp.broadcast_to(far[None], (NR, *far.shape)).reshape(near.shape)
+    far = lax.all_to_all(far, ("zr", "y"), 0, 0, tiled=True)
 
     block = jnp.stack([inputs, cotangent])
     line = line_double(block, 0)
@@ -296,19 +303,19 @@
     tiles = S((4, 4, rows, cols), BF)
     turned = S((NY * rows, 2 * hid), BF)
     joint = (4, *mine[0].shape)
-    made = [S(chunks.shape, BF), turned]
-    far = pl.BlockSpec(memory_space=pltpu.HBM)
-    shapes = (joint, joint, chunks.shape, chunks.shape, turned.shape)
+    out = (NR * NY, 3 * hid, NQ * rows_d)
+    hbm = pl.BlockSpec(memory_space=pltpu.HBM)
+    shapes = (joint, joint, near.shape, far.shape, out, turned.shape)
     shapes += ((NQ * NR, 3 * hid, NY * rows_d),)
     pieces, turned = pl.pallas_call(
         lambda *refs: layer_body(refs),
-        in_specs=[far] * 9,
-        out_specs=[far] * 2,
-        out_shape=made,
-        scratch_shapes=[pltpu.VMEM(s, BF) for s in shapes] + [pltpu.SemaphoreType.DMA((9,))],
+        in_specs=[hbm] * 10,
+        out_specs=[hbm] * 2,
+        out_shape=[S(out, BF), turned],
+        scratch_shapes=[pltpu.VMEM(s, BF) for s in shapes] + [pltpu.SemaphoreType.DMA((10,))],
         compiler_params=pltpu.CompilerParams(vmem_limit_bytes=60 * 2**20),
         name="layer",
-    )(*mine, *other, chunks)
+    )(*mine, *other, near, far)
 
     pieces = lax.all_to_all(pieces, ("zr", "y"), 0, 0, tiled=True)
     ring = call(sum_body, (pieces,), S((4, 2, 3 * hid, 2 * rows_d), BF))
@@ -317,10 +324,10 @@
 
     keep, send = call(
         back_body,
-        (turned, chunks),
+        (turned, near, far),
         [tiles, tiles],
         60,
-        far_in=2,
+        far_in=3,
         far_out=True,
         own=[pltpu.VMEM((NQ * NR, 2 * hid, NY * rows_d), BF)],
     )

time: 166 us -> 172 us (1.036)
  waiting for transfers between devices: 53.9 us -> 60.8 us
    all_to_all x1 -> x2, starting transfers between devices: 9.57 us -> 19.1 us  [the longest x1 10.1 us: per_device(): far = lax.all_to_all(far, ('zr', 'y'), 0, 0, tiled=True)]
    ppermute x5, starting transfers between devices: 15.3 us -> 10.2 us  [swapped(): return lax.ppermute(value, 'c', [(0, 1), (1, 0)])]
    ppermute x1, waiting for transfers between devices: 9.67 us -> 13.7 us  [per_device(): far = lax.ppermute(packed, 'zq', [(0, 1), (1, 0)])]
    all_to_all x1, starting transfers between devices: 11.4 us -> 7.58 us  [per_device(): ring = lax.all_to_all(ring, ('zh', 'zq'), 0, 0, tiled=True)]
    ppermute x11, waiting for transfers between devices: 23.2 us -> 26 us  [moved(): return lax.ppermute(value, PLANE, pairs)]
    unnamed x24 -> x26, local copies, waits for them, and re-layouts: 3.68 us -> 2.5 us
    pallas_call x5 -> x4, Pallas kernels: 8.59 us -> 7.92 us  [call(): pl.pallas_call(whole, in_specs=[far] * loads + [VM] * (n - loads), out_sp...]
  transfers between devices with their start and end apart: 20 -> 21, of which waited for: 8 -> 9; matrix products, arithmetic and copies ran while one was open for 1% -> 1% of each run, Pallas kernels for 3% -> 3%
where the time goes in v5:
time: 172 us; the launch traced here: 171 us
  starting transfers between devices  91.1 us (53%)
  waiting for transfers between devices  60.8 us (35%)
  Pallas kernels  13.5 us (8%)
  local copies, waits for them, and re-layouts  3.55 us (2%)
    ppermute x11, starting transfers between devices, moved(): return lax.ppermute(value, PLANE, pairs)  37.9 us
    ppermute x11, waiting for transfers between devices, moved(): return lax.ppermute(value, PLANE, pairs)  26 us
    all_to_all x1, waiting for transfers between devices, per_device(): pieces = lax.all_to_all(pieces, ('zr', 'y'), 0, 0, tiled=True)  20.7 us
    ppermute x1, waiting for transfers between devices, per_device(): far = lax.ppermute(packed, 'zq', [(0, 1), (1, 0)])  13.7 us
    ppermute x5, starting transfers between devices, swapped(): return lax.ppermute(value, 'c', [(0, 1), (1, 0)])  10.2 us
    all_to_all x1, starting transfers between devices, per_device(): far = lax.all_to_all(far, ('zr', 'y'), 0, 0, tiled=True)  10.1 us
    ppermute x1, starting transfers between devices, per_device(): far = lax.ppermute(packed, 'zq', [(0, 1), (1, 0)])  9.04 us
    all_to_all x1, starting transfers between devices, per_device(): near = lax.all_to_all(near, ('zr', 'y'), 0, 0, tiled=True)  8.99 us
  transfers between devices with their start and end apart: 21, of which 9 were waited for; matrix products, arithmetic and copies ran while one was open for 1% of the time, Pallas kernels for 3%

profile of v5, /device:TPU:32, one launch (start us, length us, event | category | flops | bytes accessed | tf_op | source)
XLA Modules:
  0.0 171.2 jit_solution(9259954452884288507)
XLA Ops:
  2.6 9.0 %all-to-all-start = ((bf16[16,144,128]{2,1,0:T(8,128)(2,1)}), bf16[16,144,128]{2,1,0:T(8,128)(2,1)S(1)}, u32[]{:S(2)}, u32[]{:S(2)}) async-start(bf16[16,144,128]{2,1,0:T(8,128)(2,1)} %get-tuple-element.13), calls=%async_computation | async-start | bytes 1179648 | tf_op jit(solution)/shard_map/all_to_all | solution.py:294
  11.7 9.0 %collective-permute-start.9 = (bf16[4,144,128]{2,1,0:T(8,128)(2,1)S(1)}, bf16[4,144,128]{2,1,0:T(8,128)(2,1)S(1)}, u32[]{:S(2)}, u32[]{:S(2)}) collective-permute-start(bf16[4,144,128]{2,1,0:T(8,128)(2,1)S(1)} %copy-done.12), channel_id=1, source_target_pairs={{0,128},{128,0},{1,129},{129,1},{2,130},{130,2},{3,131},{131,3},{4... | collective-permute-start | bytes 442376 | tf_op jit(solution)/shard_map/ppermute | solution.py:293
  20.7 13.7 %collective-permute-done.9 = bf16[4,144,128]{2,1,0:T(8,128)(2,1)S(1)} collective-permute-done((bf16[4,144,128]{2,1,0:T(8,128)(2,1)S(1)}, bf16[4,144,128]{2,1,0:T(8,128)(2,1)S(1)}, u32[]{:S(2)}, u32[]{:S(2)}) %collective-permute-start.9) | collective-permute-done | bytes 147488 | tf_op jit(solution)/shard_map/ppermute | solution.py:293
  35.4 10.1 %all-to-all-start.1 = ((bf16[16,144,128]{2,1,0:T(8,128)(2,1)}), bf16[16,144,128]{2,1,0:T(8,128)(2,1)S(1)}, u32[]{:S(2)}, u32[]{:S(2)}) async-start(bf16[16,144,128]{2,1,0:T(8,128)(2,1)} %bitcast.5), calls=%async_computation.1 | async-start | bytes 1179648 | tf_op jit(solution)/shard_map/all_to_all | solution.py:296
  45.6 3.4 %collective-permute-start = (bf16[2,128,256]{2,1,0:T(8,128)(2,1)S(1)}, bf16[2,128,256]{2,1,0:T(8,128)(2,1)S(1)}, u32[]{:S(2)}, u32[]{:S(2)}) collective-permute-start(bf16[2,128,256]{2,1,0:T(8,128)(2,1)S(1)} %get-tuple-element.29), channel_id=1, source_target_pairs={{0,2},{1,9},{2,0},{3,11},{4,6},{5,13},{6,4},{7,15},{8,10},{9,1},{1... | collective-permute-start | bytes 393224 | tf_op jit(solution)/shard_map/ppermute | solution.py:29
  49.0 3.5 %collective-permute-done = bf16[2,128,256]{2,1,0:T(8,128)(2,1)S(1)} collective-permute-done((bf16[2,128,256]{2,1,0:T(8,128)(2,1)S(1)}, bf16[2,128,256]{2,1,0:T(8,128)(2,1)S(1)}, u32[]{:S(2)}, u32[]{:S(2)}) %collective-permute-start) | collective-permute-done | bytes 131104 | tf_op jit(solution)/shard_map/ppermute | solution.py:29
  52.5 4.9 %collective-permute-start.1 = (bf16[2,2,128,256]{3,2,1,0:T(8,128)(2,1)S(1)}, bf16[2,2,128,256]{3,2,1,0:T(8,128)(2,1)S(1)}, u32[]{:S(2)}, u32[]{:S(2)}) collective-permute-start(bf16[2,2,128,256]{3,2,1,0:T(8,128)(2,1)S(1)} %pad_maximum_fusion.1), channel_id=1, source_target_pairs={{0,4},{1,17},{2,6},{3,19},{4,0},{5,21},{6,2},{7,23},{8,12},{9,25},... | collective-permute-start | bytes 786440 | tf_op jit(solution)/shard_map/ppermute | solution.py:29
  57.4 4.8 %collective-permute-done.1 = bf16[2,2,128,256]{3,2,1,0:T(8,128)(2,1)S(1)} collective-permute-done((bf16[2,2,128,256]{3,2,1,0:T(8,128)(2,1)S(1)}, bf16[2,2,128,256]{3,2,1,0:T(8,128)(2,1)S(1)}, u32[]{:S(2)}, u32[]{:S(2)}) %collective-permute-start.1) | collective-permute-done | bytes 262176 | tf_op jit(solution)/shard_map/ppermute | solution.py:29
  62.3 4.6 %collective-permute-start.4 = (bf16[4,2,128,256]{3,2,1,0:T(8,128)(2,1)S(1)}, bf16[4,2,128,256]{3,2,1,0:T(8,128)(2,1)S(1)}, u32[]{:S(2)}, u32[]{:S(2)}) collective-permute-start(bf16[4,2,128,256]{3,2,1,0:T(8,128)(2,1)S(1)} %pad_maximum_fusion.refs_0_), channel_id=1, source_target_pairs={{0,24},{1,7},{2,26},{3,5},{4,28},{5,3},{6,30},{7,1},{8,16},{9,15},... | collective-permute-start | bytes 1572872 | tf_op jit(solution)/shard_map/ppermute | solution.py:29
  66.9 2.8 %collective-permute-start.3 = (bf16[4,2,128,256]{3,2,1,0:T(8,128)(2,1)S(1)}, bf16[4,2,128,256]{3,2,1,0:T(8,128)(2,1)S(1)}, u32[]{:S(2)}, u32[]{:S(2)}) collective-permute-start(bf16[4,2,128,256]{3,2,1,0:T(8,128)(2,1)S(1)} %pad_maximum_fusion.refs_0_), channel_id=1, source_target_pairs={{0,16},{1,5},{2,18},{3,7},{4,20},{5,1},{6,22},{7,3},{8,24},{9,13},... | collective-permute-start | bytes 1572872 | tf_op jit(solution)/shard_map/ppermute | solution.py:29
  74.1 6.1 %collective-permute-done.4.refs_3_ = bf16[4,2,128,256]{3,2,1,0:T(8,128)(2,1)S(1)} collective-permute-done((bf16[4,2,128,256]{3,2,1,0:T(8,128)(2,1)S(1)}, bf16[4,2,128,256]{3,2,1,0:T(8,128)(2,1)S(1)}, u32[]{:S(2)}, u32[]{:S(2)}) %collective-permute-start.4) | collective-permute-done | bytes 524320 | tf_op jit(solution)/shard_map/ppermute | solution.py:29
  89.4 5.6 %layer.1 = (bf16[16,264,128]{2,1,0:T(8,128)(2,1)}, bf16[512,176]{1,0:T(8,128)(2,1)}) custom-call(bf16[4,2,128,256]{3,2,1,0:T(8,128)(2,1)} %copy-done.2, bf16[4,2,128,256]{3,2,1,0:T(8,128)(2,1)} %copy-done.6, bf16[4,2,128,256]{3,2,1,0:T(8,128)(2,1)} %copy-done.5, bf16[4,2,128,256]{3,2,1,0:T(8,128)(2,1)} %copy-done.4, bf16[4,2,128,256]{3,2,1,0:T(8,128)(2,1)} %copy-done.7, ...), custom_call_target="tpu_custom_call" | custom-call | tf_op jit(solution)/shard_map/layer/pallas_call | solution.py:310
  95.0 7.2 %all-to-all-start.2 = ((bf16[16,264,128]{2,1,0:T(8,128)(2,1)}), bf16[16,264,128]{2,1,0:T(8,128)(2,1)S(1)}, u32[]{:S(2)}, u32[]{:S(2)}) async-start(bf16[16,264,128]{2,1,0:T(8,128)(2,1)} %get-tuple-element.18), calls=%async_computation.2 | async-start | bytes 2162688 | tf_op jit(solution)/shard_map/all_to_all | solution.py:320
  102.2 4.0 %shard_map.85 = (bf16[4,4,128,256]{3,2,1,0:T(8,128)(2,1)}, bf16[4,4,128,256]{3,2,1,0:T(8,128)(2,1)}) custom-call(bf16[512,176]{1,0:T(8,128)(2,1)} %get-tuple-element.15.refs_0_, bf16[16,144,128]{2,1,0:T(8,128)(2,1)} %copy-done, bf16[16,144,128]{2,1,0:T(8,128)(2,1)} %copy-done.1), custom_call_target="tpu_custom_call" | custom-call | tf_op jit(solution)/shard_map/pallas_call | solution.py:84
  108.3 20.7 %all-to-all-done.2.refs_0_ = bf16[16,264,128]{2,1,0:T(8,128)(2,1)S(1)} async-done(((bf16[16,264,128]{2,1,0:T(8,128)(2,1)}), bf16[16,264,128]{2,1,0:T(8,128)(2,1)S(1)}, u32[]{:S(2)}, u32[]{:S(2)}) %all-to-all-start.2) | async-done | bytes 1081376 | tf_op jit(solution)/shard_map/all_to_all | solution.py:320
  130.0 7.6 %all-to-all-start.3 = ((bf16[4,2,264,128]{3,2,1,0:T(8,128)(2,1)}), bf16[4,2,264,128]{3,2,1,0:T(8,128)(2,1)S(1)}, u32[]{:S(2)}, u32[]{:S(2)}) async-start(bf16[4,2,264,128]{3,2,1,0:T(8,128)(2,1)} %shard_map.86), calls=%async_computation.3 | async-start | bytes 1081344 | tf_op jit(solution)/shard_map/all_to_all | solution.py:322
  137.9 3.4 %collective-permute-start.11 = (bf16[4,128,256]{2,1,0:T(8,128)(2,1)S(1)}, bf16[4,128,256]{2,1,0:T(8,128)(2,1)S(1)}, u32[]{:S(2)}, u32[]{:S(2)}) collective-permute-start(bf16[4,128,256]{2,1,0:T(8,128)(2,1)S(1)} %get-tuple-element.22), channel_id=1, source_target_pairs={{0,2},{1,9},{2,0},{3,11},{4,6},{5,13},{6,4},{7,15},{8,10},{9,1},{1... | collective-permute-start | bytes 786440 | tf_op jit(solution)/shard_map/ppermute | solution.py:29
  141.3 4.0 %collective-permute-start.13 = (bf16[4,128,256]{2,1,0:T(8,128)(2,1)S(1)}, bf16[4,128,256]{2,1,0:T(8,128)(2,1)S(1)}, u32[]{:S(2)}, u32[]{:S(2)}) collective-permute-start(bf16[4,128,256]{2,1,0:T(8,128)(2,1)S(1)} %get-tuple-element.23), channel_id=1, source_target_pairs={{0,6},{1,25},{2,4},{3,27},{4,2},{5,29},{6,0},{7,31},{8,14},{9,17},... | collective-permute-start | bytes 786440 | tf_op jit(solution)/shard_map/ppermute | solution.py:29
  145.4 2.6 %collective-permute-start.12 = (bf16[4,128,256]{2,1,0:T(8,128)(2,1)S(1)}, bf16[4,128,256]{2,1,0:T(8,128)(2,1)S(1)}, u32[]{:S(2)}, u32[]{:S(2)}) collective-permute-start(bf16[4,128,256]{2,1,0:T(8,128)(2,1)S(1)} %get-tuple-element.24), channel_id=1, source_target_pairs={{0,4},{1,17},{2,6},{3,19},{4,0},{5,21},{6,2},{7,23},{8,12},{9,25},... | collective-permute-start | bytes 786440 | tf_op jit(solution)/shard_map/ppermute | solution.py:29
  147.9 2.9 %collective-permute-done.13 = bf16[4,128,256]{2,1,0:T(8,128)(2,1)S(1)} collective-permute-done((bf16[4,128,256]{2,1,0:T(8,128)(2,1)S(1)}, bf16[4,128,256]{2,1,0:T(8,128)(2,1)S(1)}, u32[]{:S(2)}, u32[]{:S(2)}) %collective-permute-start.13) | collective-permute-done | bytes 262176 | tf_op jit(solution)/shard_map/ppermute | solution.py:29
  150.8 4.3 %collective-permute-done.12 = bf16[4,128,256]{2,1,0:T(8,128)(2,1)S(1)} collective-permute-done((bf16[4,128,256]{2,1,0:T(8,128)(2,1)S(1)}, bf16[4,128,256]{2,1,0:T(8,128)(2,1)S(1)}, u32[]{:S(2)}, u32[]{:S(2)}) %collective-permute-start.12) | collective-permute-done | bytes 262176 | tf_op jit(solution)/shard_map/ppermute | solution.py:29
  157.5 4.4 %collective-permute-start.16 = (bf16[128,256]{1,0:T(8,128)(2,1)S(1)}, bf16[128,256]{1,0:T(8,128)(2,1)S(1)}, u32[]{:S(2)}, u32[]{:S(2)}) collective-permute-start(bf16[128,256]{1,0:T(8,128)(2,1)S(1)} %get-tuple-element.26), channel_id=1, source_target_pairs={{0,24},{1,7},{2,26},{3,5},{4,28},{5,3},{6,30},{7,1},{8,16},{9,15},... | collective-permute-start | bytes 196616 | tf_op jit(solution)/shard_map/ppermute | solution.py:29
  161.9 3.3 %collective-permute-start.15 = (bf16[128,256]{1,0:T(8,128)(2,1)S(1)}, bf16[128,256]{1,0:T(8,128)(2,1)S(1)}, u32[]{:S(2)}, u32[]{:S(2)}) collective-permute-start(bf16[128,256]{1,0:T(8,128)(2,1)S(1)} %get-tuple-element.27), channel_id=1, source_target_pairs={{0,16},{1,5},{2,18},{3,7},{4,20},{5,1},{6,22},{7,3},{8,24},{9,13},... | collective-permute-start | bytes 196616 | tf_op jit(solution)/shard_map/ppermute | solution.py:29
  165.2 4.4 %collective-permute-done.15 = bf16[128,256]{1,0:T(8,128)(2,1)S(1)} collective-permute-done((bf16[128,256]{1,0:T(8,128)(2,1)S(1)}, bf16[128,256]{1,0:T(8,128)(2,1)S(1)}, u32[]{:S(2)}, u32[]{:S(2)}) %collective-permute-start.15) | collective-permute-done | bytes 65568 | tf_op jit(solution)/shard_map/ppermute | solution.py:29
  (58 shorter events, 23.9 us)
Async XLA Ops:
  2.6 31.8 %all-to-all-start = ((bf16[16,144,128]{2,1,0:T(8,128)(2,1)}), bf16[16,144,128]{2,1,0:T(8,128)(2,1)S(1)}, u32[]{:S(2)}, u32[]{:S(2)}) async-start(bf16[16,144,128]{2,1,0:T(8,128)(2,1)} %get-tuple-element.13), calls=%async_computation | async-start | bytes 1179648 | tf_op jit(solution)/shard_map/all_to_all | solution.py:294
  11.6 33.9 %copy-start.10 = (bf16[128,256]{1,0:T(8,128)(2,1)S(1)}, bf16[128,256]{1,0:T(8,128)(2,1)}, u32[]{:S(2)}) copy-start(bf16[128,256]{1,0:T(8,128)(2,1)} %param.6) | copy-start | bytes 196612
  11.6 33.9 %copy-start.11 = (bf16[128,256]{1,0:T(8,128)(2,1)S(1)}, bf16[128,256]{1,0:T(8,128)(2,1)}, u32[]{:S(2)}) copy-start(bf16[128,256]{1,0:T(8,128)(2,1)} %param.5) | copy-start | bytes 196612
  11.7 22.8 %collective-permute-start.9 = (bf16[4,144,128]{2,1,0:T(8,128)(2,1)S(1)}, bf16[4,144,128]{2,1,0:T(8,128)(2,1)S(1)}, u32[]{:S(2)}, u32[]{:S(2)}) collective-permute-start(bf16[4,144,128]{2,1,0:T(8,128)(2,1)S(1)} %copy-done.12), channel_id=1, source_target_pairs={{0,128},{128,0},{1,129},{129,1},{2,130},{130,2},{3,131},{131,3},{4... | collective-permute-start | bytes 442376 | tf_op jit(solution)/shard_map/ppermute | solution.py:293
  35.4 53.1 %all-to-all-start.1 = ((bf16[16,144,128]{2,1,0:T(8,128)(2,1)}), bf16[16,144,128]{2,1,0:T(8,128)(2,1)S(1)}, u32[]{:S(2)}, u32[]{:S(2)}) async-start(bf16[16,144,128]{2,1,0:T(8,128)(2,1)} %bitcast.5), calls=%async_computation.1 | async-start | bytes 1179648 | tf_op jit(solution)/shard_map/all_to_all | solution.py:296
  45.6 6.9 %collective-permute-start = (bf16[2,128,256]{2,1,0:T(8,128)(2,1)S(1)}, bf16[2,128,256]{2,1,0:T(8,128)(2,1)S(1)}, u32[]{:S(2)}, u32[]{:S(2)}) collective-permute-start(bf16[2,128,256]{2,1,0:T(8,128)(2,1)S(1)} %get-tuple-element.29), channel_id=1, source_target_pairs={{0,2},{1,9},{2,0},{3,11},{4,6},{5,13},{6,4},{7,15},{8,10},{9,1},{1... | collective-permute-start | bytes 393224 | tf_op jit(solution)/shard_map/ppermute | solution.py:29
  52.5 9.8 %collective-permute-start.1 = (bf16[2,2,128,256]{3,2,1,0:T(8,128)(2,1)S(1)}, bf16[2,2,128,256]{3,2,1,0:T(8,128)(2,1)S(1)}, u32[]{:S(2)}, u32[]{:S(2)}) collective-permute-start(bf16[2,2,128,256]{3,2,1,0:T(8,128)(2,1)S(1)} %pad_maximum_fusion.1), channel_id=1, source_target_pairs={{0,4},{1,17},{2,6},{3,19},{4,0},{5,21},{6,2},{7,23},{8,12},{9,25},... | collective-permute-start | bytes 786440 | tf_op jit(solution)/shard_map/ppermute | solution.py:29
  62.3 17.9 %collective-permute-start.4 = (bf16[4,2,128,256]{3,2,1,0:T(8,128)(2,1)S(1)}, bf16[4,2,128,256]{3,2,1,0:T(8,128)(2,1)S(1)}, u32[]{:S(2)}, u32[]{:S(2)}) collective-permute-start(bf16[4,2,128,256]{3,2,1,0:T(8,128)(2,1)S(1)} %pad_maximum_fusion.refs_0_), channel_id=1, source_target_pairs={{0,24},{1,7},{2,26},{3,5},{4,28},{5,3},{6,30},{7,1},{8,16},{9,15},... | collective-permute-start | bytes 1572872 | tf_op jit(solution)/shard_map/ppermute | solution.py:29
  66.9 15.2 %collective-permute-start.3 = (bf16[4,2,128,256]{3,2,1,0:T(8,128)(2,1)S(1)}, bf16[4,2,128,256]{3,2,1,0:T(8,128)(2,1)S(1)}, u32[]{:S(2)}, u32[]{:S(2)}) collective-permute-start(bf16[4,2,128,256]{3,2,1,0:T(8,128)(2,1)S(1)} %pad_maximum_fusion.refs_0_), channel_id=1, source_target_pairs={{0,16},{1,5},{2,18},{3,7},{4,20},{5,1},{6,22},{7,3},{8,24},{9,13},... | collective-permute-start | bytes 1572872 | tf_op jit(solution)/shard_map/ppermute | solution.py:29
  69.7 14.9 %collective-permute-start.2 = (bf16[4,2,128,256]{3,2,1,0:T(8,128)(2,1)S(1)}, bf16[4,2,128,256]{3,2,1,0:T(8,128)(2,1)S(1)}, u32[]{:S(2)}, u32[]{:S(2)}) collective-permute-start(bf16[4,2,128,256]{3,2,1,0:T(8,128)(2,1)S(1)} %pad_maximum_fusion.refs_0_), channel_id=1, source_target_pairs={{0,8},{1,3},{2,10},{3,1},{4,12},{5,7},{6,14},{7,5},{8,0},{9,11},{1... | collective-permute-start | bytes 1572872 | tf_op jit(solution)/shard_map/ppermute | solution.py:29
  72.1 14.4 %collective-permute-start.5 = (bf16[4,2,128,256]{3,2,1,0:T(8,128)(2,1)S(1)}, bf16[4,2,128,256]{3,2,1,0:T(8,128)(2,1)S(1)}, u32[]{:S(2)}, u32[]{:S(2)}) collective-permute-start(bf16[4,2,128,256]{3,2,1,0:T(8,128)(2,1)S(1)} %pad_maximum_fusion.refs_0_), channel_id=1, source_target_pairs={{0,1},{1,0},{2,3},{3,2},{4,5},{5,4},{6,7},{7,6},{8,9},{9,8},{10,11... | collective-permute-start | bytes 1572872 | tf_op jit(solution)/shard_map/ppermute | solution.py:19
  80.2 6.3 %collective-permute-start.8 = (bf16[4,2,128,256]{3,2,1,0:T(8,128)(2,1)S(1)}, bf16[4,2,128,256]{3,2,1,0:T(8,128)(2,1)S(1)}, u32[]{:S(2)}, u32[]{:S(2)}) collective-permute-start(bf16[4,2,128,256]{3,2,1,0:T(8,128)(2,1)S(1)} %collective-permute-done.4.refs_3_), channel_id=1, source_target_pairs={{0,1},{1,0},{2,3},{3,2},{4,5},{5,4},{6,7},{7,6},{8,9},{9,8},{10,11... | collective-permute-start | bytes 1572872 | tf_op jit(solution)/shard_map/ppermute | solution.py:19
  82.1 4.4 %collective-permute-start.7 = (bf16[4,2,128,256]{3,2,1,0:T(8,128)(2,1)S(1)}, bf16[4,2,128,256]{3,2,1,0:T(8,128)(2,1)S(1)}, u32[]{:S(2)}, u32[]{:S(2)}) collective-permute-start(bf16[4,2,128,256]{3,2,1,0:T(8,128)(2,1)S(1)} %collective-permute-done.3.refs_2_), channel_id=1, source_target_pairs={{0,1},{1,0},{2,3},{3,2},{4,5},{5,4},{6,7},{7,6},{8,9},{9,8},{10,11... | collective-permute-start | bytes 1572872 | tf_op jit(solution)/shard_map/ppermute | solution.py:19
  84.6 3.9 %collective-permute-start.6 = (bf16[4,2,128,256]{3,2,1,0:T(8,128)(2,1)S(1)}, bf16[4,2,128,256]{3,2,1,0:T(8,128)(2,1)}, u32[]{:S(2)}, u32[]{:S(2)}) collective-permute-start(bf16[4,2,128,256]{3,2,1,0:T(8,128)(2,1)S(1)} %collective-permute-done.2.refs_1_), channel_id=1, source_target_pairs={{0,1},{1,0},{2,3},{3,2},{4,5},{5,4},{6,7},{7,6},{8,9},{9,8},{10,11... | collective-permute-start | bytes 1572872 | tf_op jit(solution)/shard_map/ppermute | solution.py:19
  95.0 34.0 %all-to-all-start.2 = ((bf16[16,264,128]{2,1,0:T(8,128)(2,1)}), bf16[16,264,128]{2,1,0:T(8,128)(2,1)S(1)}, u32[]{:S(2)}, u32[]{:S(2)}) async-start(bf16[16,264,128]{2,1,0:T(8,128)(2,1)} %get-tuple-element.18), calls=%async_computation.2 | async-start | bytes 2162688 | tf_op jit(solution)/shard_map/all_to_all | solution.py:320
  106.2 31.4 %copy-start.3 = (bf16[4,4,128,256]{3,2,1,0:T(8,128)(2,1)S(1)}, bf16[4,4,128,256]{3,2,1,0:T(8,128)(2,1)}, u32[]{:S(2)}) copy-start(bf16[4,4,128,256]{3,2,1,0:T(8,128)(2,1)} %get-tuple-element.16) | copy-start | bytes 3145732
  106.2 31.4 %collective-permute-start.10 = (bf16[4,4,128,256]{3,2,1,0:T(8,128)(2,1)}, bf16[4,4,128,256]{3,2,1,0:T(8,128)(2,1)S(1)}, u32[]{:S(2)}, u32[]{:S(2)}) collective-permute-start(bf16[4,4,128,256]{3,2,1,0:T(8,128)(2,1)} %get-tuple-element.17), channel_id=1, source_target_pairs={{0,1},{1,0},{2,3},{3,2},{4,5},{5,4},{6,7},{7,6},{8,9},{9,8},{10,11... | collective-permute-start | bytes 3145736 | tf_op jit(solution)/shard_map/ppermute | solution.py:19
  130.0 40.2 %all-to-all-start.3 = ((bf16[4,2,264,128]{3,2,1,0:T(8,128)(2,1)}), bf16[4,2,264,128]{3,2,1,0:T(8,128)(2,1)S(1)}, u32[]{:S(2)}, u32[]{:S(2)}) async-start(bf16[4,2,264,128]{3,2,1,0:T(8,128)(2,1)} %shard_map.86), calls=%async_computation.3 | async-start | bytes 1081344 | tf_op jit(solution)/shard_map/all_to_all | solution.py:322
  137.9 10.0 %collective-permute-start.11 = (bf16[4,128,256]{2,1,0:T(8,128)(2,1)S(1)}, bf16[4,128,256]{2,1,0:T(8,128)(2,1)S(1)}, u32[]{:S(2)}, u32[]{:S(2)}) collective-permute-start(bf16[4,128,256]{2,1,0:T(8,128)(2,1)S(1)} %get-tuple-element.22), channel_id=1, source_target_pairs={{0,2},{1,9},{2,0},{3,11},{4,6},{5,13},{6,4},{7,15},{8,10},{9,1},{1... | collective-permute-start | bytes 786440 | tf_op jit(solution)/shard_map/ppermute | solution.py:29
  141.3 9.5 %collective-permute-start.13 = (bf16[4,128,256]{2,1,0:T(8,128)(2,1)S(1)}, bf16[4,128,256]{2,1,0:T(8,128)(2,1)S(1)}, u32[]{:S(2)}, u32[]{:S(2)}) collective-permute-start(bf16[4,128,256]{2,1,0:T(8,128)(2,1)S(1)} %get-tuple-element.23), channel_id=1, source_target_pairs={{0,6},{1,25},{2,4},{3,27},{4,2},{5,29},{6,0},{7,31},{8,14},{9,17},... | collective-permute-start | bytes 786440 | tf_op jit(solution)/shard_map/ppermute | solution.py:29
  145.4 9.8 %collective-permute-start.12 = (bf16[4,128,256]{2,1,0:T(8,128)(2,1)S(1)}, bf16[4,128,256]{2,1,0:T(8,128)(2,1)S(1)}, u32[]{:S(2)}, u32[]{:S(2)}) collective-permute-start(bf16[4,128,256]{2,1,0:T(8,128)(2,1)S(1)} %get-tuple-element.24), channel_id=1, source_target_pairs={{0,4},{1,17},{2,6},{3,19},{4,0},{5,21},{6,2},{7,23},{8,12},{9,25},... | collective-permute-start | bytes 786440 | tf_op jit(solution)/shard_map/ppermute | solution.py:29
  155.3 9.8 %collective-permute-start.14 = (bf16[128,256]{1,0:T(8,128)(2,1)S(1)}, bf16[128,256]{1,0:T(8,128)(2,1)S(1)}, u32[]{:S(2)}, u32[]{:S(2)}) collective-permute-start(bf16[128,256]{1,0:T(8,128)(2,1)S(1)} %get-tuple-element.25), channel_id=1, source_target_pairs={{0,8},{1,3},{2,10},{3,1},{4,12},{5,7},{6,14},{7,5},{8,0},{9,11},{1... | collective-permute-start | bytes 196616 | tf_op jit(solution)/shard_map/ppermute | solution.py:29
  157.5 7.7 %collective-permute-start.16 = (bf16[128,256]{1,0:T(8,128)(2,1)S(1)}, bf16[128,256]{1,0:T(8,128)(2,1)S(1)}, u32[]{:S(2)}, u32[]{:S(2)}) collective-permute-start(bf16[128,256]{1,0:T(8,128)(2,1)S(1)} %get-tuple-element.26), channel_id=1, source_target_pairs={{0,24},{1,7},{2,26},{3,5},{4,28},{5,3},{6,30},{7,1},{8,16},{9,15},... | collective-permute-start | bytes 196616 | tf_op jit(solution)/shard_map/ppermute | solution.py:29
  161.9 7.7 %collective-permute-start.15 = (bf16[128,256]{1,0:T(8,128)(2,1)S(1)}, bf16[128,256]{1,0:T(8,128)(2,1)S(1)}, u32[]{:S(2)}, u32[]{:S(2)}) collective-permute-start(bf16[128,256]{1,0:T(8,128)(2,1)S(1)} %get-tuple-element.27), channel_id=1, source_target_pairs={{0,16},{1,5},{2,18},{3,7},{4,20},{5,1},{6,22},{7,3},{8,24},{9,13},... | collective-permute-start | bytes 196616 | tf_op jit(solution)/shard_map/ppermute | solution.py:29
  (10 other events, 69.6 us)

commit v6 on v5

--- a/solution.py
+++ b/solution.py
@@ -27,11 +27,6 @@
                 ty, tx = (y, x ^ mask) if c == x_core else (y ^ mask, x)
                 pairs.append(((y * NX + x) * NC + c, (ty * NX + tx) * NC + c))
     return lax.ppermute(value, PLANE, pairs)
-
-
-def line_double(value, x_core):
-    two = jnp.stack([value, moved(value, 1, x_core)])
-    return jnp.concatenate([two, moved(two, 2, x_core)], axis=0)
 
 
 def line_gather(value, x_core):
@@ -296,7 +291,7 @@
     far = lax.all_to_all(far, ("zr", "y"), 0, 0, tiled=True)
 
     block = jnp.stack([inputs, cotangent])
-    line = line_double(block, 0)
+    line = jnp.stack(line_gather(block, 0))
     mine = line_gather(line, 1)
     other = [swapped(m) for m in mine]
 
@@ -313,7 +308,7 @@
         out_specs=[hbm] * 2,
         out_shape=[S(out, BF), turned],
         scratch_shapes=[pltpu.VMEM(s, BF) for s in shapes] + [pltpu.SemaphoreType.DMA((10,))],
-        compiler_params=pltpu.CompilerParams(vmem_limit_bytes=60 * 2**20),
+        compiler_params=pltpu.CompilerParams(vmem_limit_bytes=63 * 2**20),
         name="layer",
     )(*mine, *other, near, far)
 

time: 172 us -> 168 us (0.977)
  waiting for transfers between devices: 60.8 us -> 56 us
    ppermute x11 -> x12, waiting for transfers between devices: 26 us -> 21.2 us  [moved(): return lax.ppermute(value, PLANE, pairs)]
    ppermute x11 -> x12, starting transfers between devices: 37.9 us -> 39.4 us  [moved(): return lax.ppermute(value, PLANE, pairs)]
  transfers between devices with their start and end apart: 21 -> 22, of which waited for: 9 -> 9; matrix products, arithmetic and copies ran while one was open for 1% -> 1% of each run, Pallas kernels for 3% -> 3%
where the time goes in v6:
time: 168 us; the launch traced here: 167 us
  starting transfers between devices  92.5 us (55%)
  waiting for transfers between devices  56 us (33%)
  Pallas kernels  13.5 us (8%)
  local copies, waits for them, and re-layouts  2.8 us (2%)
    ppermute x12, starting transfers between devices, moved(): return lax.ppermute(value, PLANE, pairs)  39.4 us
    ppermute x12, waiting for transfers between devices, moved(): return lax.ppermute(value, PLANE, pairs)  21.2 us
    all_to_all x1, waiting for transfers between devices, per_device(): pieces = lax.all_to_all(pieces, ('zr', 'y'), 0, 0, tiled=True)  20.8 us
    ppermute x1, waiting for transfers between devices, per_device(): far = lax.ppermute(packed, 'zq', [(0, 1), (1, 0)])  13.7 us
    ppermute x5, starting transfers between devices, swapped(): return lax.ppermute(value, 'c', [(0, 1), (1, 0)])  10.2 us
    all_to_all x1, starting transfers between devices, per_device(): far = lax.all_to_all(far, ('zr', 'y'), 0, 0, tiled=True)  10.1 us
    ppermute x1, starting transfers between devices, per_device(): far = lax.ppermute(packed, 'zq', [(0, 1), (1, 0)])  9.04 us
    all_to_all x1, starting transfers between devices, per_device(): near = lax.all_to_all(near, ('zr', 'y'), 0, 0, tiled=True)  8.99 us
  transfers between devices with their start and end apart: 22, of which 9 were waited for; matrix products, arithmetic and copies ran while one was open for 1% of the time, Pallas kernels for 3%

profile of v6, /device:TPU:32, one launch (start us, length us, event | category | flops | bytes accessed | tf_op | source)
XLA Modules:
  0.0 167.1 jit_solution(17647296451684677324)
XLA Ops:
  2.6 9.0 %all-to-all-start = ((bf16[16,144,128]{2,1,0:T(8,128)(2,1)}), bf16[16,144,128]{2,1,0:T(8,128)(2,1)S(1)}, u32[]{:S(2)}, u32[]{:S(2)}) async-start(bf16[16,144,128]{2,1,0:T(8,128)(2,1)} %get-tuple-element.13), calls=%async_computation | async-start | bytes 1179648 | tf_op jit(solution)/shard_map/all_to_all | solution.py:289
  11.7 9.0 %collective-permute-start.10 = (bf16[4,144,128]{2,1,0:T(8,128)(2,1)S(1)}, bf16[4,144,128]{2,1,0:T(8,128)(2,1)S(1)}, u32[]{:S(2)}, u32[]{:S(2)}) collective-permute-start(bf16[4,144,128]{2,1,0:T(8,128)(2,1)S(1)} %copy-done.11), channel_id=1, source_target_pairs={{0,128},{128,0},{1,129},{129,1},{2,130},{130,2},{3,131},{131,3},{4... | collective-permute-start | bytes 442376 | tf_op jit(solution)/shard_map/ppermute | solution.py:288
  20.7 13.7 %collective-permute-done.10 = bf16[4,144,128]{2,1,0:T(8,128)(2,1)S(1)} collective-permute-done((bf16[4,144,128]{2,1,0:T(8,128)(2,1)S(1)}, bf16[4,144,128]{2,1,0:T(8,128)(2,1)S(1)}, u32[]{:S(2)}, u32[]{:S(2)}) %collective-permute-start.10) | collective-permute-done | bytes 147488 | tf_op jit(solution)/shard_map/ppermute | solution.py:288
  35.4 10.1 %all-to-all-start.1 = ((bf16[16,144,128]{2,1,0:T(8,128)(2,1)}), bf16[16,144,128]{2,1,0:T(8,128)(2,1)}, u32[]{:S(2)}, u32[]{:S(2)}) async-start(bf16[16,144,128]{2,1,0:T(8,128)(2,1)} %bitcast.7), calls=%async_computation.1 | async-start | bytes 1179648 | tf_op jit(solution)/shard_map/all_to_all | solution.py:291
  45.6 4.9 %collective-permute-start.1 = (bf16[2,128,256]{2,1,0:T(8,128)(2,1)S(1)}, bf16[2,128,256]{2,1,0:T(8,128)(2,1)S(1)}, u32[]{:S(2)}, u32[]{:S(2)}) collective-permute-start(bf16[2,128,256]{2,1,0:T(8,128)(2,1)S(1)} %get-tuple-element.29), channel_id=1, source_target_pairs={{0,4},{1,17},{2,6},{3,19},{4,0},{5,21},{6,2},{7,23},{8,12},{9,25},... | collective-permute-start | bytes 393224 | tf_op jit(solution)/shard_map/ppermute | solution.py:29
  50.5 2.5 %collective-permute-start = (bf16[2,128,256]{2,1,0:T(8,128)(2,1)S(1)}, bf16[2,128,256]{2,1,0:T(8,128)(2,1)S(1)}, u32[]{:S(2)}, u32[]{:S(2)}) collective-permute-start(bf16[2,128,256]{2,1,0:T(8,128)(2,1)S(1)} %get-tuple-element.29), channel_id=1, source_target_pairs={{0,2},{1,9},{2,0},{3,11},{4,6},{5,13},{6,4},{7,15},{8,10},{9,1},{1... | collective-permute-start | bytes 393224 | tf_op jit(solution)/shard_map/ppermute | solution.py:29
  53.0 2.5 %collective-permute-start.2 = (bf16[2,128,256]{2,1,0:T(8,128)(2,1)S(1)}, bf16[2,128,256]{2,1,0:T(8,128)(2,1)S(1)}, u32[]{:S(2)}, u32[]{:S(2)}) collective-permute-start(bf16[2,128,256]{2,1,0:T(8,128)(2,1)S(1)} %get-tuple-element.29), channel_id=1, source_target_pairs={{0,6},{1,25},{2,4},{3,27},{4,2},{5,29},{6,0},{7,31},{8,14},{9,17},... | collective-permute-start | bytes 393224 | tf_op jit(solution)/shard_map/ppermute | solution.py:29
  57.4 3.7 %collective-permute-done.2 = bf16[2,128,256]{2,1,0:T(8,128)(2,1)S(1)} collective-permute-done((bf16[2,128,256]{2,1,0:T(8,128)(2,1)S(1)}, bf16[2,128,256]{2,1,0:T(8,128)(2,1)S(1)}, u32[]{:S(2)}, u32[]{:S(2)}) %collective-permute-start.2) | collective-permute-done | bytes 131104 | tf_op jit(solution)/shard_map/ppermute | solution.py:29
  61.2 4.6 %collective-permute-start.5 = (bf16[4,2,128,256]{3,2,1,0:T(8,128)(2,1)S(1)}, bf16[4,2,128,256]{3,2,1,0:T(8,128)(2,1)S(1)}, u32[]{:S(2)}, u32[]{:S(2)}) collective-permute-start(bf16[4,2,128,256]{3,2,1,0:T(8,128)(2,1)S(1)} %pad_maximum_fusion.refs_0_), channel_id=1, source_target_pairs={{0,24},{1,7},{2,26},{3,5},{4,28},{5,3},{6,30},{7,1},{8,16},{9,15},... | collective-permute-start | bytes 1572872 | tf_op jit(solution)/shard_map/ppermute | solution.py:29
  65.8 2.8 %collective-permute-start.4 = (bf16[4,2,128,256]{3,2,1,0:T(8,128)(2,1)S(1)}, bf16[4,2,128,256]{3,2,1,0:T(8,128)(2,1)S(1)}, u32[]{:S(2)}, u32[]{:S(2)}) collective-permute-start(bf16[4,2,128,256]{3,2,1,0:T(8,128)(2,1)S(1)} %pad_maximum_fusion.refs_0_), channel_id=1, source_target_pairs={{0,16},{1,5},{2,18},{3,7},{4,20},{5,1},{6,22},{7,3},{8,24},{9,13},... | collective-permute-start | bytes 1572872 | tf_op jit(solution)/shard_map/ppermute | solution.py:29
  68.5 2.5 %collective-permute-start.3 = (bf16[4,2,128,256]{3,2,1,0:T(8,128)(2,1)S(1)}, bf16[4,2,128,256]{3,2,1,0:T(8,128)(2,1)S(1)}, u32[]{:S(2)}, u32[]{:S(2)}) collective-permute-start(bf16[4,2,128,256]{3,2,1,0:T(8,128)(2,1)S(1)} %pad_maximum_fusion.refs_0_), channel_id=1, source_target_pairs={{0,8},{1,3},{2,10},{3,1},{4,12},{5,7},{6,14},{7,5},{8,0},{9,11},{1... | collective-permute-start | bytes 1572872 | tf_op jit(solution)/shard_map/ppermute | solution.py:29
  73.0 6.1 %collective-permute-done.5.refs_3_ = bf16[4,2,128,256]{3,2,1,0:T(8,128)(2,1)S(1)} collective-permute-done((bf16[4,2,128,256]{3,2,1,0:T(8,128)(2,1)S(1)}, bf16[4,2,128,256]{3,2,1,0:T(8,128)(2,1)S(1)}, u32[]{:S(2)}, u32[]{:S(2)}) %collective-permute-start.5) | collective-permute-done | bytes 524320 | tf_op jit(solution)/shard_map/ppermute | solution.py:29
  81.0 2.4 %collective-permute-start.8 = (bf16[4,2,128,256]{3,2,1,0:T(8,128)(2,1)S(1)}, bf16[4,2,128,256]{3,2,1,0:T(8,128)(2,1)S(1)}, u32[]{:S(2)}, u32[]{:S(2)}) collective-permute-start(bf16[4,2,128,256]{3,2,1,0:T(8,128)(2,1)S(1)} %collective-permute-done.4.refs_2_), channel_id=1, source_target_pairs={{0,1},{1,0},{2,3},{3,2},{4,5},{5,4},{6,7},{7,6},{8,9},{9,8},{10,11... | collective-permute-start | bytes 1572872 | tf_op jit(solution)/shard_map/ppermute | solution.py:19
  87.4 5.6 %layer.1 = (bf16[16,264,128]{2,1,0:T(8,128)(2,1)}, bf16[512,176]{1,0:T(8,128)(2,1)}) custom-call(bf16[4,2,128,256]{3,2,1,0:T(8,128)(2,1)} %copy-done.1, bf16[4,2,128,256]{3,2,1,0:T(8,128)(2,1)} %copy-done.5, bf16[4,2,128,256]{3,2,1,0:T(8,128)(2,1)} %copy-done.4, bf16[4,2,128,256]{3,2,1,0:T(8,128)(2,1)} %copy-done.3, bf16[4,2,128,256]{3,2,1,0:T(8,128)(2,1)} %copy-done.6, ...), custom_call_target="tpu_custom_call" | custom-call | tf_op jit(solution)/shard_map/layer/pallas_call | solution.py:305
  93.0 7.2 %all-to-all-start.2 = ((bf16[16,264,128]{2,1,0:T(8,128)(2,1)}), bf16[16,264,128]{2,1,0:T(8,128)(2,1)S(1)}, u32[]{:S(2)}, u32[]{:S(2)}) async-start(bf16[16,264,128]{2,1,0:T(8,128)(2,1)} %get-tuple-element.18), calls=%async_computation.2 | async-start | bytes 2162688 | tf_op jit(solution)/shard_map/all_to_all | solution.py:315
  100.2 4.0 %shard_map.85 = (bf16[4,4,128,256]{3,2,1,0:T(8,128)(2,1)}, bf16[4,4,128,256]{3,2,1,0:T(8,128)(2,1)}) custom-call(bf16[512,176]{1,0:T(8,128)(2,1)} %get-tuple-element.15.refs_0_, bf16[16,144,128]{2,1,0:T(8,128)(2,1)} %copy-done, bf16[16,144,128]{2,1,0:T(8,128)(2,1)} %all-to-all-done.1.refs_9_.refs_2_), custom_call_target="tpu_custom_call" | custom-call | tf_op jit(solution)/shard_map/pallas_call | solution.py:79
  106.3 20.8 %all-to-all-done.2.refs_0_ = bf16[16,264,128]{2,1,0:T(8,128)(2,1)S(1)} async-done(((bf16[16,264,128]{2,1,0:T(8,128)(2,1)}), bf16[16,264,128]{2,1,0:T(8,128)(2,1)S(1)}, u32[]{:S(2)}, u32[]{:S(2)}) %all-to-all-start.2) | async-done | bytes 1081376 | tf_op jit(solution)/shard_map/all_to_all | solution.py:315
  128.1 7.6 %all-to-all-start.3 = ((bf16[4,2,264,128]{3,2,1,0:T(8,128)(2,1)}), bf16[4,2,264,128]{3,2,1,0:T(8,128)(2,1)S(1)}, u32[]{:S(2)}, u32[]{:S(2)}) async-start(bf16[4,2,264,128]{3,2,1,0:T(8,128)(2,1)} %shard_map.86), calls=%async_computation.3 | async-start | bytes 1081344 | tf_op jit(solution)/shard_map/all_to_all | solution.py:317
  138.2 3.1 %collective-permute-start.14 = (bf16[4,128,256]{2,1,0:T(8,128)(2,1)S(1)}, bf16[4,128,256]{2,1,0:T(8,128)(2,1)S(1)}, u32[]{:S(2)}, u32[]{:S(2)}) collective-permute-start(bf16[4,128,256]{2,1,0:T(8,128)(2,1)S(1)} %get-tuple-element.23), channel_id=1, source_target_pairs={{0,6},{1,25},{2,4},{3,27},{4,2},{5,29},{6,0},{7,31},{8,14},{9,17},... | collective-permute-start | bytes 786440 | tf_op jit(solution)/shard_map/ppermute | solution.py:29
  141.3 4.6 %collective-permute-start.13 = (bf16[4,128,256]{2,1,0:T(8,128)(2,1)S(1)}, bf16[4,128,256]{2,1,0:T(8,128)(2,1)S(1)}, u32[]{:S(2)}, u32[]{:S(2)}) collective-permute-start(bf16[4,128,256]{2,1,0:T(8,128)(2,1)S(1)} %get-tuple-element.24), channel_id=1, source_target_pairs={{0,4},{1,17},{2,6},{3,19},{4,0},{5,21},{6,2},{7,23},{8,12},{9,25},... | collective-permute-start | bytes 786440 | tf_op jit(solution)/shard_map/ppermute | solution.py:29
  147.7 3.4 %collective-permute-done.13 = bf16[4,128,256]{2,1,0:T(8,128)(2,1)S(1)} collective-permute-done((bf16[4,128,256]{2,1,0:T(8,128)(2,1)S(1)}, bf16[4,128,256]{2,1,0:T(8,128)(2,1)S(1)}, u32[]{:S(2)}, u32[]{:S(2)}) %collective-permute-start.13) | collective-permute-done | bytes 262176 | tf_op jit(solution)/shard_map/ppermute | solution.py:29
  153.4 4.4 %collective-permute-start.17 = (bf16[128,256]{1,0:T(8,128)(2,1)S(1)}, bf16[128,256]{1,0:T(8,128)(2,1)S(1)}, u32[]{:S(2)}, u32[]{:S(2)}) collective-permute-start(bf16[128,256]{1,0:T(8,128)(2,1)S(1)} %get-tuple-element.26), channel_id=1, source_target_pairs={{0,24},{1,7},{2,26},{3,5},{4,28},{5,3},{6,30},{7,1},{8,16},{9,15},... | collective-permute-start | bytes 196616 | tf_op jit(solution)/shard_map/ppermute | solution.py:29
  157.8 3.3 %collective-permute-start.16 = (bf16[128,256]{1,0:T(8,128)(2,1)S(1)}, bf16[128,256]{1,0:T(8,128)(2,1)S(1)}, u32[]{:S(2)}, u32[]{:S(2)}) collective-permute-start(bf16[128,256]{1,0:T(8,128)(2,1)S(1)} %get-tuple-element.27), channel_id=1, source_target_pairs={{0,16},{1,5},{2,18},{3,7},{4,20},{5,1},{6,22},{7,3},{8,24},{9,13},... | collective-permute-start | bytes 196616 | tf_op jit(solution)/shard_map/ppermute | solution.py:29
  161.1 4.4 %collective-permute-done.16 = bf16[128,256]{1,0:T(8,128)(2,1)S(1)} collective-permute-done((bf16[128,256]{1,0:T(8,128)(2,1)S(1)}, bf16[128,256]{1,0:T(8,128)(2,1)S(1)}, u32[]{:S(2)}, u32[]{:S(2)}) %collective-permute-start.16) | collective-permute-done | bytes 65568 | tf_op jit(solution)/shard_map/ppermute | solution.py:29
  (57 shorter events, 23.9 us)
Async XLA Ops:
  2.6 31.8 %all-to-all-start = ((bf16[16,144,128]{2,1,0:T(8,128)(2,1)}), bf16[16,144,128]{2,1,0:T(8,128)(2,1)S(1)}, u32[]{:S(2)}, u32[]{:S(2)}) async-start(bf16[16,144,128]{2,1,0:T(8,128)(2,1)} %get-tuple-element.13), calls=%async_computation | async-start | bytes 1179648 | tf_op jit(solution)/shard_map/all_to_all | solution.py:289
  11.6 33.9 %copy-start.9 = (bf16[128,256]{1,0:T(8,128)(2,1)S(1)}, bf16[128,256]{1,0:T(8,128)(2,1)}, u32[]{:S(2)}) copy-start(bf16[128,256]{1,0:T(8,128)(2,1)} %param.6) | copy-start | bytes 196612
  11.6 33.9 %copy-start.10 = (bf16[128,256]{1,0:T(8,128)(2,1)S(1)}, bf16[128,256]{1,0:T(8,128)(2,1)}, u32[]{:S(2)}) copy-start(bf16[128,256]{1,0:T(8,128)(2,1)} %param.5) | copy-start | bytes 196612
  11.7 22.8 %collective-permute-start.10 = (bf16[4,144,128]{2,1,0:T(8,128)(2,1)S(1)}, bf16[4,144,128]{2,1,0:T(8,128)(2,1)S(1)}, u32[]{:S(2)}, u32[]{:S(2)}) collective-permute-start(bf16[4,144,128]{2,1,0:T(8,128)(2,1)S(1)} %copy-done.11), channel_id=1, source_target_pairs={{0,128},{128,0},{1,129},{129,1},{2,130},{130,2},{3,131},{131,3},{4... | collective-permute-start | bytes 442376 | tf_op jit(solution)/shard_map/ppermute | solution.py:288
  35.4 52.0 %all-to-all-start.1 = ((bf16[16,144,128]{2,1,0:T(8,128)(2,1)}), bf16[16,144,128]{2,1,0:T(8,128)(2,1)}, u32[]{:S(2)}, u32[]{:S(2)}) async-start(bf16[16,144,128]{2,1,0:T(8,128)(2,1)} %bitcast.7), calls=%async_computation.1 | async-start | bytes 1179648 | tf_op jit(solution)/shard_map/all_to_all | solution.py:291
  45.6 9.9 %collective-permute-start.1 = (bf16[2,128,256]{2,1,0:T(8,128)(2,1)S(1)}, bf16[2,128,256]{2,1,0:T(8,128)(2,1)S(1)}, u32[]{:S(2)}, u32[]{:S(2)}) collective-permute-start(bf16[2,128,256]{2,1,0:T(8,128)(2,1)S(1)} %get-tuple-element.29), channel_id=1, source_target_pairs={{0,4},{1,17},{2,6},{3,19},{4,0},{5,21},{6,2},{7,23},{8,12},{9,25},... | collective-permute-start | bytes 393224 | tf_op jit(solution)/shard_map/ppermute | solution.py:29
  50.5 6.9 %collective-permute-start = (bf16[2,128,256]{2,1,0:T(8,128)(2,1)S(1)}, bf16[2,128,256]{2,1,0:T(8,128)(2,1)S(1)}, u32[]{:S(2)}, u32[]{:S(2)}) collective-permute-start(bf16[2,128,256]{2,1,0:T(8,128)(2,1)S(1)} %get-tuple-element.29), channel_id=1, source_target_pairs={{0,2},{1,9},{2,0},{3,11},{4,6},{5,13},{6,4},{7,15},{8,10},{9,1},{1... | collective-permute-start | bytes 393224 | tf_op jit(solution)/shard_map/ppermute | solution.py:29
  53.0 8.1 %collective-permute-start.2 = (bf16[2,128,256]{2,1,0:T(8,128)(2,1)S(1)}, bf16[2,128,256]{2,1,0:T(8,128)(2,1)S(1)}, u32[]{:S(2)}, u32[]{:S(2)}) collective-permute-start(bf16[2,128,256]{2,1,0:T(8,128)(2,1)S(1)} %get-tuple-element.29), channel_id=1, source_target_pairs={{0,6},{1,25},{2,4},{3,27},{4,2},{5,29},{6,0},{7,31},{8,14},{9,17},... | collective-permute-start | bytes 393224 | tf_op jit(solution)/shard_map/ppermute | solution.py:29
  61.2 17.9 %collective-permute-start.5 = (bf16[4,2,128,256]{3,2,1,0:T(8,128)(2,1)S(1)}, bf16[4,2,128,256]{3,2,1,0:T(8,128)(2,1)S(1)}, u32[]{:S(2)}, u32[]{:S(2)}) collective-permute-start(bf16[4,2,128,256]{3,2,1,0:T(8,128)(2,1)S(1)} %pad_maximum_fusion.refs_0_), channel_id=1, source_target_pairs={{0,24},{1,7},{2,26},{3,5},{4,28},{5,3},{6,30},{7,1},{8,16},{9,15},... | collective-permute-start | bytes 1572872 | tf_op jit(solution)/shard_map/ppermute | solution.py:29
  65.8 15.2 %collective-permute-start.4 = (bf16[4,2,128,256]{3,2,1,0:T(8,128)(2,1)S(1)}, bf16[4,2,128,256]{3,2,1,0:T(8,128)(2,1)S(1)}, u32[]{:S(2)}, u32[]{:S(2)}) collective-permute-start(bf16[4,2,128,256]{3,2,1,0:T(8,128)(2,1)S(1)} %pad_maximum_fusion.refs_0_), channel_id=1, source_target_pairs={{0,16},{1,5},{2,18},{3,7},{4,20},{5,1},{6,22},{7,3},{8,24},{9,13},... | collective-permute-start | bytes 1572872 | tf_op jit(solution)/shard_map/ppermute | solution.py:29
  68.5 14.9 %collective-permute-start.3 = (bf16[4,2,128,256]{3,2,1,0:T(8,128)(2,1)S(1)}, bf16[4,2,128,256]{3,2,1,0:T(8,128)(2,1)S(1)}, u32[]{:S(2)}, u32[]{:S(2)}) collective-permute-start(bf16[4,2,128,256]{3,2,1,0:T(8,128)(2,1)S(1)} %pad_maximum_fusion.refs_0_), channel_id=1, source_target_pairs={{0,8},{1,3},{2,10},{3,1},{4,12},{5,7},{6,14},{7,5},{8,0},{9,11},{1... | collective-permute-start | bytes 1572872 | tf_op jit(solution)/shard_map/ppermute | solution.py:29
  71.0 14.4 %collective-permute-start.6 = (bf16[4,2,128,256]{3,2,1,0:T(8,128)(2,1)S(1)}, bf16[4,2,128,256]{3,2,1,0:T(8,128)(2,1)S(1)}, u32[]{:S(2)}, u32[]{:S(2)}) collective-permute-start(bf16[4,2,128,256]{3,2,1,0:T(8,128)(2,1)S(1)} %pad_maximum_fusion.refs_0_), channel_id=1, source_target_pairs={{0,1},{1,0},{2,3},{3,2},{4,5},{5,4},{6,7},{7,6},{8,9},{9,8},{10,11... | collective-permute-start | bytes 1572872 | tf_op jit(solution)/shard_map/ppermute | solution.py:19
  79.1 6.3 %collective-permute-start.9 = (bf16[4,2,128,256]{3,2,1,0:T(8,128)(2,1)S(1)}, bf16[4,2,128,256]{3,2,1,0:T(8,128)(2,1)S(1)}, u32[]{:S(2)}, u32[]{:S(2)}) collective-permute-start(bf16[4,2,128,256]{3,2,1,0:T(8,128)(2,1)S(1)} %collective-permute-done.5.refs_3_), channel_id=1, source_target_pairs={{0,1},{1,0},{2,3},{3,2},{4,5},{5,4},{6,7},{7,6},{8,9},{9,8},{10,11... | collective-permute-start | bytes 1572872 | tf_op jit(solution)/shard_map/ppermute | solution.py:19
  81.0 4.4 %collective-permute-start.8 = (bf16[4,2,128,256]{3,2,1,0:T(8,128)(2,1)S(1)}, bf16[4,2,128,256]{3,2,1,0:T(8,128)(2,1)S(1)}, u32[]{:S(2)}, u32[]{:S(2)}) collective-permute-start(bf16[4,2,128,256]{3,2,1,0:T(8,128)(2,1)S(1)} %collective-permute-done.4.refs_2_), channel_id=1, source_target_pairs={{0,1},{1,0},{2,3},{3,2},{4,5},{5,4},{6,7},{7,6},{8,9},{9,8},{10,11... | collective-permute-start | bytes 1572872 | tf_op jit(solution)/shard_map/ppermute | solution.py:19
  83.5 3.9 %collective-permute-start.7 = (bf16[4,2,128,256]{3,2,1,0:T(8,128)(2,1)S(1)}, bf16[4,2,128,256]{3,2,1,0:T(8,128)(2,1)}, u32[]{:S(2)}, u32[]{:S(2)}) collective-permute-start(bf16[4,2,128,256]{3,2,1,0:T(8,128)(2,1)S(1)} %collective-permute-done.3.refs_1_), channel_id=1, source_target_pairs={{0,1},{1,0},{2,3},{3,2},{4,5},{5,4},{6,7},{7,6},{8,9},{9,8},{10,11... | collective-permute-start | bytes 1572872 | tf_op jit(solution)/shard_map/ppermute | solution.py:19
  93.0 34.1 %all-to-all-start.2 = ((bf16[16,264,128]{2,1,0:T(8,128)(2,1)}), bf16[16,264,128]{2,1,0:T(8,128)(2,1)S(1)}, u32[]{:S(2)}, u32[]{:S(2)}) async-start(bf16[16,264,128]{2,1,0:T(8,128)(2,1)} %get-tuple-element.18), calls=%async_computation.2 | async-start | bytes 2162688 | tf_op jit(solution)/shard_map/all_to_all | solution.py:315
  104.2 31.5 %collective-permute-start.11 = (bf16[4,4,128,256]{3,2,1,0:T(8,128)(2,1)}, bf16[4,4,128,256]{3,2,1,0:T(8,128)(2,1)S(1)}, u32[]{:S(2)}, u32[]{:S(2)}) collective-permute-start(bf16[4,4,128,256]{3,2,1,0:T(8,128)(2,1)} %get-tuple-element.17), channel_id=1, source_target_pairs={{0,1},{1,0},{2,3},{3,2},{4,5},{5,4},{6,7},{7,6},{8,9},{9,8},{10,11... | collective-permute-start | bytes 3145736 | tf_op jit(solution)/shard_map/ppermute | solution.py:19
  128.1 38.0 %all-to-all-start.3 = ((bf16[4,2,264,128]{3,2,1,0:T(8,128)(2,1)}), bf16[4,2,264,128]{3,2,1,0:T(8,128)(2,1)S(1)}, u32[]{:S(2)}, u32[]{:S(2)}) async-start(bf16[4,2,264,128]{3,2,1,0:T(8,128)(2,1)} %shard_map.86), calls=%async_computation.3 | async-start | bytes 1081344 | tf_op jit(solution)/shard_map/all_to_all | solution.py:317
  136.1 9.8 %collective-permute-start.12 = (bf16[4,128,256]{2,1,0:T(8,128)(2,1)S(1)}, bf16[4,128,256]{2,1,0:T(8,128)(2,1)S(1)}, u32[]{:S(2)}, u32[]{:S(2)}) collective-permute-start(bf16[4,128,256]{2,1,0:T(8,128)(2,1)S(1)} %get-tuple-element.22), channel_id=1, source_target_pairs={{0,2},{1,9},{2,0},{3,11},{4,6},{5,13},{6,4},{7,15},{8,10},{9,1},{1... | collective-permute-start | bytes 786440 | tf_op jit(solution)/shard_map/ppermute | solution.py:29
  138.2 9.5 %collective-permute-start.14 = (bf16[4,128,256]{2,1,0:T(8,128)(2,1)S(1)}, bf16[4,128,256]{2,1,0:T(8,128)(2,1)S(1)}, u32[]{:S(2)}, u32[]{:S(2)}) collective-permute-start(bf16[4,128,256]{2,1,0:T(8,128)(2,1)S(1)} %get-tuple-element.23), channel_id=1, source_target_pairs={{0,6},{1,25},{2,4},{3,27},{4,2},{5,29},{6,0},{7,31},{8,14},{9,17},... | collective-permute-start | bytes 786440 | tf_op jit(solution)/shard_map/ppermute | solution.py:29
  141.3 9.8 %collective-permute-start.13 = (bf16[4,128,256]{2,1,0:T(8,128)(2,1)S(1)}, bf16[4,128,256]{2,1,0:T(8,128)(2,1)S(1)}, u32[]{:S(2)}, u32[]{:S(2)}) collective-permute-start(bf16[4,128,256]{2,1,0:T(8,128)(2,1)S(1)} %get-tuple-element.24), channel_id=1, source_target_pairs={{0,4},{1,17},{2,6},{3,19},{4,0},{5,21},{6,2},{7,23},{8,12},{9,25},... | collective-permute-start | bytes 786440 | tf_op jit(solution)/shard_map/ppermute | solution.py:29
  151.2 9.8 %collective-permute-start.15 = (bf16[128,256]{1,0:T(8,128)(2,1)S(1)}, bf16[128,256]{1,0:T(8,128)(2,1)S(1)}, u32[]{:S(2)}, u32[]{:S(2)}) collective-permute-start(bf16[128,256]{1,0:T(8,128)(2,1)S(1)} %get-tuple-element.25), channel_id=1, source_target_pairs={{0,8},{1,3},{2,10},{3,1},{4,12},{5,7},{6,14},{7,5},{8,0},{9,11},{1... | collective-permute-start | bytes 196616 | tf_op jit(solution)/shard_map/ppermute | solution.py:29
  153.4 7.7 %collective-permute-start.17 = (bf16[128,256]{1,0:T(8,128)(2,1)S(1)}, bf16[128,256]{1,0:T(8,128)(2,1)S(1)}, u32[]{:S(2)}, u32[]{:S(2)}) collective-permute-start(bf16[128,256]{1,0:T(8,128)(2,1)S(1)} %get-tuple-element.26), channel_id=1, source_target_pairs={{0,24},{1,7},{2,26},{3,5},{4,28},{5,3},{6,30},{7,1},{8,16},{9,15},... | collective-permute-start | bytes 196616 | tf_op jit(solution)/shard_map/ppermute | solution.py:29
  157.8 7.7 %collective-permute-start.16 = (bf16[128,256]{1,0:T(8,128)(2,1)S(1)}, bf16[128,256]{1,0:T(8,128)(2,1)S(1)}, u32[]{:S(2)}, u32[]{:S(2)}) collective-permute-start(bf16[128,256]{1,0:T(8,128)(2,1)S(1)} %get-tuple-element.27), channel_id=1, source_target_pairs={{0,16},{1,5},{2,18},{3,7},{4,20},{5,1},{6,22},{7,3},{8,24},{9,13},... | collective-permute-start | bytes 196616 | tf_op jit(solution)/shard_map/ppermute | solution.py:29
  (10 other events, 93.1 us)

commit v7 on v6

--- a/solution.py
+++ b/solution.py
@@ -292,8 +292,11 @@
 
     block = jnp.stack([inputs, cotangent])
     line = jnp.stack(line_gather(block, 0))
-    mine = line_gather(line, 1)
-    other = [swapped(m) for m in mine]
+    other = [swapped(line)]
+    mine = [line]
+    for m in (1, 2, 3):
+        mine.append(moved(line, m, 1))
+        other.append(swapped(mine[-1]))
 
     tiles = S((4, 4, rows, cols), BF)
     turned = S((NY * rows, 2 * hid), BF)

time: 168 us -> 168 us (level)
  no operation moved by 1% of the time
where the time goes in v7:
time: 168 us; the launch traced here: 167 us
  starting transfers between devices  92.5 us (55%)
  waiting for transfers between devices  56 us (33%)
  Pallas kernels  13.5 us (8%)
  local copies, waits for them, and re-layouts  2.8 us (2%)
    ppermute x12, starting transfers between devices, moved(): return lax.ppermute(value, PLANE, pairs)  39.4 us
    ppermute x12, waiting for transfers between devices, moved(): return lax.ppermute(value, PLANE, pairs)  21.2 us
    all_to_all x1, waiting for transfers between devices, per_device(): pieces = lax.all_to_all(pieces, ('zr', 'y'), 0, 0, tiled=True)  20.8 us
    ppermute x1, waiting for transfers between devices, per_device(): far = lax.ppermute(packed, 'zq', [(0, 1), (1, 0)])  13.7 us
    ppermute x5, starting transfers between devices, swapped(): return lax.ppermute(value, 'c', [(0, 1), (1, 0)])  10.2 us
    all_to_all x1, starting transfers between devices, per_device(): far = lax.all_to_all(far, ('zr', 'y'), 0, 0, tiled=True)  10.1 us
    ppermute x1, starting transfers between devices, per_device(): far = lax.ppermute(packed, 'zq', [(0, 1), (1, 0)])  9.04 us
    all_to_all x1, starting transfers between devices, per_device(): near = lax.all_to_all(near, ('zr', 'y'), 0, 0, tiled=True)  8.99 us
  transfers between devices with their start and end apart: 22, of which 9 were waited for; matrix products, arithmetic and copies ran while one was open for 1% of the time, Pallas kernels for 3%

profile of v7, /device:TPU:32, one launch (start us, length us, event | category | flops | bytes accessed | tf_op | source)
XLA Modules:
  0.0 167.1 jit_solution(17647296451684677324)
XLA Ops:
  2.6 9.0 %all-to-all-start = ((bf16[16,144,128]{2,1,0:T(8,128)(2,1)}), bf16[16,144,128]{2,1,0:T(8,128)(2,1)S(1)}, u32[]{:S(2)}, u32[]{:S(2)}) async-start(bf16[16,144,128]{2,1,0:T(8,128)(2,1)} %get-tuple-element.13), calls=%async_computation | async-start | bytes 1179648 | tf_op jit(solution)/shard_map/all_to_all | solution.py:289
  11.7 9.0 %collective-permute-start.10 = (bf16[4,144,128]{2,1,0:T(8,128)(2,1)S(1)}, bf16[4,144,128]{2,1,0:T(8,128)(2,1)S(1)}, u32[]{:S(2)}, u32[]{:S(2)}) collective-permute-start(bf16[4,144,128]{2,1,0:T(8,128)(2,1)S(1)} %copy-done.11), channel_id=1, source_target_pairs={{0,128},{128,0},{1,129},{129,1},{2,130},{130,2},{3,131},{131,3},{4... | collective-permute-start | bytes 442376 | tf_op jit(solution)/shard_map/ppermute | solution.py:288
  20.7 13.7 %collective-permute-done.10 = bf16[4,144,128]{2,1,0:T(8,128)(2,1)S(1)} collective-permute-done((bf16[4,144,128]{2,1,0:T(8,128)(2,1)S(1)}, bf16[4,144,128]{2,1,0:T(8,128)(2,1)S(1)}, u32[]{:S(2)}, u32[]{:S(2)}) %collective-permute-start.10) | collective-permute-done | bytes 147488 | tf_op jit(solution)/shard_map/ppermute | solution.py:288
  35.4 10.1 %all-to-all-start.1 = ((bf16[16,144,128]{2,1,0:T(8,128)(2,1)}), bf16[16,144,128]{2,1,0:T(8,128)(2,1)}, u32[]{:S(2)}, u32[]{:S(2)}) async-start(bf16[16,144,128]{2,1,0:T(8,128)(2,1)} %bitcast.7), calls=%async_computation.1 | async-start | bytes 1179648 | tf_op jit(solution)/shard_map/all_to_all | solution.py:291
  45.6 4.9 %collective-permute-start.1 = (bf16[2,128,256]{2,1,0:T(8,128)(2,1)S(1)}, bf16[2,128,256]{2,1,0:T(8,128)(2,1)S(1)}, u32[]{:S(2)}, u32[]{:S(2)}) collective-permute-start(bf16[2,128,256]{2,1,0:T(8,128)(2,1)S(1)} %get-tuple-element.29), channel_id=1, source_target_pairs={{0,4},{1,17},{2,6},{3,19},{4,0},{5,21},{6,2},{7,23},{8,12},{9,25},... | collective-permute-start | bytes 393224 | tf_op jit(solution)/shard_map/ppermute | solution.py:29
  50.5 2.5 %collective-permute-start = (bf16[2,128,256]{2,1,0:T(8,128)(2,1)S(1)}, bf16[2,128,256]{2,1,0:T(8,128)(2,1)S(1)}, u32[]{:S(2)}, u32[]{:S(2)}) collective-permute-start(bf16[2,128,256]{2,1,0:T(8,128)(2,1)S(1)} %get-tuple-element.29), channel_id=1, source_target_pairs={{0,2},{1,9},{2,0},{3,11},{4,6},{5,13},{6,4},{7,15},{8,10},{9,1},{1... | collective-permute-start | bytes 393224 | tf_op jit(solution)/shard_map/ppermute | solution.py:29
  53.0 2.5 %collective-permute-start.2 = (bf16[2,128,256]{2,1,0:T(8,128)(2,1)S(1)}, bf16[2,128,256]{2,1,0:T(8,128)(2,1)S(1)}, u32[]{:S(2)}, u32[]{:S(2)}) collective-permute-start(bf16[2,128,256]{2,1,0:T(8,128)(2,1)S(1)} %get-tuple-element.29), channel_id=1, source_target_pairs={{0,6},{1,25},{2,4},{3,27},{4,2},{5,29},{6,0},{7,31},{8,14},{9,17},... | collective-permute-start | bytes 393224 | tf_op jit(solution)/shard_map/ppermute | solution.py:29
  57.4 3.7 %collective-permute-done.2 = bf16[2,128,256]{2,1,0:T(8,128)(2,1)S(1)} collective-permute-done((bf16[2,128,256]{2,1,0:T(8,128)(2,1)S(1)}, bf16[2,128,256]{2,1,0:T(8,128)(2,1)S(1)}, u32[]{:S(2)}, u32[]{:S(2)}) %collective-permute-start.2) | collective-permute-done | bytes 131104 | tf_op jit(solution)/shard_map/ppermute | solution.py:29
  61.2 4.6 %collective-permute-start.5 = (bf16[4,2,128,256]{3,2,1,0:T(8,128)(2,1)S(1)}, bf16[4,2,128,256]{3,2,1,0:T(8,128)(2,1)S(1)}, u32[]{:S(2)}, u32[]{:S(2)}) collective-permute-start(bf16[4,2,128,256]{3,2,1,0:T(8,128)(2,1)S(1)} %pad_maximum_fusion.refs_0_), channel_id=1, source_target_pairs={{0,24},{1,7},{2,26},{3,5},{4,28},{5,3},{6,30},{7,1},{8,16},{9,15},... | collective-permute-start | bytes 1572872 | tf_op jit(solution)/shard_map/ppermute | solution.py:29
  65.8 2.8 %collective-permute-start.4 = (bf16[4,2,128,256]{3,2,1,0:T(8,128)(2,1)S(1)}, bf16[4,2,128,256]{3,2,1,0:T(8,128)(2,1)S(1)}, u32[]{:S(2)}, u32[]{:S(2)}) collective-permute-start(bf16[4,2,128,256]{3,2,1,0:T(8,128)(2,1)S(1)} %pad_maximum_fusion.refs_0_), channel_id=1, source_target_pairs={{0,16},{1,5},{2,18},{3,7},{4,20},{5,1},{6,22},{7,3},{8,24},{9,13},... | collective-permute-start | bytes 1572872 | tf_op jit(solution)/shard_map/ppermute | solution.py:29
  68.5 2.5 %collective-permute-start.3 = (bf16[4,2,128,256]{3,2,1,0:T(8,128)(2,1)S(1)}, bf16[4,2,128,256]{3,2,1,0:T(8,128)(2,1)S(1)}, u32[]{:S(2)}, u32[]{:S(2)}) collective-permute-start(bf16[4,2,128,256]{3,2,1,0:T(8,128)(2,1)S(1)} %pad_maximum_fusion.refs_0_), channel_id=1, source_target_pairs={{0,8},{1,3},{2,10},{3,1},{4,12},{5,7},{6,14},{7,5},{8,0},{9,11},{1... | collective-permute-start | bytes 1572872 | tf_op jit(solution)/shard_map/ppermute | solution.py:29
  73.0 6.1 %collective-permute-done.5.refs_3_ = bf16[4,2,128,256]{3,2,1,0:T(8,128)(2,1)S(1)} collective-permute-done((bf16[4,2,128,256]{3,2,1,0:T(8,128)(2,1)S(1)}, bf16[4,2,128,256]{3,2,1,0:T(8,128)(2,1)S(1)}, u32[]{:S(2)}, u32[]{:S(2)}) %collective-permute-start.5) | collective-permute-done | bytes 524320 | tf_op jit(solution)/shard_map/ppermute | solution.py:29
  81.0 2.4 %collective-permute-start.8 = (bf16[4,2,128,256]{3,2,1,0:T(8,128)(2,1)S(1)}, bf16[4,2,128,256]{3,2,1,0:T(8,128)(2,1)S(1)}, u32[]{:S(2)}, u32[]{:S(2)}) collective-permute-start(bf16[4,2,128,256]{3,2,1,0:T(8,128)(2,1)S(1)} %collective-permute-done.4.refs_2_), channel_id=1, source_target_pairs={{0,1},{1,0},{2,3},{3,2},{4,5},{5,4},{6,7},{7,6},{8,9},{9,8},{10,11... | collective-permute-start | bytes 1572872 | tf_op jit(solution)/shard_map/ppermute | solution.py:19
  87.4 5.6 %layer.1 = (bf16[16,264,128]{2,1,0:T(8,128)(2,1)}, bf16[512,176]{1,0:T(8,128)(2,1)}) custom-call(bf16[4,2,128,256]{3,2,1,0:T(8,128)(2,1)} %copy-done.1, bf16[4,2,128,256]{3,2,1,0:T(8,128)(2,1)} %copy-done.5, bf16[4,2,128,256]{3,2,1,0:T(8,128)(2,1)} %copy-done.4, bf16[4,2,128,256]{3,2,1,0:T(8,128)(2,1)} %copy-done.3, bf16[4,2,128,256]{3,2,1,0:T(8,128)(2,1)} %copy-done.6, ...), custom_call_target="tpu_custom_call" | custom-call | tf_op jit(solution)/shard_map/layer/pallas_call | solution.py:308
  93.0 7.2 %all-to-all-start.2 = ((bf16[16,264,128]{2,1,0:T(8,128)(2,1)}), bf16[16,264,128]{2,1,0:T(8,128)(2,1)S(1)}, u32[]{:S(2)}, u32[]{:S(2)}) async-start(bf16[16,264,128]{2,1,0:T(8,128)(2,1)} %get-tuple-element.18), calls=%async_computation.2 | async-start | bytes 2162688 | tf_op jit(solution)/shard_map/all_to_all | solution.py:318
  100.2 4.0 %shard_map.85 = (bf16[4,4,128,256]{3,2,1,0:T(8,128)(2,1)}, bf16[4,4,128,256]{3,2,1,0:T(8,128)(2,1)}) custom-call(bf16[512,176]{1,0:T(8,128)(2,1)} %get-tuple-element.15.refs_0_, bf16[16,144,128]{2,1,0:T(8,128)(2,1)} %copy-done, bf16[16,144,128]{2,1,0:T(8,128)(2,1)} %all-to-all-done.1.refs_9_.refs_2_), custom_call_target="tpu_custom_call" | custom-call | tf_op jit(solution)/shard_map/pallas_call | solution.py:79
  106.3 20.8 %all-to-all-done.2.refs_0_ = bf16[16,264,128]{2,1,0:T(8,128)(2,1)S(1)} async-done(((bf16[16,264,128]{2,1,0:T(8,128)(2,1)}), bf16[16,264,128]{2,1,0:T(8,128)(2,1)S(1)}, u32[]{:S(2)}, u32[]{:S(2)}) %all-to-all-start.2) | async-done | bytes 1081376 | tf_op jit(solution)/shard_map/all_to_all | solution.py:318
  128.1 7.6 %all-to-all-start.3 = ((bf16[4,2,264,128]{3,2,1,0:T(8,128)(2,1)}), bf16[4,2,264,128]{3,2,1,0:T(8,128)(2,1)S(1)}, u32[]{:S(2)}, u32[]{:S(2)}) async-start(bf16[4,2,264,128]{3,2,1,0:T(8,128)(2,1)} %shard_map.86), calls=%async_computation.3 | async-start | bytes 1081344 | tf_op jit(solution)/shard_map/all_to_all | solution.py:320
  138.2 3.1 %collective-permute-start.14 = (bf16[4,128,256]{2,1,0:T(8,128)(2,1)S(1)}, bf16[4,128,256]{2,1,0:T(8,128)(2,1)S(1)}, u32[]{:S(2)}, u32[]{:S(2)}) collective-permute-start(bf16[4,128,256]{2,1,0:T(8,128)(2,1)S(1)} %get-tuple-element.23), channel_id=1, source_target_pairs={{0,6},{1,25},{2,4},{3,27},{4,2},{5,29},{6,0},{7,31},{8,14},{9,17},... | collective-permute-start | bytes 786440 | tf_op jit(solution)/shard_map/ppermute | solution.py:29
  141.3 4.6 %collective-permute-start.13 = (bf16[4,128,256]{2,1,0:T(8,128)(2,1)S(1)}, bf16[4,128,256]{2,1,0:T(8,128)(2,1)S(1)}, u32[]{:S(2)}, u32[]{:S(2)}) collective-permute-start(bf16[4,128,256]{2,1,0:T(8,128)(2,1)S(1)} %get-tuple-element.24), channel_id=1, source_target_pairs={{0,4},{1,17},{2,6},{3,19},{4,0},{5,21},{6,2},{7,23},{8,12},{9,25},... | collective-permute-start | bytes 786440 | tf_op jit(solution)/shard_map/ppermute | solution.py:29
  147.7 3.4 %collective-permute-done.13 = bf16[4,128,256]{2,1,0:T(8,128)(2,1)S(1)} collective-permute-done((bf16[4,128,256]{2,1,0:T(8,128)(2,1)S(1)}, bf16[4,128,256]{2,1,0:T(8,128)(2,1)S(1)}, u32[]{:S(2)}, u32[]{:S(2)}) %collective-permute-start.13) | collective-permute-done | bytes 262176 | tf_op jit(solution)/shard_map/ppermute | solution.py:29
  153.4 4.4 %collective-permute-start.17 = (bf16[128,256]{1,0:T(8,128)(2,1)S(1)}, bf16[128,256]{1,0:T(8,128)(2,1)S(1)}, u32[]{:S(2)}, u32[]{:S(2)}) collective-permute-start(bf16[128,256]{1,0:T(8,128)(2,1)S(1)} %get-tuple-element.26), channel_id=1, source_target_pairs={{0,24},{1,7},{2,26},{3,5},{4,28},{5,3},{6,30},{7,1},{8,16},{9,15},... | collective-permute-start | bytes 196616 | tf_op jit(solution)/shard_map/ppermute | solution.py:29
  157.8 3.3 %collective-permute-start.16 = (bf16[128,256]{1,0:T(8,128)(2,1)S(1)}, bf16[128,256]{1,0:T(8,128)(2,1)S(1)}, u32[]{:S(2)}, u32[]{:S(2)}) collective-permute-start(bf16[128,256]{1,0:T(8,128)(2,1)S(1)} %get-tuple-element.27), channel_id=1, source_target_pairs={{0,16},{1,5},{2,18},{3,7},{4,20},{5,1},{6,22},{7,3},{8,24},{9,13},... | collective-permute-start | bytes 196616 | tf_op jit(solution)/shard_map/ppermute | solution.py:29
  161.1 4.4 %collective-permute-done.16 = bf16[128,256]{1,0:T(8,128)(2,1)S(1)} collective-permute-done((bf16[128,256]{1,0:T(8,128)(2,1)S(1)}, bf16[128,256]{1,0:T(8,128)(2,1)S(1)}, u32[]{:S(2)}, u32[]{:S(2)}) %collective-permute-start.16) | collective-permute-done | bytes 65568 | tf_op jit(solution)/shard_map/ppermute | solution.py:29
  (57 shorter events, 23.9 us)
Async XLA Ops:
  2.6 31.8 %all-to-all-start = ((bf16[16,144,128]{2,1,0:T(8,128)(2,1)}), bf16[16,144,128]{2,1,0:T(8,128)(2,1)S(1)}, u32[]{:S(2)}, u32[]{:S(2)}) async-start(bf16[16,144,128]{2,1,0:T(8,128)(2,1)} %get-tuple-element.13), calls=%async_computation | async-start | bytes 1179648 | tf_op jit(solution)/shard_map/all_to_all | solution.py:289
  11.6 33.9 %copy-start.9 = (bf16[128,256]{1,0:T(8,128)(2,1)S(1)}, bf16[128,256]{1,0:T(8,128)(2,1)}, u32[]{:S(2)}) copy-start(bf16[128,256]{1,0:T(8,128)(2,1)} %param.6) | copy-start | bytes 196612
  11.6 33.9 %copy-start.10 = (bf16[128,256]{1,0:T(8,128)(2,1)S(1)}, bf16[128,256]{1,0:T(8,128)(2,1)}, u32[]{:S(2)}) copy-start(bf16[128,256]{1,0:T(8,128)(2,1)} %param.5) | copy-start | bytes 196612
  11.7 22.8 %collective-permute-start.10 = (bf16[4,144,128]{2,1,0:T(8,128)(2,1)S(1)}, bf16[4,144,128]{2,1,0:T(8,128)(2,1)S(1)}, u32[]{:S(2)}, u32[]{:S(2)}) collective-permute-start(bf16[4,144,128]{2,1,0:T(8,128)(2,1)S(1)} %copy-done.11), channel_id=1, source_target_pairs={{0,128},{128,0},{1,129},{129,1},{2,130},{130,2},{3,131},{131,3},{4... | collective-permute-start | bytes 442376 | tf_op jit(solution)/shard_map/ppermute | solution.py:288
  35.4 52.0 %all-to-all-start.1 = ((bf16[16,144,128]{2,1,0:T(8,128)(2,1)}), bf16[16,144,128]{2,1,0:T(8,128)(2,1)}, u32[]{:S(2)}, u32[]{:S(2)}) async-start(bf16[16,144,128]{2,1,0:T(8,128)(2,1)} %bitcast.7), calls=%async_computation.1 | async-start | bytes 1179648 | tf_op jit(solution)/shard_map/all_to_all | solution.py:291
  45.6 9.9 %collective-permute-start.1 = (bf16[2,128,256]{2,1,0:T(8,128)(2,1)S(1)}, bf16[2,128,256]{2,1,0:T(8,128)(2,1)S(1)}, u32[]{:S(2)}, u32[]{:S(2)}) collective-permute-start(bf16[2,128,256]{2,1,0:T(8,128)(2,1)S(1)} %get-tuple-element.29), channel_id=1, source_target_pairs={{0,4},{1,17},{2,6},{3,19},{4,0},{5,21},{6,2},{7,23},{8,12},{9,25},... | collective-permute-start | bytes 393224 | tf_op jit(solution)/shard_map/ppermute | solution.py:29
  50.5 6.9 %collective-permute-start = (bf16[2,128,256]{2,1,0:T(8,128)(2,1)S(1)}, bf16[2,128,256]{2,1,0:T(8,128)(2,1)S(1)}, u32[]{:S(2)}, u32[]{:S(2)}) collective-permute-start(bf16[2,128,256]{2,1,0:T(8,128)(2,1)S(1)} %get-tuple-element.29), channel_id=1, source_target_pairs={{0,2},{1,9},{2,0},{3,11},{4,6},{5,13},{6,4},{7,15},{8,10},{9,1},{1... | collective-permute-start | bytes 393224 | tf_op jit(solution)/shard_map/ppermute | solution.py:29
  53.0 8.1 %collective-permute-start.2 = (bf16[2,128,256]{2,1,0:T(8,128)(2,1)S(1)}, bf16[2,128,256]{2,1,0:T(8,128)(2,1)S(1)}, u32[]{:S(2)}, u32[]{:S(2)}) collective-permute-start(bf16[2,128,256]{2,1,0:T(8,128)(2,1)S(1)} %get-tuple-element.29), channel_id=1, source_target_pairs={{0,6},{1,25},{2,4},{3,27},{4,2},{5,29},{6,0},{7,31},{8,14},{9,17},... | collective-permute-start | bytes 393224 | tf_op jit(solution)/shard_map/ppermute | solution.py:29
  61.2 17.9 %collective-permute-start.5 = (bf16[4,2,128,256]{3,2,1,0:T(8,128)(2,1)S(1)}, bf16[4,2,128,256]{3,2,1,0:T(8,128)(2,1)S(1)}, u32[]{:S(2)}, u32[]{:S(2)}) collective-permute-start(bf16[4,2,128,256]{3,2,1,0:T(8,128)(2,1)S(1)} %pad_maximum_fusion.refs_0_), channel_id=1, source_target_pairs={{0,24},{1,7},{2,26},{3,5},{4,28},{5,3},{6,30},{7,1},{8,16},{9,15},... | collective-permute-start | bytes 1572872 | tf_op jit(solution)/shard_map/ppermute | solution.py:29
  65.8 15.2 %collective-permute-start.4 = (bf16[4,2,128,256]{3,2,1,0:T(8,128)(2,1)S(1)}, bf16[4,2,128,256]{3,2,1,0:T(8,128)(2,1)S(1)}, u32[]{:S(2)}, u32[]{:S(2)}) collective-permute-start(bf16[4,2,128,256]{3,2,1,0:T(8,128)(2,1)S(1)} %pad_maximum_fusion.refs_0_), channel_id=1, source_target_pairs={{0,16},{1,5},{2,18},{3,7},{4,20},{5,1},{6,22},{7,3},{8,24},{9,13},... | collective-permute-start | bytes 1572872 | tf_op jit(solution)/shard_map/ppermute | solution.py:29
  68.5 14.9 %collective-permute-start.3 = (bf16[4,2,128,256]{3,2,1,0:T(8,128)(2,1)S(1)}, bf16[4,2,128,256]{3,2,1,0:T(8,128)(2,1)S(1)}, u32[]{:S(2)}, u32[]{:S(2)}) collective-permute-start(bf16[4,2,128,256]{3,2,1,0:T(8,128)(2,1)S(1)} %pad_maximum_fusion.refs_0_), channel_id=1, source_target_pairs={{0,8},{1,3},{2,10},{3,1},{4,12},{5,7},{6,14},{7,5},{8,0},{9,11},{1... | collective-permute-start | bytes 1572872 | tf_op jit(solution)/shard_map/ppermute | solution.py:29
  71.0 14.4 %collective-permute-start.6 = (bf16[4,2,128,256]{3,2,1,0:T(8,128)(2,1)S(1)}, bf16[4,2,128,256]{3,2,1,0:T(8,128)(2,1)S(1)}, u32[]{:S(2)}, u32[]{:S(2)}) collective-permute-start(bf16[4,2,128,256]{3,2,1,0:T(8,128)(2,1)S(1)} %pad_maximum_fusion.refs_0_), channel_id=1, source_target_pairs={{0,1},{1,0},{2,3},{3,2},{4,5},{5,4},{6,7},{7,6},{8,9},{9,8},{10,11... | collective-permute-start | bytes 1572872 | tf_op jit(solution)/shard_map/ppermute | solution.py:19
  79.1 6.3 %collective-permute-start.9 = (bf16[4,2,128,256]{3,2,1,0:T(8,128)(2,1)S(1)}, bf16[4,2,128,256]{3,2,1,0:T(8,128)(2,1)S(1)}, u32[]{:S(2)}, u32[]{:S(2)}) collective-permute-start(bf16[4,2,128,256]{3,2,1,0:T(8,128)(2,1)S(1)} %collective-permute-done.5.refs_3_), channel_id=1, source_target_pairs={{0,1},{1,0},{2,3},{3,2},{4,5},{5,4},{6,7},{7,6},{8,9},{9,8},{10,11... | collective-permute-start | bytes 1572872 | tf_op jit(solution)/shard_map/ppermute | solution.py:19
  81.0 4.4 %collective-permute-start.8 = (bf16[4,2,128,256]{3,2,1,0:T(8,128)(2,1)S(1)}, bf16[4,2,128,256]{3,2,1,0:T(8,128)(2,1)S(1)}, u32[]{:S(2)}, u32[]{:S(2)}) collective-permute-start(bf16[4,2,128,256]{3,2,1,0:T(8,128)(2,1)S(1)} %collective-permute-done.4.refs_2_), channel_id=1, source_target_pairs={{0,1},{1,0},{2,3},{3,2},{4,5},{5,4},{6,7},{7,6},{8,9},{9,8},{10,11... | collective-permute-start | bytes 1572872 | tf_op jit(solution)/shard_map/ppermute | solution.py:19
  83.5 3.9 %collective-permute-start.7 = (bf16[4,2,128,256]{3,2,1,0:T(8,128)(2,1)S(1)}, bf16[4,2,128,256]{3,2,1,0:T(8,128)(2,1)}, u32[]{:S(2)}, u32[]{:S(2)}) collective-permute-start(bf16[4,2,128,256]{3,2,1,0:T(8,128)(2,1)S(1)} %collective-permute-done.3.refs_1_), channel_id=1, source_target_pairs={{0,1},{1,0},{2,3},{3,2},{4,5},{5,4},{6,7},{7,6},{8,9},{9,8},{10,11... | collective-permute-start | bytes 1572872 | tf_op jit(solution)/shard_map/ppermute | solution.py:19
  93.0 34.1 %all-to-all-start.2 = ((bf16[16,264,128]{2,1,0:T(8,128)(2,1)}), bf16[16,264,128]{2,1,0:T(8,128)(2,1)S(1)}, u32[]{:S(2)}, u32[]{:S(2)}) async-start(bf16[16,264,128]{2,1,0:T(8,128)(2,1)} %get-tuple-element.18), calls=%async_computation.2 | async-start | bytes 2162688 | tf_op jit(solution)/shard_map/all_to_all | solution.py:318
  104.2 31.5 %collective-permute-start.11 = (bf16[4,4,128,256]{3,2,1,0:T(8,128)(2,1)}, bf16[4,4,128,256]{3,2,1,0:T(8,128)(2,1)S(1)}, u32[]{:S(2)}, u32[]{:S(2)}) collective-permute-start(bf16[4,4,128,256]{3,2,1,0:T(8,128)(2,1)} %get-tuple-element.17), channel_id=1, source_target_pairs={{0,1},{1,0},{2,3},{3,2},{4,5},{5,4},{6,7},{7,6},{8,9},{9,8},{10,11... | collective-permute-start | bytes 3145736 | tf_op jit(solution)/shard_map/ppermute | solution.py:19
  128.1 38.0 %all-to-all-start.3 = ((bf16[4,2,264,128]{3,2,1,0:T(8,128)(2,1)}), bf16[4,2,264,128]{3,2,1,0:T(8,128)(2,1)S(1)}, u32[]{:S(2)}, u32[]{:S(2)}) async-start(bf16[4,2,264,128]{3,2,1,0:T(8,128)(2,1)} %shard_map.86), calls=%async_computation.3 | async-start | bytes 1081344 | tf_op jit(solution)/shard_map/all_to_all | solution.py:320
  136.1 9.8 %collective-permute-start.12 = (bf16[4,128,256]{2,1,0:T(8,128)(2,1)S(1)}, bf16[4,128,256]{2,1,0:T(8,128)(2,1)S(1)}, u32[]{:S(2)}, u32[]{:S(2)}) collective-permute-start(bf16[4,128,256]{2,1,0:T(8,128)(2,1)S(1)} %get-tuple-element.22), channel_id=1, source_target_pairs={{0,2},{1,9},{2,0},{3,11},{4,6},{5,13},{6,4},{7,15},{8,10},{9,1},{1... | collective-permute-start | bytes 786440 | tf_op jit(solution)/shard_map/ppermute | solution.py:29
  138.2 9.5 %collective-permute-start.14 = (bf16[4,128,256]{2,1,0:T(8,128)(2,1)S(1)}, bf16[4,128,256]{2,1,0:T(8,128)(2,1)S(1)}, u32[]{:S(2)}, u32[]{:S(2)}) collective-permute-start(bf16[4,128,256]{2,1,0:T(8,128)(2,1)S(1)} %get-tuple-element.23), channel_id=1, source_target_pairs={{0,6},{1,25},{2,4},{3,27},{4,2},{5,29},{6,0},{7,31},{8,14},{9,17},... | collective-permute-start | bytes 786440 | tf_op jit(solution)/shard_map/ppermute | solution.py:29
  141.3 9.8 %collective-permute-start.13 = (bf16[4,128,256]{2,1,0:T(8,128)(2,1)S(1)}, bf16[4,128,256]{2,1,0:T(8,128)(2,1)S(1)}, u32[]{:S(2)}, u32[]{:S(2)}) collective-permute-start(bf16[4,128,256]{2,1,0:T(8,128)(2,1)S(1)} %get-tuple-element.24), channel_id=1, source_target_pairs={{0,4},{1,17},{2,6},{3,19},{4,0},{5,21},{6,2},{7,23},{8,12},{9,25},... | collective-permute-start | bytes 786440 | tf_op jit(solution)/shard_map/ppermute | solution.py:29
  151.2 9.8 %collective-permute-start.15 = (bf16[128,256]{1,0:T(8,128)(2,1)S(1)}, bf16[128,256]{1,0:T(8,128)(2,1)S(1)}, u32[]{:S(2)}, u32[]{:S(2)}) collective-permute-start(bf16[128,256]{1,0:T(8,128)(2,1)S(1)} %get-tuple-element.25), channel_id=1, source_target_pairs={{0,8},{1,3},{2,10},{3,1},{4,12},{5,7},{6,14},{7,5},{8,0},{9,11},{1... | collective-permute-start | bytes 196616 | tf_op jit(solution)/shard_map/ppermute | solution.py:29
  153.4 7.7 %collective-permute-start.17 = (bf16[128,256]{1,0:T(8,128)(2,1)S(1)}, bf16[128,256]{1,0:T(8,128)(2,1)S(1)}, u32[]{:S(2)}, u32[]{:S(2)}) collective-permute-start(bf16[128,256]{1,0:T(8,128)(2,1)S(1)} %get-tuple-element.26), channel_id=1, source_target_pairs={{0,24},{1,7},{2,26},{3,5},{4,28},{5,3},{6,30},{7,1},{8,16},{9,15},... | collective-permute-start | bytes 196616 | tf_op jit(solution)/shard_map/ppermute | solution.py:29
  157.8 7.7 %collective-permute-start.16 = (bf16[128,256]{1,0:T(8,128)(2,1)S(1)}, bf16[128,256]{1,0:T(8,128)(2,1)S(1)}, u32[]{:S(2)}, u32[]{:S(2)}) collective-permute-start(bf16[128,256]{1,0:T(8,128)(2,1)S(1)} %get-tuple-element.27), channel_id=1, source_target_pairs={{0,16},{1,5},{2,18},{3,7},{4,20},{5,1},{6,22},{7,3},{8,24},{9,13},... | collective-permute-start | bytes 196616 | tf_op jit(solution)/shard_map/ppermute | solution.py:29
  (10 other events, 93.1 us)
